TPU v7x, 512 devices: a whole 4x8x8 slice. The times are simulated.
512 devices in a mesh: sp: 64 (over z, y), tp: 8 (over x, core).
Axes of the slice: x: 4, y: 8, z: 8, core: 2. Of those that a mesh axis runs over, the one named last changes fastest.
Arguments:
- residual: bfloat16 [2048, 16384], P('tp', 'sp'), may hold values from -6 to 6
- values: bfloat16 [16384, 4096], P('sp', 'tp'), may hold values from -6 to 6
- gate_input: bfloat16 [16384, 4096], P('sp', 'tp'), may hold values from -6 to 6
- group_keys: bfloat16 [16384, 3072], P('sp', 'tp'), may hold values from -6 to 6
- time_step: float32 [64, 16384], P('tp', 'sp'), may hold values from -8 to 14
- decay_rate: float32 [64], P('tp'), may hold values from 0 to 2
- skip_gain: float32 [64], P('tp'), may hold values from 0.25 to 2
- conv_values: bfloat16 [4, 4096], P(None, 'tp'), may hold values from -3 to 3
- conv_keys: bfloat16 [4, 3072], P(None, 'tp'), may hold values from -3 to 3
- mix_gain: float32 [4096], P('tp'), may hold values from 0.1 to 1.9
- out_weight: bfloat16 [4096, 2048], P('tp'), may hold values from -0.09375 to 0.09375
- norm_gain: float32 [2048], replicated, may hold values from 0.1 to 1.9
- hidden_gate: bfloat16 [2048, 5120], P('sp', 'tp'), may hold values from -0.125 to 0.125
- hidden_up: bfloat16 [2048, 5120], P('sp', 'tp'), may hold values from -0.125 to 0.125
- hidden_conv: bfloat16 [2, 3, 5120], P(None, None, 'tp'), may hold values from -3.5 to 3.5
- hidden_down: bfloat16 [5120, 2048], P('tp', 'sp'), may hold values from -0.078125 to 0.078125
Outputs:
- layer_out: bfloat16 [2048, 16384], P('tp', 'sp')
All inputs are finite; a program needn't handle non-finite values.
Results may differ from a plain program's by a relative error of at most 0.019.
Values may be sent and summed in bfloat16 or wider, within the bound.
No kernel may reach another device: no remote copies, remote signals or barrier semaphores. Data moves between devices by JAX's collectives and lax.ppermute only.
A program may use at most 64 MiB of HBM per device.

v0:
```python
import jax
import jax.numpy as jnp
from jax import lax
from jax.sharding import Mesh
from jax.sharding import PartitionSpec as P

GROUP_HEADS = 8
HEAD_SIZE = 64
STATE_WIDE = 128
STATE_NARROW = 64
BLOCK = 128
SP = ("sp_0", "sp_1")


NORM_FLOOR = 0.1


def side_by_side(arrays, axis, dim, along):
    ends, at = ([], 0)
    for a in arrays[:-1]:
        at += a.shape[along]
        ends.append(at)
    both = jnp.concatenate(arrays, axis=along)
    return tuple(jnp.split(lax.all_gather(both, axis, axis=dim, tiled=True), ends, axis=along))


def from_behind(value, axis, steps):
    count = lax.axis_size(axis)
    first, last = (max(0, -steps), min(count, count - steps))
    return lax.ppermute(value, axis, [(source, source + steps) for source in range(first, last)])


def nothing_yet(shard, identity):
    return jax.tree.map(
        lambda a, e: jnp.broadcast_to(jnp.asarray(e, a.dtype), a.shape), shard, identity
    )


def gathered_once(shard, axis):
    leaves = jax.tree.leaves(shard)
    sequence = sorted(range(len(leaves)), key=lambda k: -leaves[k].size)
    width = (1, *leaves[sequence[0]].shape)[-1]
    lines = [
        jnp.pad(leaves[k].reshape(-1), (0, -leaves[k].size % width)).reshape(-1, width)
        for k in sequence
    ]
    both, at, found = (lax.all_gather(jnp.concatenate(lines), axis), 0, {})
    for k, line in zip(sequence, lines):
        piece = both[:, at : at + len(line)].reshape(len(both), -1)
        found[k] = piece[:, : leaves[k].size].reshape(-1, *leaves[k].shape)
        at += len(line)
    numbers = iter(range(len(leaves)))
    return jax.tree.map(lambda _: found[next(numbers)], shard)


def prefix_by_axis(shard, axes, combine, identity):
    before = start = nothing_yet(shard, identity)
    subtotal = shard
    for axis in reversed(axes):
        count, place = (lax.axis_size(axis), lax.axis_index(axis))
        pieces = gathered_once(
            jax.tree.map(
                lambda part, kind: part.astype(kind),
                subtotal,
                (jnp.bfloat16, jnp.bfloat16, jnp.bfloat16, jnp.bfloat16),
            ),
            axis,
        )
        inside, subtotal = (start, start)
        for k in range(count):
            passed = k < place
            subtotal = combine(
                subtotal, jax.tree.map(lambda part, own: part[k].astype(own.dtype), pieces, shard)
            )
            inside = jax.tree.map(lambda new, old: jnp.where(passed, new, old), subtotal, inside)
        before = combine(inside, before)
    return before


def from_everyone(shard, axis):
    copies = jnp.broadcast_to(shard, (lax.axis_size(axis), *shard.shape))
    return lax.all_to_all(copies, axis, split_axis=0, concat_axis=0, tiled=True)


def taken_together(shard, axis):
    everything = from_everyone(shard, axis)
    return jnp.sum(everything, axis=0)


def split_up(shard, dim, count):
    lengths = shard.shape
    parts = shard.reshape(*lengths[:dim], count, lengths[dim] // count, *lengths[dim + 1 :])
    return jnp.moveaxis(parts, dim, 0)


def sent_and_summed(shard, axis, dim):
    count = lax.axis_size(axis)
    parts = lax.all_to_all(split_up(shard, dim, count), axis, 0, 0, tiled=True)
    return jnp.sum(parts.astype(jnp.float32), axis=0)


def laid_out(parts, dim):
    parts = jnp.moveaxis(parts, 0, dim)
    lengths = parts.shape
    return parts.reshape(*lengths[:dim], lengths[dim] * lengths[dim + 1], *lengths[dim + 2 :])


def collect(shard, axis, dim):
    return laid_out(from_everyone(shard, axis), dim)


def tap_sum(joined, weights, row_count):
    summed = weights[0].astype(jnp.float32) * joined[0:row_count]
    for tap_index in range(1, weights.shape[0]):
        summed = (
            summed
            + weights[tap_index].astype(jnp.float32) * joined[tap_index : tap_index + row_count]
        )
    return summed


def block_heads(inputs, in_keys, out_keys, deltas, decay_rates, skip_table, carried):
    length = inputs.shape[0]
    running = jnp.cumsum(-decay_rates * deltas, axis=0)
    weighted = inputs * deltas[..., None]
    scores = jnp.einsum("ign,jgn->gij", out_keys, in_keys)
    by_head = jnp.transpose(running, (1, 2, 0))
    between = by_head[..., :, None] - by_head[..., None, :]
    lower_mask = jnp.tril(jnp.ones((length, length), dtype=bool))
    decays = jnp.exp(jnp.where(lower_mask, between, -jnp.inf))
    inside = jnp.einsum("ghij,jghp->ighp", scores[:, None] * decays, weighted)
    carried_part = jnp.einsum("ign,ghpn->ighp", out_keys, carried) * jnp.exp(running)[..., None]
    to_end = jnp.exp(by_head[..., -1:] - by_head)
    fresh_state = jnp.einsum("jgn,ghj,jghp->ghpn", in_keys, to_end, weighted)
    updated = carried * jnp.exp(by_head[..., -1])[..., None, None] + fresh_state
    return (inside + carried_part + inputs * skip_table[..., None], updated)


def contract_rows(left, right):
    return lax.dot_general(
        left, right, (((0,), (0,)), ((), ())), preferred_element_type=jnp.float32
    )


def combine_states(first_part, second_part):
    return (
        first_part[0] * second_part[0],
        first_part[1] * second_part[0][..., None, None] + second_part[1],
        first_part[2] * second_part[2],
        first_part[3] * second_part[2][..., None, None] + second_part[3],
    )


def hidden_taps(both_pre, edge_cols, taps, row_count):
    joined_hidden = jnp.concatenate([edge_cols, both_pre], axis=2).astype(jnp.float32)
    conv_total = taps[:, 0, :, None].astype(jnp.float32) * joined_hidden[:, :, 0:row_count]
    for tap_index in range(1, taps.shape[1]):
        conv_total = (
            conv_total
            + taps[:, tap_index, :, None].astype(jnp.float32)
            * joined_hidden[:, :, tap_index : tap_index + row_count]
        )
    return (jax.nn.silu(conv_total[0]) * conv_total[1]).astype(jnp.bfloat16)


def local(
    residual,
    values,
    gate_input,
    group_keys,
    time_step,
    decay_rate,
    skip_gain,
    conv_values,
    conv_keys,
    mix_gain,
    out_weight,
    norm_gain,
    hidden_gate,
    hidden_up,
    hidden_conv,
    hidden_down,
):
    early_gate, early_up = side_by_side((hidden_gate, hidden_up), SP, 0, 1)
    early_down = lax.all_gather(hidden_down, SP, axis=1, tiled=True)
    row_count = values.shape[0]
    value_cols = values.shape[1]
    tap_count = conv_values.shape[0]
    tail_rows = jnp.concatenate(
        [values[row_count - tap_count + 1 :], group_keys[row_count - tap_count + 1 :]], axis=1
    )
    before_rows = from_behind(tail_rows, SP, 1)
    joined_values = jnp.concatenate([before_rows[:, :value_cols], values], axis=0).astype(
        jnp.float32
    )
    joined_keys = jnp.concatenate([before_rows[:, value_cols:], group_keys], axis=0).astype(
        jnp.float32
    )
    group_count = group_keys.shape[1] // (2 * STATE_WIDE + 2 * STATE_NARROW)
    inputs = jax.nn.silu(tap_sum(joined_values, conv_values, row_count)).reshape(
        row_count, group_count, GROUP_HEADS, HEAD_SIZE
    )
    key_rows = jax.nn.silu(tap_sum(joined_keys, conv_keys, row_count)).reshape(
        row_count, group_count, -1
    )
    deltas = jax.nn.softplus(time_step).T.reshape(row_count, group_count, GROUP_HEADS)
    rate_table = decay_rate.reshape(group_count, GROUP_HEADS)
    skip_table = skip_gain.reshape(group_count, GROUP_HEADS)
    running = jnp.cumsum(-rate_table * deltas, axis=0)
    half_heads = GROUP_HEADS // 2
    wide_end = 2 * STATE_WIDE

    def run_kind(head_first, head_last, key_first, state_width):
        in_keys = key_rows[..., key_first : key_first + state_width]
        out_keys = key_rows[..., key_first + state_width : key_first + 2 * state_width]
        carried = jnp.zeros(
            (group_count, head_last - head_first, HEAD_SIZE, state_width), jnp.float32
        )
        block_outs = []
        for block_index in range(row_count // BLOCK):
            row_first = block_index * BLOCK
            row_last = row_first + BLOCK
            block_out, carried = block_heads(
                inputs[row_first:row_last, :, head_first:head_last],
                in_keys[row_first:row_last],
                out_keys[row_first:row_last],
                deltas[row_first:row_last, :, head_first:head_last],
                rate_table[:, head_first:head_last],
                skip_table[:, head_first:head_last],
                carried,
            )
            block_outs.append(block_out)
        return (jnp.concatenate(block_outs, axis=0), carried, out_keys)

    wide_local, wide_state, wide_keys = run_kind(0, half_heads, 0, STATE_WIDE)
    narrow_local, narrow_state, narrow_keys = run_kind(
        half_heads, GROUP_HEADS, wide_end, STATE_NARROW
    )
    span_decay = jnp.exp(running[-1])
    start_value = (
        jnp.ones_like(span_decay[:, :half_heads]),
        jnp.zeros_like(wide_state),
        jnp.ones_like(span_decay[:, half_heads:]),
        jnp.zeros_like(narrow_state),
    )
    incoming = prefix_by_axis(
        (span_decay[:, :half_heads], wide_state, span_decay[:, half_heads:], narrow_state),
        SP,
        combine_states,
        start_value,
    )
    growth = jnp.exp(running)[..., None]
    wide_out = (
        wide_local
        + jnp.einsum("ign,ghpn->ighp", wide_keys, incoming[1]) * growth[:, :, :half_heads]
    )
    narrow_out = (
        narrow_local
        + jnp.einsum("ign,ghpn->ighp", narrow_keys, incoming[3]) * growth[:, :, half_heads:]
    )
    mixer_out = jnp.concatenate([wide_out, narrow_out], axis=2).reshape(row_count, value_cols)
    gated_out = mixer_out * jax.nn.silu(gate_input.astype(jnp.float32))
    squares = taken_together(jnp.sum(gated_out * gated_out, axis=1), "tp")
    inverse_rms = lax.rsqrt(squares / (value_cols * lax.axis_size("tp")) + NORM_FLOOR)
    normed = (gated_out * inverse_rms[:, None] * mix_gain).astype(jnp.bfloat16)
    mixer_sum = sent_and_summed(
        lax.dot_general(
            out_weight, normed, (((0,), (1,)), ((), ())), preferred_element_type=jnp.float32
        ).astype(jnp.bfloat16),
        "tp",
        0,
    )
    own_merged = (residual.astype(jnp.float32) + mixer_sum).astype(jnp.bfloat16)
    merged = collect(own_merged, "tp", 0)
    merged_wide = merged.astype(jnp.float32)
    inverse_norm = lax.rsqrt(jnp.mean(merged_wide * merged_wide, axis=0) + NORM_FLOOR)
    lifted = (merged_wide * inverse_norm[None, :] * norm_gain[:, None]).astype(jnp.bfloat16)
    edge_taps = hidden_conv.shape[1]
    gate_pre = contract_rows(early_gate, lifted)
    up_pre = contract_rows(early_up, lifted)
    both_pre = jnp.stack([gate_pre, up_pre]).astype(jnp.bfloat16)
    edge_cols = from_behind(both_pre[:, :, row_count - edge_taps + 1 :], SP, 1)
    hidden = hidden_taps(both_pre, edge_cols, hidden_conv, row_count)
    hidden_sum = sent_and_summed(contract_rows(early_down, hidden).astype(jnp.bfloat16), "tp", 0)
    return (own_merged.astype(jnp.float32) + hidden_sum).astype(jnp.bfloat16)


def solution(mesh):
    split = Mesh(mesh.devices.reshape(8, 8, mesh.shape["tp"]), ("sp_0", "sp_1", "tp"))
    placed = (
        P("tp", SP),
        P(SP, "tp"),
        P(SP, "tp"),
        P(SP, "tp"),
        P("tp", SP),
        P("tp"),
        P("tp"),
        P(None, "tp"),
        P(None, "tp"),
        P("tp"),
        P("tp", None),
        P(),
        P(SP, "tp"),
        P(SP, "tp"),
        P(None, None, "tp"),
        P("tp", SP),
    )
    return jax.shard_map(local, mesh=split, in_specs=placed, out_specs=P("tp", SP), check_vma=False)
```

profile of v0, /device:TPU:1, one launch (start us, length us, event | category | flops | bytes accessed | tf_op | source)
XLA Modules:
  0.0 267.2 jit_solution(17710106803041564632)
XLA Ops:
  6.5 0.9 slice.547
  8.1 4.0 %collective-permute-start = (bf16[3,896]{1,0:T(4,128)(2,1)S(1)}, bf16[3,896]{1,0:T(4,128)(2,1)S(1)}, u32[]{:S(2)}, u32[]{:S(2)}) collective-permute-start(bf16[3,896]{1,0:T(4,128)(2,1)S(1)} %pad_maximum_fusion.2), channel_id=1, source_target_pairs={{0,8},{8,16},{16,24},{24,32},{32,40},{40,48},{48,56},{56,64},{64,7... | collective-permute-start | bytes 16136 | tf_op jit(solution)/shard_map/ppermute | solution.py:30
  12.1 1.4 pad_maximum_fusion.1
  13.6 0.8 negate_bitcast_fusion.1
  17.3 0.9 convert_reduce_fusion.5
  18.2 0.8 slice_convert_fusion.3
  19.6 0.8 fusion.189
  21.5 1.4 slice_bitcast_fusion.20
  31.5 23.6 %all-gather.2 = bf16[8,386,128]{2,1,0:T(8,128)(2,1)S(1)} all-gather(bf16[1,386,128]{2,1,0:T(8,128)(2,1)S(1)} %maximum_bitcast_fusion), channel_id=2, replica_groups=mesh['sp_0'=8,'sp_1'=8,'tp'=8] {'sp_1'}, dimensions={0}, use_global_device_ids=true | all-gather | bytes 889344 | tf_op jit(solution)/shard_map/all_gather | solution.py:47
  57.6 1.6 convert_bitcast_fusion.24
  59.9 0.7 mul.1448
  64.8 0.7 mul.1297
  67.0 0.7 mul.1301
  69.2 0.7 mul.1305
  70.6 0.7 mul.1458
  71.3 0.7 mul.1309
  76.4 1.1 fusion.171
  77.6 31.6 %all-gather.3 = bf16[8,386,128]{2,1,0:T(8,128)(2,1)S(1)} all-gather(bf16[1,386,128]{2,1,0:T(8,128)(2,1)S(1)} %maximum_bitcast_fusion.1), channel_id=3, replica_groups=mesh['sp_0'=8,'sp_1'=8,'tp'=8] {'sp_0'}, dimensions={0}, use_global_device_ids=true | all-gather | bytes 889344 | tf_op jit(solution)/shard_map/all_gather | solution.py:47
  109.2 0.9 copy-done.1
  117.8 0.7 mul.1415
  118.6 0.7 mul.1416
  119.3 0.7 mul.1420
  122.1 0.7 mul.1430
  124.2 0.7 mul.1436
  129.3 1.5 fusion.136
  131.6 0.8 fusion.32
  132.4 0.9 fusion.34
  133.4 1.8 fusion.79
  135.2 0.8 fusion.33
  138.3 1.2 multiply_reduce_fusion.1
  140.1 11.7 %all-to-all-start = ((f32[8,1,256]{2,1,0:T(1,128)}), f32[8,1,256]{2,1,0:T(1,128)S(1)}, u32[]{:S(2)}, u32[]{:S(2)}) async-start(f32[8,1,256]{2,1,0:T(1,128)} %broadcast_in_dim.34), calls=%async_computation | async-start | bytes 16384 | tf_op jit(solution)/shard_map/all_to_all | solution.py:82
  151.8 0.7 all-gather.9.cloned.1.call-update
  152.6 3.9 %all-to-all-done = f32[8,1,256]{2,1,0:T(1,128)S(1)} async-done(((f32[8,1,256]{2,1,0:T(1,128)}), f32[8,1,256]{2,1,0:T(1,128)S(1)}, u32[]{:S(2)}, u32[]{:S(2)}) %all-to-all-start) | async-done | bytes 8224 | tf_op jit(solution)/shard_map/all_to_all | solution.py:82
  156.5 1.8 convolution_convert_fusion
  158.3 1.1 copy.298
  159.4 4.2 %all-to-all-start.1 = ((bf16[8,256,256]{1,2,0:T(8,128)(2,1)}), bf16[8,256,256]{1,2,0:T(8,128)(2,1)S(1)}, u32[]{:S(2)}, u32[]{:S(2)}) async-start(bf16[8,256,256]{1,2,0:T(8,128)(2,1)} %bitcast.584), calls=%async_computation.1 | async-start | bytes 2097152 | tf_op jit(solution)/shard_map/all_to_all | solution.py:98
  163.6 0.8 copy.232
  164.3 14.2 %all-to-all-done.1 = bf16[8,256,256]{1,2,0:T(8,128)(2,1)S(1)} async-done(((bf16[8,256,256]{1,2,0:T(8,128)(2,1)}), bf16[8,256,256]{1,2,0:T(8,128)(2,1)S(1)}, u32[]{:S(2)}, u32[]{:S(2)}) %all-to-all-start.1) | async-done | bytes 1048608 | tf_op jit(solution)/shard_map/all_to_all | solution.py:98
  178.7 0.9 add_convert_fusion.1
  179.8 18.3 %all_to_all.21 = bf16[8,256,256]{2,1,0:T(8,128)(2,1)S(1)} all-to-all(bf16[8,256,256]{2,1,0:T(8,128)(2,1)S(1)} %broadcast_in_dim.35), channel_id=1, replica_groups=mesh['sp_0'=8,'sp_1'=8,'tp'=8] {'tp'}, dimensions={0} | all-to-all | bytes 2097152 | tf_op jit(solution)/shard_map/all_to_all | solution.py:82
  198.9 2.9 %fusion.14 = bf16[1,640,256]{1,2,0:T(8,128)(2,1)S(1)} fusion(bf16[2048,256]{1,0:T(8,128)(2,1)S(1)} %fusion.5, bf16[2048,1280]{1,0:T(8,128)(2,1)} %all-gather.7.cloned.1.call-done), kind=kOutput, calls=%fused_computation.19 | convolution fusion | flops 671252480 | bytes 3997696 | tf_op jit(solution)/shard_map/dot_general | solution.py:140
  202.1 1.0 fusion.17
  203.2 3.7 %collective-permute-start.1 = (bf16[2,640,2]{1,2,0:T(2,128)(2,1)S(1)}, bf16[2,640,2]{1,2,0:T(2,128)(2,1)S(1)}, u32[]{:S(2)}, u32[]{:S(2)}) collective-permute-start(bf16[2,640,2]{1,2,0:T(2,128)(2,1)S(1)} %pad_maximum_fusion.3), channel_id=1, source_target_pairs={{0,8},{8,16},{16,24},{24,32},{32,40},{40,48},{48,56},{56,64},{64,7... | collective-permute-start | bytes 15368 | tf_op jit(solution)/shard_map/ppermute | solution.py:30
  206.9 0.7 collective-permute-done.1
  208.2 24.8 %all-gather.9.cloned.1.call-done = bf16[640,2048]{0,1:T(8,128)(2,1)} async-done(((bf16[640,32]{0,1:T(8,128)(2,1)}), bf16[640,2048]{0,1:T(8,128)(2,1)}) %all-gather.9.cloned.1.call-update) | async-done | bytes 2621456 | tf_op jit(solution)/shard_map/all_gather | solution.py:185
  233.0 2.8 %convolution_convert_fusion.1 = bf16[256,2048]{1,0:T(8,128)(2,1)S(1)} fusion(bf16[640,2048]{0,1:T(8,128)(2,1)} %all-gather.9.cloned.1.call-done, f32[2,640,256]{1,2,0:T(8,128)S(1)} %fusion.6), kind=kOutput, calls=%fused_computation.5 | convolution fusion | flops 672595968 | bytes 4980736 | tf_op jit(solution)/shard_map/dot_general | solution.py:140
  235.8 23.6 %all_to_all.22 = bf16[8,256,256]{1,2,0:T(8,128)(2,1)S(1)} all-to-all(bf16[8,256,256]{1,2,0:T(8,128)(2,1)S(1)} %bitcast.585), channel_id=1, replica_groups=mesh['sp_0'=8,'sp_1'=8,'tp'=8] {'tp'}, dimensions={0} | all-to-all | bytes 2097152 | tf_op jit(solution)/shard_map/all_to_all | solution.py:98
  259.6 0.8 copy.271
  (266 shorter events, 50.1 us)
Async XLA Ops:
  6.5 150.0 %copy-start = (bf16[512,2048]{1,0:T(8,128)(2,1)S(1)}, bf16[512,2048]{1,0:T(8,128)(2,1)}, u32[]{:S(2)}) copy-start(bf16[512,2048]{1,0:T(8,128)(2,1)} %param.26) | copy-start | bytes 6291460
  6.5 22.9 %copy-start.4 = (bf16[256,512]{1,0:T(8,128)(2,1)S(1)}, bf16[256,512]{1,0:T(8,128)(2,1)}, u32[]{:S(2)}) copy-start(bf16[256,512]{1,0:T(8,128)(2,1)} %param.17) | copy-start | bytes 786436
  6.5 192.3 %all-gather.7.cloned.1.call-start = ((), (), s32[]{:S(2)}) async-start(), calls=%async_computation.4 | async-start | bytes 5324800 | tf_op jit(solution)/shard_map/all_gather | solution.py:24
  8.1 21.3 %collective-permute-start = (bf16[3,896]{1,0:T(4,128)(2,1)S(1)}, bf16[3,896]{1,0:T(4,128)(2,1)S(1)}, u32[]{:S(2)}, u32[]{:S(2)}) collective-permute-start(bf16[3,896]{1,0:T(4,128)(2,1)S(1)} %pad_maximum_fusion.2), channel_id=1, source_target_pairs={{0,8},{8,16},{16,24},{24,32},{32,40},{40,48},{48,56},{56,64},{64,7... | collective-permute-start | bytes 16136 | tf_op jit(solution)/shard_map/ppermute | solution.py:30
  15.2 15.5 %copy-start.24 = (f32[128,4]{0,1:T(4,128)}, f32[128,4]{0,1:T(4,128)S(1)}, u32[]{:S(2)}) copy-start(f32[128,4]{0,1:T(4,128)S(1)} %get-tuple-element.26) | copy-start | bytes 6148
  15.2 15.7 %copy-start.26 = (f32[128,4]{0,1:T(4,128)}, f32[128,4]{0,1:T(4,128)S(1)}, u32[]{:S(2)}) copy-start(f32[128,4]{0,1:T(4,128)S(1)} %get-tuple-element.30) | copy-start | bytes 6148
  15.2 15.9 %copy-start.28 = (f32[128,4]{0,1:T(4,128)}, f32[128,4]{0,1:T(4,128)S(1)}, u32[]{:S(2)}) copy-start(f32[128,4]{0,1:T(4,128)S(1)} %get-tuple-element.27) | copy-start | bytes 6148
  15.2 16.1 %copy-start.30 = (f32[128,4]{0,1:T(4,128)}, f32[128,4]{0,1:T(4,128)S(1)}, u32[]{:S(2)}) copy-start(f32[128,4]{0,1:T(4,128)S(1)} %get-tuple-element.25) | copy-start | bytes 6148
  29.5 0.9 copy-start.5
  30.1 1.4 copy-start.2
  55.7 1.0 copy-start.7
  74.4 1.7 copy-start.12
  74.5 1.5 copy-start.14
  74.7 1.4 copy-start.16
  74.8 1.2 copy-start.18
  75.0 1.1 copy-start.19
  75.1 0.9 copy-start.20
  75.3 0.8 copy-start.21
  75.5 0.6 copy-start.22
  109.2 0.9 copy-start.1
  116.4 0.6 copy-start.11
  129.2 4.1 %copy-start.13 = (f32[256]{0:T(256)S(1)}, f32[256]{0:T(256)}, u32[]{:S(2)}) copy-start(f32[256]{0:T(256)} %copy-done.12) | copy-start | bytes 3076
  129.2 4.1 %copy-start.15 = (f32[256]{0:T(256)S(1)}, f32[256]{0:T(256)}, u32[]{:S(2)}) copy-start(f32[256]{0:T(256)} %copy-done.14) | copy-start | bytes 3076
  129.3 4.1 %copy-start.17 = (f32[256]{0:T(256)S(1)}, f32[256]{0:T(256)}, u32[]{:S(2)}) copy-start(f32[256]{0:T(256)} %copy-done.16) | copy-start | bytes 3076
  129.3 7.1 %copy-start.10 = (pred[128,128]{1,0:T(8,128)(4,1)S(1)}, pred[128,128]{1,0:T(8,128)(4,1)}, u32[]{:S(2)}) copy-start(pred[128,128]{1,0:T(8,128)(4,1)} %iota_compare_fusion) | copy-start | bytes 49156
  130.7 5.3 %copy-start.32 = (f32[128,4]{0,1:T(4,128)S(1)}, f32[128,4]{0,1:T(4,128)}, u32[]{:S(2)}) copy-start(f32[128,4]{0,1:T(4,128)} %copy.261) | copy-start | bytes 6148
  130.7 5.6 %copy-start.31 = (f32[128,4]{0,1:T(4,128)S(1)}, f32[128,4]{0,1:T(4,128)}, u32[]{:S(2)}) copy-start(f32[128,4]{0,1:T(4,128)} %copy-done.30) | copy-start | bytes 6148
  130.8 5.6 %copy-start.37 = (f32[4,128]{1,0:T(4,128)S(1)}, f32[4,128]{1,0:T(4,128)}, u32[]{:S(2)}) copy-start(f32[4,128]{1,0:T(4,128)} %copy.239) | copy-start | bytes 6148
  130.8 5.6 %copy-start.39 = (f32[4]{0:T(128)S(1)}, f32[4]{0:T(128)}, u32[]{:S(2)}) copy-start(f32[4]{0:T(128)} %get-tuple-element.70) | copy-start | bytes 52
  130.8 5.9 %copy-start.29 = (f32[128,4]{0,1:T(4,128)S(1)}, f32[128,4]{0,1:T(4,128)}, u32[]{:S(2)}) copy-start(f32[128,4]{0,1:T(4,128)} %copy-done.28) | copy-start | bytes 6148
  130.8 5.9 %copy-start.36 = (f32[4,128]{1,0:T(4,128)S(1)}, f32[4,128]{1,0:T(4,128)}, u32[]{:S(2)}) copy-start(f32[4,128]{1,0:T(4,128)} %copy.235) | copy-start | bytes 6148
  130.8 6.1 %copy-start.9 = (f32[256,4]{0,1:T(4,128)S(1)}, f32[256,4]{0,1:T(4,128)}, u32[]{:S(2)}) copy-start(f32[256,4]{0,1:T(4,128)} %get-tuple-element.23) | copy-start | bytes 12292
  130.9 5.5 %copy-start.3 = (f32[256,512]{0,1:T(8,128)S(1)}, f32[256,512]{0,1:T(8,128)}, u32[]{:S(2)}) copy-start(f32[256,512]{0,1:T(8,128)} %copy-done.2) | copy-start | bytes 1572868
  131.2 6.0 %copy-start.27 = (f32[128,4]{0,1:T(4,128)S(1)}, f32[128,4]{0,1:T(4,128)}, u32[]{:S(2)}) copy-start(f32[128,4]{0,1:T(4,128)} %copy-done.26) | copy-start | bytes 6148
  131.2 6.0 %copy-start.35 = (f32[4,128]{1,0:T(4,128)S(1)}, f32[4,128]{1,0:T(4,128)}, u32[]{:S(2)}) copy-start(f32[4,128]{1,0:T(4,128)} %copy.258) | copy-start | bytes 6148
  131.2 6.0 %copy-start.38 = (f32[4]{0:T(128)S(1)}, f32[4]{0:T(128)}, u32[]{:S(2)}) copy-start(f32[4]{0:T(128)} %get-tuple-element.71) | copy-start | bytes 52
  133.4 4.1 %copy-start.25 = (f32[128,4]{0,1:T(4,128)S(1)}, f32[128,4]{0,1:T(4,128)}, u32[]{:S(2)}) copy-start(f32[128,4]{0,1:T(4,128)} %copy-done.24) | copy-start | bytes 6148
  133.4 4.1 %copy-start.34 = (f32[4,128]{1,0:T(4,128)S(1)}, f32[4,128]{1,0:T(4,128)}, u32[]{:S(2)}) copy-start(f32[4,128]{1,0:T(4,128)} %copy.254) | copy-start | bytes 6148
  133.4 4.4 %copy-start.8 = (f32[256,4]{0,1:T(4,128)S(1)}, f32[256,4]{0,1:T(4,128)}, u32[]{:S(2)}) copy-start(f32[256,4]{0,1:T(4,128)} %get-tuple-element.24) | copy-start | bytes 12292
  137.5 19.0 %copy-start.41 = (f32[512]{0:T(512)S(1)}, f32[512]{0:T(512)}, u32[]{:S(2)}) copy-start(f32[512]{0:T(512)} %param.25) | copy-start | bytes 6148
  140.1 16.3 %all-to-all-start = ((f32[8,1,256]{2,1,0:T(1,128)}), f32[8,1,256]{2,1,0:T(1,128)S(1)}, u32[]{:S(2)}, u32[]{:S(2)}) async-start(f32[8,1,256]{2,1,0:T(1,128)} %broadcast_in_dim.34), calls=%async_computation | async-start | bytes 16384 | tf_op jit(solution)/shard_map/all_to_all | solution.py:82
  151.8 81.2 %all-gather.9.cloned.1.call-start = ((), (), s32[]{:S(2)}) async-start(), calls=%async_computation.5 | async-start | bytes 2662400 | tf_op jit(solution)/shard_map/all_gather | solution.py:185
  158.3 5.3 %copy-start.6 = (bf16[256,256]{1,0:T(8,128)(2,1)S(1)}, bf16[256,256]{1,0:T(8,128)(2,1)}, u32[]{:S(2)}) copy-start(bf16[256,256]{1,0:T(8,128)(2,1)} %param.16) | copy-start | bytes 393220
  159.4 19.2 %all-to-all-start.1 = ((bf16[8,256,256]{1,2,0:T(8,128)(2,1)}), bf16[8,256,256]{1,2,0:T(8,128)(2,1)S(1)}, u32[]{:S(2)}, u32[]{:S(2)}) async-start(bf16[8,256,256]{1,2,0:T(8,128)(2,1)} %bitcast.584), calls=%async_computation.1 | async-start | bytes 2097152 | tf_op jit(solution)/shard_map/all_to_all | solution.py:98
  179.7 18.7 %copy-start.23 = (f32[2048]{0:T(1024)S(1)}, f32[2048]{0:T(1024)}, u32[]{:S(2)}) copy-start(f32[2048]{0:T(1024)} %param.27) | copy-start | bytes 24580
  198.8 3.3 %copy-start.40 = (bf16[2048,1280]{1,0:T(8,128)(2,1)S(1)}, bf16[2048,1280]{1,0:T(8,128)(2,1)}, u32[]{:S(2)}) copy-start(bf16[2048,1280]{1,0:T(8,128)(2,1)} %all-gather.7.cloned.1.call-done) | copy-start | bytes 15728644
  202.1 4.8 %copy-start.33 = (bf16[2,3,640]{2,0,1:T(2,128)(2,1)S(1)}, bf16[2,3,640]{2,0,1:T(2,128)(2,1)}, u32[]{:S(2)}) copy-start(bf16[2,3,640]{2,0,1:T(2,128)(2,1)} %param.30) | copy-start | bytes 23044
  203.2 4.4 %collective-permute-start.1 = (bf16[2,640,2]{1,2,0:T(2,128)(2,1)S(1)}, bf16[2,640,2]{1,2,0:T(2,128)(2,1)S(1)}, u32[]{:S(2)}, u32[]{:S(2)}) collective-permute-start(bf16[2,640,2]{1,2,0:T(2,128)(2,1)S(1)} %pad_maximum_fusion.3), channel_id=1, source_target_pairs={{0,8},{8,16},{16,24},{24,32},{32,40},{40,48},{48,56},{56,64},{64,7... | collective-permute-start | bytes 15368 | tf_op jit(solution)/shard_map/ppermute | solution.py:30
Sparse Core Ops, SparseCore 0:
  13.7 93.1 all-gather.6
  155.6 77.2 all-gather.8
where the time goes:
time: 268 us; the launch traced here: 267 us
  blocking collectives  97.1 us (36%)
  local copies, waits for them, and re-layouts  52 us (19%)
  waiting for transfers between devices  44.4 us (17%)
  starting transfers between devices  23.6 us (9%)
  other arithmetic  21.6 us (8%)
  between operations  14.3 us (5%)
  matrix products  14.1 us (5%)
    all_gather x2, blocking collectives, gathered_once(): both, at, found = (lax.all_gather(jnp.concatenate(lines), axis), 0, {})  55.2 us
    mul x42, local copies, waits for them, and re-layouts, combine_states(): first_part[3] * second_part[2][..., None, None] + second_part[3]  26.7 us
    all_gather x1, waiting for transfers between devices, local(): early_down = lax.all_gather(hidden_down, SP, axis=1, tiled=True)  24.8 us
    all_to_all x1, blocking collectives, sent_and_summed(): parts = lax.all_to_all(split_up(shard, dim, count), axis, 0, 0, tiled=True)  23.6 us
    all_to_all x1, blocking collectives, from_everyone(): return lax.all_to_all(copies, axis, split_axis=0, concat_axis=0, tiled=True)  18.3 us
    all_to_all x1, waiting for transfers between devices, sent_and_summed(): parts = lax.all_to_all(split_up(shard, dim, count), axis, 0, 0, tiled=True)  14.2 us
    all_to_all x1, starting transfers between devices, from_everyone(): return lax.all_to_all(copies, axis, split_axis=0, concat_axis=0, tiled=True)  11.7 us
    ppermute x2, starting transfers between devices, from_behind(): lax.ppermute(value, axis, [(source, source + steps) for source in range(f...  7.71 us
  transfers between devices with their start and end apart: 6, of which 4 were waited for; matrix products, arithmetic and copies ran while one was open for 30% of the time, Pallas kernels for 0%

commit v1 on v0

v1 whole, which is shorter than its diff:
```python
import functools

import jax
import jax.numpy as jnp
from jax import lax
from jax.experimental import pallas as pl
from jax.experimental.pallas import tpu as pltpu
from jax.sharding import Mesh
from jax.sharding import PartitionSpec as P

GROUP_HEADS = 8
HEAD_SIZE = 64
STATE_WIDE = 128
STATE_NARROW = 64
HALF = GROUP_HEADS // 2 * HEAD_SIZE
SP = ("sp_0", "sp_1")
NORM_FLOOR = 0.1
F32 = jnp.float32
BF16 = jnp.bfloat16
HIGHEST = lax.Precision.HIGHEST
LAST = (((1,), (1,)), ((), ()))
FIRST = (((0,), (0,)), ((), ()))


def call(kernel, outs, scratch=(), **more):
    return pl.pallas_call(
        kernel,
        out_shape=[jax.ShapeDtypeStruct(shape, kind) for shape, kind in outs],
        scratch_shapes=[pltpu.VMEM(shape, kind) for shape, kind in scratch],
        **more,
    )


def silu(a):
    return a / (1.0 + jnp.exp(-a))


def pieces(row, count):
    found = []
    for _ in range(count):
        part = row.astype(BF16).astype(F32)
        found.append(part)
        row = row - part
    return found


def head_lanes(cols):
    rows = cols.shape[0]
    lane = lax.broadcasted_iota(jnp.int32, (rows, 2 * HEAD_SIZE), 1)
    both = [
        jnp.where(lane < HEAD_SIZE, cols[:, h : h + 1], cols[:, h + 1 : h + 2])
        for h in range(0, GROUP_HEADS, 2)
    ]
    return jnp.concatenate(both, axis=1)


def as_row(col):
    return jnp.transpose(jnp.broadcast_to(col, (col.shape[0], 128)))[0:1, :]


def as_col(row):
    return jnp.transpose(jnp.broadcast_to(row, (8, row.shape[1])))[:, 0:1]


def conv_silu(buf, taps, rows):
    count = taps.shape[0]
    total = taps[count - 1 : count, :].astype(F32) * buf[8 : 8 + rows, :]
    for k in range(count - 1):
        at = 8 - (count - 1) + k
        total = total + taps[k : k + 1, :].astype(F32) * buf[at : at + rows, :]
    return silu(total)


def state_kernel(
    values, keys, before, step, rate, taps_v, taps_k, x_out, key_out, run_out, delta_out, run_col, pay, vbuf, kbuf
):
    rows, cols = values.shape
    vbuf[0:8, :] = before[:, :cols].astype(F32)
    vbuf[8 : 8 + rows, :] = values[...].astype(F32)
    kbuf[0:8, :] = before[:, cols:].astype(F32)
    kbuf[8 : 8 + rows, :] = keys[...].astype(F32)
    x = conv_silu(vbuf, taps_v, rows)
    k = conv_silu(kbuf, taps_k, rows).astype(BF16)
    x_out[...] = x.astype(BF16)
    key_out[...] = k
    pre = step[...]
    delta = jnp.maximum(pre, 0.0) + jnp.log1p(jnp.exp(-jnp.abs(pre)))
    upper = lax.broadcasted_iota(jnp.int32, (rows, rows), 0) <= lax.broadcasted_iota(
        jnp.int32, (rows, rows), 1
    )
    run = jnp.dot(-rate[...] * delta, upper.astype(F32), precision=HIGHEST, preferred_element_type=F32)
    run_out[...] = run
    delta_out[...] = delta
    run_t = jnp.transpose(run)
    run_col[...] = run_t
    end = run_t[rows - 1 : rows, :]
    to_end = jnp.exp(end - run_t) * jnp.transpose(delta)
    weighted = (x * head_lanes(to_end)).astype(BF16)
    wide = lax.dot_general(k[:, :STATE_WIDE], weighted[:, :HALF], FIRST, preferred_element_type=F32)
    narrow = lax.dot_general(
        k[:, 2 * STATE_WIDE :], weighted[:, HALF:], FIRST, preferred_element_type=F32
    )
    ends = head_lanes(jnp.broadcast_to(end, (8, GROUP_HEADS)))[0:1, :]
    marks = pieces(ends[:, :HALF], 3) + pieces(ends[:, HALF:], 3) + [jnp.zeros((2, HALF), F32)]
    count = pay.shape[0]
    w, n = STATE_WIDE // count, STATE_NARROW // count
    for c in range(count):
        part = [wide[c * w : (c + 1) * w], narrow[c * n : (c + 1) * n]] + marks
        pay[c] = jnp.concatenate(part, axis=0).astype(BF16)


def inside_kernel(x, keys, run, delta, run_col, skip, gate, base_out, slope_out):
    rows = x.shape[0]
    xs = x[...]
    k = keys[...]
    wide_end = 2 * STATE_WIDE
    score_w = lax.dot_general(k[:, STATE_WIDE:wide_end], k[:, :STATE_WIDE], LAST, preferred_element_type=F32)
    score_n = lax.dot_general(
        k[:, wide_end + STATE_NARROW :], k[:, wide_end : wide_end + STATE_NARROW], LAST, preferred_element_type=F32
    )
    keep = lax.broadcasted_iota(jnp.int32, (rows, rows), 0) >= lax.broadcasted_iota(
        jnp.int32, (rows, rows), 1
    )
    runs, deltas, cols = run[...], delta[...], run_col[...]
    outs = []
    for h in range(GROUP_HEADS):
        gap = jnp.where(keep, cols[:, h : h + 1] - runs[h : h + 1, :], -jnp.inf)
        score = score_w if h < GROUP_HEADS // 2 else score_n
        mixed = (score * (jnp.exp(gap) * deltas[h : h + 1, :])).astype(BF16)
        outs.append(
            jnp.dot(mixed, xs[:, h * HEAD_SIZE : (h + 1) * HEAD_SIZE], preferred_element_type=F32)
        )
    opened = silu(gate[...].astype(F32))
    direct = jnp.concatenate(outs, axis=1) + skip[...] * xs.astype(F32)
    base_out[...] = direct * opened
    slope_out[...] = head_lanes(jnp.exp(cols)) * opened


def span_parts(piece):
    w = STATE_WIDE // 8
    n = STATE_NARROW // 8
    state = piece[: w + n]
    at = w + n
    wide = piece[at : at + 1] + piece[at + 1 : at + 2] + piece[at + 2 : at + 3]
    narrow = piece[at + 3 : at + 4] + piece[at + 4 : at + 5] + piece[at + 5 : at + 6]
    return state, wide, narrow


def fade(wide, narrow):
    w = STATE_WIDE // 8
    n = STATE_NARROW // 8
    lanes = wide.shape[1]
    return jnp.concatenate(
        [
            jnp.broadcast_to(jnp.exp(wide), (w, lanes)),
            jnp.broadcast_to(jnp.exp(narrow), (n, lanes)),
        ],
        axis=0,
    )


def row_total_kernel(got, pay):
    count = got.shape[0]
    total = None
    for c in range(count):
        state, wide, narrow = span_parts(got[c].astype(F32))
        if total is None:
            total, log_w, log_n = state, wide, narrow
        else:
            total = total * fade(wide, narrow) + state
            log_w, log_n = log_w + wide, log_n + narrow
    marks = pieces(log_w, 3) + pieces(log_n, 3) + [jnp.zeros((2, log_w.shape[1]), F32)]
    piece = jnp.concatenate([total] + marks, axis=0).astype(BF16)
    for c in range(count):
        pay[c] = piece


def prefix_kernel(place, got, totals, pay):
    count = got.shape[0]
    mine = place[0]
    total = jnp.zeros((pay.shape[1] - 8, pay.shape[2]), F32)
    for c in range(totals.shape[0]):
        state, wide, narrow = span_parts(totals[c].astype(F32))
        total = jnp.where(c < mine, total * fade(wide, narrow) + state, total)
    pad = jnp.zeros((8, pay.shape[2]), F32)
    for c in range(count):
        pay[c] = jnp.concatenate([total, pad], axis=0).astype(BF16)
        state, wide, narrow = span_parts(got[c].astype(F32))
        total = total * fade(wide, narrow) + state


def apply_kernel(base, slope, keys, got, gain, weight, pay):
    count = got.shape[0]
    w = STATE_WIDE // count
    n = STATE_NARROW // count
    carried = [got[c].astype(F32) for c in range(count)]
    wide = jnp.concatenate([c[:w] for c in carried], axis=0).astype(BF16)
    narrow = jnp.concatenate([c[w : w + n] for c in carried], axis=0).astype(BF16)
    k = keys[...]
    wide_end = 2 * STATE_WIDE
    from_wide = jnp.dot(k[:, STATE_WIDE:wide_end], wide, preferred_element_type=F32)
    from_narrow = jnp.dot(k[:, wide_end + STATE_NARROW :], narrow, preferred_element_type=F32)
    gated = base[...] + slope[...] * jnp.concatenate([from_wide, from_narrow], axis=1)
    squares = as_row(jnp.sum(gated * gated, axis=1, keepdims=True))
    marks = pieces(squares, 2) + [jnp.zeros((14, squares.shape[1]), F32)]
    marks = jnp.concatenate(marks, axis=0).astype(BF16)
    scaled = (gated * gain[...]).astype(BF16)
    rows, share = scaled.shape[0], pay.shape[2]
    for c in range(pay.shape[0]):
        part = jnp.dot(scaled, weight[:, c * share : (c + 1) * share], preferred_element_type=F32)
        pay[c, 0:rows, :] = part.astype(BF16)
        pay[c, rows : rows + 16, :] = marks


def merge_kernel(channels, got, residual, gain, lifted_out, tile_out, merged_out):
    rows = residual.shape[1]
    total = got[0].astype(F32)
    for c in range(1, got.shape[0]):
        total = total + got[c].astype(F32)
    squares = total[rows : rows + 1] + total[rows + 1 : rows + 2]
    inverse = as_col(lax.rsqrt(squares / channels + NORM_FLOOR))
    merged = jnp.transpose(residual[...].astype(F32)) + inverse * total[:rows]
    merged = merged.astype(BF16).astype(F32)
    merged_out[...] = jnp.transpose(merged).astype(BF16)
    own = as_row(jnp.sum(merged * merged, axis=1, keepdims=True))
    lifted = (merged * gain[...]).astype(BF16)
    lifted_out[...] = lifted
    edge = lifted[rows - 8 :, :].astype(F32)
    tile = pieces(own, 2) + [jnp.zeros((4, own.shape[1]), F32), edge[6:8]]
    tile_out[...] = jnp.concatenate(tile, axis=0).astype(BF16)


def channel_kernel(blocks, features, got, weight_in, weight_out, taps, pay, total, marks, buf, hidden):
    step = pl.program_id(0)
    rows = hidden.shape[0]
    units = hidden.shape[1]

    @pl.when(step < blocks)
    def _():
        mine = got[0]
        part = jnp.dot(mine, weight_in[...], preferred_element_type=F32)
        mark = mine[rows : rows + 16].astype(F32)

        @pl.when(step == 0)
        def _():
            total[...] = part
            marks[...] = mark

        @pl.when(step > 0)
        def _():
            total[...] += part
            marks[...] += mark

    @pl.when(step == blocks - 1)
    def _():
        def inverse_of(at):
            squares = marks[at : at + 1, :] + marks[at + 1 : at + 2, :]
            return as_col(lax.rsqrt(squares / features + NORM_FLOOR))

        own, before = inverse_of(0), inverse_of(8)
        buf[0:8, :] = (total[rows + 8 : rows + 16, :] * before[rows - 8 :, :]).astype(BF16).astype(F32)
        buf[8 : 8 + rows, :] = (total[0:rows, :] * own).astype(BF16).astype(F32)

        def conv(branch):
            first, last = branch * units, (branch + 1) * units
            count = taps.shape[1]
            summed = None
            for k in range(count):
                at = 8 - (count - 1) + k
                term = taps[branch, k : k + 1, :].astype(F32) * buf[at : at + rows, first:last]
                summed = term if summed is None else summed + term
            return summed

        hidden[...] = (silu(conv(0)) * conv(1)).astype(BF16)

    @pl.when(step >= blocks)
    def _():
        pay[0] = lax.dot_general(
            weight_out[...], hidden[...], LAST, preferred_element_type=F32
        ).astype(BF16)


def exchange(parts, axis):
    return lax.all_to_all(parts, axis, split_axis=0, concat_axis=0, tiled=True)


def from_behind(value, axis):
    count = lax.axis_size(axis)
    return lax.ppermute(value, axis, [(source, source + 1) for source in range(count - 1)])


def local(
    residual,
    values,
    gate_input,
    group_keys,
    time_step,
    decay_rate,
    skip_gain,
    conv_values,
    conv_keys,
    mix_gain,
    out_weight,
    norm_gain,
    hidden_gate,
    hidden_up,
    hidden_conv,
    hidden_down,
):
    own_rows = jnp.concatenate([hidden_gate, hidden_up, hidden_down.T], axis=1)
    weights = lax.all_gather(own_rows, SP, axis=0, tiled=True)
    rows, cols = values.shape
    n_tp = lax.axis_size("tp")
    n_row = lax.axis_size(SP[1])
    features = residual.shape[0]
    units = hidden_gate.shape[1]
    tail = jnp.concatenate([values[rows - 8 :], group_keys[rows - 8 :]], axis=1)
    before = from_behind(tail, SP)
    key_cols = group_keys.shape[1]
    span = STATE_WIDE // n_row + STATE_NARROW // n_row + 8
    x, keys, run, delta, run_col, pay = call(
        state_kernel,
        [
            ((rows, cols), BF16),
            ((rows, key_cols), BF16),
            ((GROUP_HEADS, rows), F32),
            ((GROUP_HEADS, rows), F32),
            ((rows, GROUP_HEADS), F32),
            ((n_row, span, HALF), BF16),
        ],
        [((rows + 8, cols), F32), ((rows + 8, key_cols), F32)],
        name="span_state",
    )(
        values,
        group_keys,
        before,
        time_step,
        decay_rate.reshape(-1, 1),
        conv_values,
        conv_keys,
    )
    by_row = exchange(pay, SP[1])
    base, slope = call(
        inside_kernel, [((rows, cols), F32), ((rows, cols), F32)], name="inside_span"
    )(x, keys, run, delta, run_col, jnp.repeat(skip_gain, HEAD_SIZE).reshape(1, -1), gate_input)
    (sums,) = call(
        row_total_kernel, [((lax.axis_size(SP[0]), span, HALF), BF16)], name="row_total"
    )(by_row)
    totals = exchange(sums, SP[0])
    place = lax.axis_index(SP[0]).astype(jnp.int32).reshape(1)
    (starts,) = call(
        prefix_kernel,
        [((n_row, span, HALF), BF16)],
        in_specs=[
            pl.BlockSpec(memory_space=pltpu.SMEM),
            pl.BlockSpec(memory_space=pltpu.VMEM),
            pl.BlockSpec(memory_space=pltpu.VMEM),
        ],
        name="prefix",
    )(place, by_row, totals)
    carried = exchange(starts, SP[1])
    (partial,) = call(
        apply_kernel, [((n_tp, rows + 16, features), BF16)], name="apply_project"
    )(base, slope, keys, carried, mix_gain.reshape(1, -1), out_weight)
    summed = exchange(partial, "tp")
    own_gain = lax.dynamic_slice_in_dim(norm_gain, lax.axis_index("tp") * features, features, 0)
    lifted, tile, merged = call(
        functools.partial(merge_kernel, cols * n_tp),
        [((rows, features), BF16), ((8, features), BF16), ((features, rows), BF16)],
        name="merge",
    )(summed, residual, own_gain.reshape(1, -1))
    stream = jnp.concatenate([lifted, tile, from_behind(tile, SP)], axis=0)
    stream = exchange(jnp.broadcast_to(stream, (n_tp, *stream.shape)), "tp")
    down_first = 2 * units // units
    (down,) = call(
        functools.partial(channel_kernel, n_tp, features * n_tp),
        [((n_tp, features, rows), BF16)],
        [
            ((rows + 16, 2 * units), F32),
            ((16, features), F32),
            ((rows + 8, 2 * units), F32),
            ((rows, units), BF16),
        ],
        grid=(2 * n_tp,),
        in_specs=[
            pl.BlockSpec((1, rows + 16, features), lambda i: (jnp.minimum(i, n_tp - 1), 0, 0)),
            pl.BlockSpec((features, 2 * units), lambda i: (jnp.minimum(i, n_tp - 1), 0)),
            pl.BlockSpec((features, units), lambda i: (jnp.maximum(i - n_tp, 0), down_first)),
            pl.BlockSpec(hidden_conv.shape, lambda i: (0, 0, 0)),
        ],
        out_specs=[pl.BlockSpec((1, features, rows), lambda i: (jnp.maximum(i - n_tp, 0), 0, 0))],
        name="channel_mixer",
    )(stream, weights, weights, hidden_conv)
    got = exchange(down, "tp")
    return (merged.astype(F32) + jnp.sum(got.astype(F32), axis=0)).astype(BF16)


def solution(mesh):
    split = Mesh(mesh.devices.reshape(8, 8, mesh.shape["tp"]), ("sp_0", "sp_1", "tp"))
    placed = (
        P("tp", SP),
        P(SP, "tp"),
        P(SP, "tp"),
        P(SP, "tp"),
        P("tp", SP),
        P("tp"),
        P("tp"),
        P(None, "tp"),
        P(None, "tp"),
        P("tp"),
        P("tp", None),
        P(),
        P(SP, "tp"),
        P(SP, "tp"),
        P(None, None, "tp"),
        P("tp", SP),
    )
    return jax.shard_map(local, mesh=split, in_specs=placed, out_specs=P("tp", SP), check_vma=False)
```

time: 268 us -> 175 us (0.65)
  blocking collectives: 97.1 us -> 35.5 us
  local copies, waits for them, and re-layouts: 52 us -> 11.3 us
  Pallas kernels: 0 us -> 30.1 us
  other arithmetic: 21.6 us -> 3.24 us
  matrix products: 14.1 us -> 0 us
  starting transfers between devices: 23.6 us -> 35.2 us
    all_gather x2 -> x0, blocking collectives: 55.2 us -> none  [gathered_once(): both, at, found = (lax.all_gather(jnp.concatenate(lines), axis), 0, {})]
    mul x83 -> x0, local copies, waits for them, and re-layouts: 36.8 us -> none  [the longest x42 26.7 us: combine_states(): first_part[3] * second_part[2][..., None, None] + second_part[3]]
    pallas_call x0 -> x7, Pallas kernels: none -> 30.1 us  [the longest x1 14.3 us: local(): call(functools.partial(channel_kernel, n_tp, features * n_tp), [((n_tp, f...]
    all_gather x2 -> x1, waiting for transfers between devices: 24.8 us -> 0.01 us  [local(): weights = lax.all_gather(own_rows, SP, axis=0, tiled=True)]
    all_to_all x2 -> x4, waiting for transfers between devices: 18.1 us -> 41.9 us  [exchange(): return lax.all_to_all(parts, axis, split_axis=0, concat_axis=0, tiled=True)]
    dot_general x22 -> x0, matrix products: 14.1 us -> none  [the longest x3 6.73 us: contract_rows(): lax.dot_general(left, right, (((0,), (0,)), ((), ())), preferred_element_...]
    all_to_all x2 -> x4, starting transfers between devices: 15.9 us -> 29.1 us  [exchange(): return lax.all_to_all(parts, axis, split_axis=0, concat_axis=0, tiled=True)]
    all_to_all x2, blocking collectives: 41.9 us -> 35.5 us  [exchange(): return lax.all_to_all(parts, axis, split_axis=0, concat_axis=0, tiled=True)]
  transfers between devices with their start and end apart: 6 -> 7, of which waited for: 4 -> 5; matrix products, arithmetic and copies ran while one was open for 30% -> 4% of each run, Pallas kernels for 0% -> 9%
where the time goes in v1:
time: 175 us; the launch traced here: 172 us
  waiting for transfers between devices  42.9 us (25%)
  blocking collectives  35.5 us (20%)
  starting transfers between devices  35.2 us (20%)
  Pallas kernels  30.1 us (17%)
  between operations  13.4 us (8%)
  local copies, waits for them, and re-layouts  11.3 us (6%)
  other arithmetic  3.24 us (2%)
    all_to_all x4, waiting for transfers between devices, exchange(): return lax.all_to_all(parts, axis, split_axis=0, concat_axis=0, tiled=True)  41.9 us
    all_to_all x2, blocking collectives, exchange(): return lax.all_to_all(parts, axis, split_axis=0, concat_axis=0, tiled=True)  35.5 us
    all_to_all x4, starting transfers between devices, exchange(): return lax.all_to_all(parts, axis, split_axis=0, concat_axis=0, tiled=True)  29.1 us
    pallas_call x1, Pallas kernels, local(): call(functools.partial(channel_kernel, n_tp, features * n_tp), [((n_tp, f...  14.3 us
    ppermute x2, starting transfers between devices, from_behind(): lax.ppermute(value, axis, [(source, source + 1) for source in range(count...  6.14 us
    unnamed x17, local copies, waits for them, and re-layouts  5.41 us
    pallas_call x1, Pallas kernels, local(): call(apply_kernel, [((n_tp, rows + 16, features), BF16)], name='apply_pro...  3.92 us
  transfers between devices with their start and end apart: 7, of which 5 were waited for; matrix products, arithmetic and copies ran while one was open for 4% of the time, Pallas kernels for 9%

profile of v1, /device:TPU:1, one launch (start us, length us, event | category | flops | bytes accessed | tf_op | source)
XLA Modules:
  0.0 171.7 jit_solution(10060240268742872986)
XLA Ops:
  6.5 0.0 all-gather.2.cloned.1.call-start
  6.5 1.5 pad_maximum_fusion.1
  8.0 0.0 copy-start.7
  8.0 0.0 all-gather.2.cloned.1.call-update
  8.0 0.7 slice.6
  8.7 0.7 slice.7
  9.4 4.0 %collective-permute-start = (bf16[8,896]{1,0:T(8,128)(2,1)S(1)}, bf16[8,896]{1,0:T(8,128)(2,1)S(1)}, u32[]{:S(2)}, u32[]{:S(2)}) collective-permute-start(bf16[8,896]{1,0:T(8,128)(2,1)S(1)} %pad_maximum_fusion.2), channel_id=1, source_target_pairs={{0,8},{8,16},{16,24},{24,32},{32,40},{40,48},{48,56},{56,64},{64,7... | collective-permute-start | bytes 43016 | tf_op jit(solution)/shard_map/ppermute | solution.py:289
  13.5 1.3 copy.17.rate
  14.8 0.0 collective-permute-done.before
  14.8 0.0 copy-start.5
  14.8 0.6 copy-done.5
  15.4 3.0 %span_state.1 = (bf16[256,512]{1,0:T(8,128)(2,1)}, bf16[256,384]{1,0:T(8,128)(2,1)}, f32[8,256]{1,0:T(8,128)}, f32[8,256]{1,0:T(8,128)}, f32[256,8]{1,0:T(8,128)}, /*index=5*/bf16[8,32,256]{2,1,0:T(8,128)(2,1)}) custom-call(bf16[256,512]{1,0:T(8,128)(2,1)} %values.1, bf16[256,384]{1,0:T(8,128)(2,1)} %keys.1, bf16[8,896]{1,0:T(8,128)(2,1)} %copy-done.5, ...), custom_call_target="tpu_custom_call" | custom-call | tf_op jit(solution)/shard_map/span_state/pallas_call | solution.py:321
  18.4 16.1 %all_to_all.30.got = bf16[8,32,256]{2,1,0:T(8,128)(2,1)} all-to-all(bf16[8,32,256]{2,1,0:T(8,128)(2,1)} %get-tuple-element.23), channel_id=1, replica_groups=mesh['sp_0'=8,'sp_1'=8,'tp'=8] {'sp_1'}, dimensions={0} | all-to-all | bytes 262144 | tf_op jit(solution)/shard_map/all_to_all | solution.py:284
  34.5 1.6 row_total.1
  36.1 10.6 %all-to-all-start.1 = ((bf16[8,32,256]{2,1,0:T(8,128)(2,1)}), bf16[8,32,256]{2,1,0:T(8,128)(2,1)S(1)}, u32[]{:S(2)}, u32[]{:S(2)}) async-start(bf16[8,32,256]{2,1,0:T(8,128)(2,1)} %row_total.1), calls=%async_computation.1 | async-start | bytes 262144 | tf_op jit(solution)/shard_map/all_to_all | solution.py:284
  46.7 8.6 %all-to-all-done.1.totals = bf16[8,32,256]{2,1,0:T(8,128)(2,1)S(1)} async-done(((bf16[8,32,256]{2,1,0:T(8,128)(2,1)}), bf16[8,32,256]{2,1,0:T(8,128)(2,1)S(1)}, u32[]{:S(2)}, u32[]{:S(2)}) %all-to-all-start.1) | async-done | bytes 131104 | tf_op jit(solution)/shard_map/all_to_all | solution.py:284
  55.2 0.0 copy-start.3
  55.2 0.7 copy-done.3
  55.9 1.7 prefix.1
  57.6 3.4 %all-to-all-start.2 = ((bf16[8,32,256]{2,1,0:T(8,128)(2,1)}), bf16[8,32,256]{2,1,0:T(8,128)(2,1)S(1)}, u32[]{:S(2)}, u32[]{:S(2)}) async-start(bf16[8,32,256]{2,1,0:T(8,128)(2,1)} %prefix.1), calls=%async_computation.2 | async-start | bytes 262144 | tf_op jit(solution)/shard_map/all_to_all | solution.py:284
  61.0 0.0 copy-done.7
  61.0 0.1 broadcast_in_dim.6
  61.0 0.7 reshape_reshape.3.skip
  61.7 3.2 %inside_span.1 = (f32[256,512]{1,0:T(8,128)}, f32[256,512]{1,0:T(8,128)}) custom-call(bf16[256,512]{1,0:T(8,128)(2,1)} %get-tuple-element.16.x, bf16[256,384]{1,0:T(8,128)(2,1)} %get-tuple-element.17.keys, f32[8,256]{1,0:T(8,128)} %get-tuple-element.18.run, f32[8,256]{1,0:T(8,128)} %get-tuple-element.19.delta, f32[256,8]{1,0:T(8,128)} %get-tuple-element.20.run_col, ...), custom_call_target="tpu_custom_call" | custom-call | tf_op jit(solution)/shard_map/inside_span/pallas_call | solution.py:343
  64.9 3.9 %all-to-all-done.2.got = bf16[8,32,256]{2,1,0:T(8,128)(2,1)S(1)} async-done(((bf16[8,32,256]{2,1,0:T(8,128)(2,1)}), bf16[8,32,256]{2,1,0:T(8,128)(2,1)S(1)}, u32[]{:S(2)}, u32[]{:S(2)}) %all-to-all-start.2) | async-done | bytes 131104 | tf_op jit(solution)/shard_map/all_to_all | solution.py:284
  68.8 0.0 copy-start.2
  68.8 0.7 copy-done.2
  69.4 3.9 %apply_project.1 = bf16[8,272,256]{2,1,0:T(8,128)(2,1)} custom-call(f32[256,512]{1,0:T(8,128)} %get-tuple-element.21.base, f32[256,512]{1,0:T(8,128)} %get-tuple-element.22.slope, bf16[256,384]{1,0:T(8,128)(2,1)} %get-tuple-element.17.keys, bf16[8,32,256]{2,1,0:T(8,128)(2,1)} %copy-done.2, f32[1,512]{1,0:T(1,128)} %bitcast.7, bf16[512,2048]{1,0:T(8,128)(2,1)} %weight.1), custom_call_target="tpu_custom_call" | custom-call | tf_op jit(solution)/shard_map/apply_project/pallas_call | solution.py:362
  73.4 9.7 %all-to-all-start.3 = ((bf16[8,272,256]{2,1,0:T(8,128)(2,1)}), bf16[8,272,256]{2,1,0:T(8,128)(2,1)S(1)}, u32[]{:S(2)}, u32[]{:S(2)}) async-start(bf16[8,272,256]{2,1,0:T(8,128)(2,1)} %apply_project.1), calls=%async_computation.3 | async-start | bytes 2228224 | tf_op jit(solution)/shard_map/all_to_all | solution.py:284
  83.0 1.3 dynamic_slice.3
  84.4 14.3 %all-to-all-done.3.got = bf16[8,272,256]{2,1,0:T(8,128)(2,1)S(1)} async-done(((bf16[8,272,256]{2,1,0:T(8,128)(2,1)}), bf16[8,272,256]{2,1,0:T(8,128)(2,1)S(1)}, u32[]{:S(2)}, u32[]{:S(2)}) %all-to-all-start.3) | async-done | bytes 1114144 | tf_op jit(solution)/shard_map/all_to_all | solution.py:284
  98.7 0.0 copy-start.1
  98.7 1.1 copy-done.1
  99.8 2.5 %merge.1 = (bf16[256,256]{1,0:T(8,128)(2,1)}, bf16[8,256]{1,0:T(8,128)(2,1)}, bf16[256,256]{1,0:T(8,128)(2,1)}) custom-call(bf16[8,272,256]{2,1,0:T(8,128)(2,1)} %copy-done.1, bf16[256,256]{1,0:T(8,128)(2,1)} %residual.1, f32[1,256]{1,0:T(1,128)} %bitcast.6), custom_call_target="tpu_custom_call" | custom-call | tf_op jit(solution)/shard_map/merge/pallas_call | solution.py:367
  102.2 2.1 %collective-permute-start.1 = (bf16[8,256]{1,0:T(8,128)(2,1)}, bf16[8,256]{1,0:T(8,128)(2,1)S(1)}, u32[]{:S(2)}, u32[]{:S(2)}) collective-permute-start(bf16[8,256]{1,0:T(8,128)(2,1)} %get-tuple-element.26), channel_id=1, source_target_pairs={{0,8},{8,16},{16,24},{24,32},{32,40},{40,48},{48,56},{56,64},{64,7... | collective-permute-start | bytes 12296 | tf_op jit(solution)/shard_map/ppermute | solution.py:289
  104.4 0.9 collective-permute-done.1
  105.3 0.9 pad_maximum_fusion
  106.3 1.1 broadcast_in_dim.7
  107.4 5.4 %all-to-all-start.4 = ((bf16[8,272,256]{2,1,0:T(8,128)(2,1)}), bf16[8,272,256]{2,1,0:T(8,128)(2,1)S(1)}, u32[]{:S(2)}, u32[]{:S(2)}) async-start(bf16[8,272,256]{2,1,0:T(8,128)(2,1)} %broadcast_in_dim.7), calls=%async_computation.4 | async-start | bytes 2228224 | tf_op jit(solution)/shard_map/all_to_all | solution.py:284
  112.8 0.0 copy-done.6
  112.9 0.6 copy.18.taps
  113.5 15.1 %all-to-all-done.4.got = bf16[8,272,256]{2,1,0:T(8,128)(2,1)S(1)} async-done(((bf16[8,272,256]{2,1,0:T(8,128)(2,1)}), bf16[8,272,256]{2,1,0:T(8,128)(2,1)S(1)}, u32[]{:S(2)}, u32[]{:S(2)}) %all-to-all-start.4) | async-done | bytes 1114144 | tf_op jit(solution)/shard_map/all_to_all | solution.py:284
  128.6 1.1 copy-done
  129.6 14.3 %channel_mixer.1 = bf16[8,256,256]{2,1,0:T(8,128)(2,1)} custom-call(bf16[8,272,256]{2,1,0:T(8,128)(2,1)} %copy-done, bf16[2048,1920]{1,0:T(8,128)(2,1)} %all-gather.2.cloned.1.call-done.weight_in.weight_out, bf16[2048,1920]{1,0:T(8,128)(2,1)} %all-gather.2.cloned.1.call-done.weight_in.weight_out, bf16[2,3,640]{2,1,0:T(4,128)(2,1)} %copy.18.taps), custom_call_target="tpu_custom_call" | custom-call | tf_op jit(solution)/shard_map/channel_mixer/pallas_call | solution.py:375
  143.9 19.4 %all_to_all.31 = bf16[8,256,256]{2,1,0:T(8,128)(2,1)S(1)} all-to-all(bf16[8,256,256]{2,1,0:T(8,128)(2,1)} %channel_mixer.1), channel_id=1, replica_groups=mesh['sp_0'=8,'sp_1'=8,'tp'=8] {'tp'}, dimensions={0} | all-to-all | bytes 2097152 | tf_op jit(solution)/shard_map/all_to_all | solution.py:284
  163.3 0.1 convert_reduce_fusion
  163.4 0.8 copy-done.4
  164.2 0.7 add_convert_fusion
  (5 shorter events, 0.0 us)
Async XLA Ops:
  6.5 122.0 %all-gather.2.cloned.1.call-start = ((), (), s32[]{:S(2)}) async-start(), calls=%async_computation.6 | async-start | bytes 7987200 | tf_op jit(solution)/shard_map/all_gather | solution.py:311
  8.0 52.9 %copy-start.7 = (f32[8]{0:T(128)S(1)}, f32[8]{0:T(128)}, u32[]{:S(2)}) copy-start(f32[8]{0:T(128)} %param.22) | copy-start | bytes 100
  9.4 5.3 %collective-permute-start = (bf16[8,896]{1,0:T(8,128)(2,1)S(1)}, bf16[8,896]{1,0:T(8,128)(2,1)S(1)}, u32[]{:S(2)}, u32[]{:S(2)}) collective-permute-start(bf16[8,896]{1,0:T(8,128)(2,1)S(1)} %pad_maximum_fusion.2), channel_id=1, source_target_pairs={{0,8},{8,16},{16,24},{24,32},{32,40},{40,48},{48,56},{56,64},{64,7... | collective-permute-start | bytes 43016 | tf_op jit(solution)/shard_map/ppermute | solution.py:289
  14.8 0.6 copy-start.5
  36.1 19.2 %all-to-all-start.1 = ((bf16[8,32,256]{2,1,0:T(8,128)(2,1)}), bf16[8,32,256]{2,1,0:T(8,128)(2,1)S(1)}, u32[]{:S(2)}, u32[]{:S(2)}) async-start(bf16[8,32,256]{2,1,0:T(8,128)(2,1)} %row_total.1), calls=%async_computation.1 | async-start | bytes 262144 | tf_op jit(solution)/shard_map/all_to_all | solution.py:284
  55.2 0.7 copy-start.3
  57.6 11.2 %all-to-all-start.2 = ((bf16[8,32,256]{2,1,0:T(8,128)(2,1)}), bf16[8,32,256]{2,1,0:T(8,128)(2,1)S(1)}, u32[]{:S(2)}, u32[]{:S(2)}) async-start(bf16[8,32,256]{2,1,0:T(8,128)(2,1)} %prefix.1), calls=%async_computation.2 | async-start | bytes 262144 | tf_op jit(solution)/shard_map/all_to_all | solution.py:284
  68.8 0.7 copy-start.2
  73.4 25.3 %all-to-all-start.3 = ((bf16[8,272,256]{2,1,0:T(8,128)(2,1)}), bf16[8,272,256]{2,1,0:T(8,128)(2,1)S(1)}, u32[]{:S(2)}, u32[]{:S(2)}) async-start(bf16[8,272,256]{2,1,0:T(8,128)(2,1)} %apply_project.1), calls=%async_computation.3 | async-start | bytes 2228224 | tf_op jit(solution)/shard_map/all_to_all | solution.py:284
  98.7 1.1 copy-start.1
  102.2 3.1 %collective-permute-start.1 = (bf16[8,256]{1,0:T(8,128)(2,1)}, bf16[8,256]{1,0:T(8,128)(2,1)S(1)}, u32[]{:S(2)}, u32[]{:S(2)}) collective-permute-start(bf16[8,256]{1,0:T(8,128)(2,1)} %get-tuple-element.26), channel_id=1, source_target_pairs={{0,8},{8,16},{16,24},{24,32},{32,40},{40,48},{48,56},{56,64},{64,7... | collective-permute-start | bytes 12296 | tf_op jit(solution)/shard_map/ppermute | solution.py:289
  107.4 5.4 %copy-start.6 = (bf16[2,3,640]{2,0,1:T(2,128)(2,1)S(1)}, bf16[2,3,640]{2,0,1:T(2,128)(2,1)}, u32[]{:S(2)}) copy-start(bf16[2,3,640]{2,0,1:T(2,128)(2,1)} %param.30) | copy-start | bytes 23044
  107.4 21.1 %all-to-all-start.4 = ((bf16[8,272,256]{2,1,0:T(8,128)(2,1)}), bf16[8,272,256]{2,1,0:T(8,128)(2,1)S(1)}, u32[]{:S(2)}, u32[]{:S(2)}) async-start(bf16[8,272,256]{2,1,0:T(8,128)(2,1)} %broadcast_in_dim.7), calls=%async_computation.4 | async-start | bytes 2228224 | tf_op jit(solution)/shard_map/all_to_all | solution.py:284
  128.5 1.1 copy-start
  163.3 0.9 copy-start.4
Sparse Core Ops, SparseCore 0:
  10.3 102.8 all-gather.1

commit v2 on v1

--- a/solution.py
+++ b/solution.py
@@ -22,13 +22,28 @@
 FIRST = (((0,), (0,)), ((), ()))
 
 
-def call(kernel, outs, scratch=(), **more):
+SMEM = pl.BlockSpec(memory_space=pltpu.SMEM)
+VMEM = pl.BlockSpec(memory_space=pltpu.VMEM)
+
+
+def call(kernel, outs, scratch=(), grant=12, more_scratch=(), **more):
     return pl.pallas_call(
         kernel,
         out_shape=[jax.ShapeDtypeStruct(shape, kind) for shape, kind in outs],
-        scratch_shapes=[pltpu.VMEM(shape, kind) for shape, kind in scratch],
+        scratch_shapes=[pltpu.VMEM(shape, kind) for shape, kind in scratch] + list(more_scratch),
+        compiler_params=pltpu.CompilerParams(vmem_limit_bytes=grant << 20),
         **more,
     )
+
+
+def pack_kernel(gate, up, down, values, keys, rows_out, tail_out):
+    units = gate.shape[1]
+    cols = values.shape[1]
+    rows_out[:, :units] = gate[...]
+    rows_out[:, units : 2 * units] = up[...]
+    rows_out[:, 2 * units :] = down[...]
+    tail_out[:, :cols] = values[...]
+    tail_out[:, cols:] = keys[...]
 
 
 def silu(a):
@@ -88,7 +103,11 @@
     upper = lax.broadcasted_iota(jnp.int32, (rows, rows), 0) <= lax.broadcasted_iota(
         jnp.int32, (rows, rows), 1
     )
-    run = jnp.dot(-rate[...] * delta, upper.astype(F32), precision=HIGHEST, preferred_element_type=F32)
+    head = lax.broadcasted_iota(jnp.int32, delta.shape, 0)
+    rates = jnp.zeros(delta.shape, F32)
+    for h in range(GROUP_HEADS):
+        rates = jnp.where(head == h, rate[h], rates)
+    run = jnp.dot(-rates * delta, upper.astype(F32), precision=HIGHEST, preferred_element_type=F32)
     run_out[...] = run
     delta_out[...] = delta
     run_t = jnp.transpose(run)
@@ -189,7 +208,7 @@
         total = total * fade(wide, narrow) + state
 
 
-def apply_kernel(base, slope, keys, got, gain, weight, pay):
+def apply_kernel(core, base, slope, keys, got, gain, weight, keep, give):
     count = got.shape[0]
     w = STATE_WIDE // count
     n = STATE_NARROW // count
@@ -202,14 +221,21 @@
     from_narrow = jnp.dot(k[:, wide_end + STATE_NARROW :], narrow, preferred_element_type=F32)
     gated = base[...] + slope[...] * jnp.concatenate([from_wide, from_narrow], axis=1)
     squares = as_row(jnp.sum(gated * gated, axis=1, keepdims=True))
-    marks = pieces(squares, 2) + [jnp.zeros((14, squares.shape[1]), F32)]
-    marks = jnp.concatenate(marks, axis=0).astype(BF16)
+    lanes = squares.shape[1]
+    hi_lo = pieces(squares, 2)
+    blank = jnp.zeros((2, lanes), F32)
+    rest = jnp.zeros((12, lanes), F32)
+    marks = jnp.concatenate(hi_lo + [blank, rest], axis=0).astype(BF16)
+    given = jnp.concatenate([blank] + hi_lo + [rest], axis=0).astype(BF16)
     scaled = (gated * gain[...]).astype(BF16)
-    rows, share = scaled.shape[0], pay.shape[2]
-    for c in range(pay.shape[0]):
-        part = jnp.dot(scaled, weight[:, c * share : (c + 1) * share], preferred_element_type=F32)
-        pay[c, 0:rows, :] = part.astype(BF16)
-        pay[c, rows : rows + 16, :] = marks
+    rows, share = scaled.shape[0], keep.shape[2]
+    mine = core[0]
+    for target, side, mark in ((give, 1 - mine, given), (keep, mine, marks)):
+        for c in range(target.shape[0]):
+            at = pl.multiple_of((2 * c + side) * share, share)
+            part = jnp.dot(scaled, weight[:, pl.ds(at, share)], preferred_element_type=F32)
+            target[c, 0:rows, :] = part.astype(BF16)
+            target[c, rows : rows + 16, :] = mark
 
 
 def merge_kernel(channels, got, residual, gain, lifted_out, tile_out, merged_out):
@@ -217,7 +243,7 @@
     total = got[0].astype(F32)
     for c in range(1, got.shape[0]):
         total = total + got[c].astype(F32)
-    squares = total[rows : rows + 1] + total[rows + 1 : rows + 2]
+    squares = jnp.sum(total[rows : rows + 8], axis=0, keepdims=True)
     inverse = as_col(lax.rsqrt(squares / channels + NORM_FLOOR))
     merged = jnp.transpose(residual[...].astype(F32)) + inverse * total[:rows]
     merged = merged.astype(BF16).astype(F32)
@@ -230,54 +256,62 @@
     tile_out[...] = jnp.concatenate(tile, axis=0).astype(BF16)
 
 
-def channel_kernel(blocks, features, got, weight_in, weight_out, taps, pay, total, marks, buf, hidden):
-    step = pl.program_id(0)
-    rows = hidden.shape[0]
+def channel_kernel(features, core, own, other, weights, taps, keep, give, lhs, wide, down, buf, hidden, sems):
+    chips, high, share = own.shape
+    rows = high - 16
     units = hidden.shape[1]
-
-    @pl.when(step < blocks)
-    def _():
-        mine = got[0]
-        part = jnp.dot(mine, weight_in[...], preferred_element_type=F32)
-        mark = mine[rows : rows + 16].astype(F32)
-
-        @pl.when(step == 0)
-        def _():
-            total[...] = part
-            marks[...] = mark
-
-        @pl.when(step > 0)
-        def _():
-            total[...] += part
-            marks[...] += mark
-
-    @pl.when(step == blocks - 1)
-    def _():
-        def inverse_of(at):
-            squares = marks[at : at + 1, :] + marks[at + 1 : at + 2, :]
-            return as_col(lax.rsqrt(squares / features + NORM_FLOOR))
-
-        own, before = inverse_of(0), inverse_of(8)
-        buf[0:8, :] = (total[rows + 8 : rows + 16, :] * before[rows - 8 :, :]).astype(BF16).astype(F32)
-        buf[8 : 8 + rows, :] = (total[0:rows, :] * own).astype(BF16).astype(F32)
-
-        def conv(branch):
-            first, last = branch * units, (branch + 1) * units
-            count = taps.shape[1]
-            summed = None
-            for k in range(count):
-                at = 8 - (count - 1) + k
-                term = taps[branch, k : k + 1, :].astype(F32) * buf[at : at + rows, first:last]
-                summed = term if summed is None else summed + term
-            return summed
-
-        hidden[...] = (silu(conv(0)) * conv(1)).astype(BF16)
-
-    @pl.when(step >= blocks)
-    def _():
-        pay[0] = lax.dot_general(
-            weight_out[...], hidden[...], LAST, preferred_element_type=F32
-        ).astype(BF16)
+    step = wide.shape[2]
+    copies = []
+    for n in range(wide.shape[0]):
+        copies.append(
+            pltpu.make_async_copy(weights.at[:, n * step : (n + 1) * step], wide.at[n], sems.at[n])
+        )
+    copies.append(
+        pltpu.make_async_copy(weights.at[:, 2 * units :], down, sems.at[wide.shape[0]])
+    )
+    for copy in copies:
+        copy.start()
+    mine = core[0]
+    marks = jnp.zeros((16, share), F32)
+    for c in range(chips):
+        first, second = own[c], other[c]
+        marks = marks + first[rows:].astype(F32) + second[rows:].astype(F32)
+        at = 2 * c * share
+        lhs[:, at : at + share] = jnp.where(mine == 0, first, second)
+        lhs[:, at + share : at + 2 * share] = jnp.where(mine == 0, second, first)
+
+    def inverse_of(at):
+        squares = marks[at : at + 1, :] + marks[at + 1 : at + 2, :]
+        return as_col(lax.rsqrt(squares / features + NORM_FLOOR))
+
+    scale, before = inverse_of(0), inverse_of(8)
+    for n in range(wide.shape[0]):
+        copies[n].wait()
+        total = jnp.dot(lhs[...], wide[n], preferred_element_type=F32)
+        at = n * step
+        edge = total[rows + 8 :] * before[rows - 8 :, :]
+        buf[0:8, at : at + step] = edge.astype(BF16).astype(F32)
+        buf[8 : 8 + rows, at : at + step] = (total[:rows] * scale).astype(BF16).astype(F32)
+
+    def conv(branch):
+        first, last = branch * units, (branch + 1) * units
+        count = taps.shape[1]
+        summed = None
+        for k in range(count):
+            at = 8 - (count - 1) + k
+            term = taps[branch, k : k + 1, :].astype(F32) * buf[at : at + rows, first:last]
+            summed = term if summed is None else summed + term
+        return summed
+
+    hidden[...] = (silu(conv(0)) * conv(1)).astype(BF16)
+    copies[-1].wait()
+    for target, side in ((give, 1 - mine), (keep, mine)):
+        for c in range(chips):
+            at = pl.multiple_of((2 * c + side) * share, share)
+            part = lax.dot_general(
+                down[pl.ds(at, share), :], hidden[...], LAST, preferred_element_type=F32
+            )
+            target[c] = part.astype(BF16)
 
 
 def exchange(parts, axis):
@@ -287,6 +321,15 @@
 def from_behind(value, axis):
     count = lax.axis_size(axis)
     return lax.ppermute(value, axis, [(source, source + 1) for source in range(count - 1)])
+
+
+def swapped(value):
+    return lax.ppermute(value, "core", [(0, 1), (1, 0)])
+
+
+def pair_then_chips(kept, given):
+    both = (kept.astype(F32) + swapped(given).astype(F32)).astype(BF16)
+    return exchange(both, "x")
 
 
 def local(
@@ -307,16 +350,27 @@
     hidden_conv,
     hidden_down,
 ):
-    own_rows = jnp.concatenate([hidden_gate, hidden_up, hidden_down.T], axis=1)
+    rows, cols = values.shape
+    key_cols = group_keys.shape[1]
+    last = rows // 8 - 1
+    whole = lambda a: pl.BlockSpec(a.shape, lambda i: (0, 0))
+    own_rows, tail = call(
+        pack_kernel,
+        [((hidden_gate.shape[0], 3 * hidden_gate.shape[1]), BF16), ((8, cols + key_cols), BF16)],
+        grid=(1,),
+        in_specs=[whole(hidden_gate), whole(hidden_up), whole(hidden_gate)]
+        + [pl.BlockSpec((8, width), lambda i: (last, 0)) for width in (cols, key_cols)],
+        grant=60,
+        name="pack",
+    )(hidden_gate, hidden_up, hidden_down.T, values, group_keys)
     weights = lax.all_gather(own_rows, SP, axis=0, tiled=True)
-    rows, cols = values.shape
-    n_tp = lax.axis_size("tp")
+    chips = lax.axis_size("x")
+    n_tp = chips * lax.axis_size("core")
     n_row = lax.axis_size(SP[1])
     features = residual.shape[0]
     units = hidden_gate.shape[1]
-    tail = jnp.concatenate([values[rows - 8 :], group_keys[rows - 8 :]], axis=1)
     before = from_behind(tail, SP)
-    key_cols = group_keys.shape[1]
+    core = lax.axis_index("core").astype(jnp.int32).reshape(1)
     span = STATE_WIDE // n_row + STATE_NARROW // n_row + 8
     x, keys, run, delta, run_col, pay = call(
         state_kernel,
@@ -329,13 +383,15 @@
             ((n_row, span, HALF), BF16),
         ],
         [((rows + 8, cols), F32), ((rows + 8, key_cols), F32)],
+        in_specs=[VMEM, VMEM, VMEM, VMEM, SMEM, VMEM, VMEM],
+        grant=60,
         name="span_state",
     )(
         values,
         group_keys,
         before,
         time_step,
-        decay_rate.reshape(-1, 1),
+        decay_rate,
         conv_values,
         conv_keys,
     )
@@ -359,60 +415,64 @@
         name="prefix",
     )(place, by_row, totals)
     carried = exchange(starts, SP[1])
-    (partial,) = call(
-        apply_kernel, [((n_tp, rows + 16, features), BF16)], name="apply_project"
-    )(base, slope, keys, carried, mix_gain.reshape(1, -1), out_weight)
-    summed = exchange(partial, "tp")
-    own_gain = lax.dynamic_slice_in_dim(norm_gain, lax.axis_index("tp") * features, features, 0)
+    kept, given = call(
+        apply_kernel,
+        [((chips, rows + 16, features), BF16)] * 2,
+        in_specs=[SMEM] + [VMEM] * 6,
+        name="apply_project",
+    )(core, base, slope, keys, carried, mix_gain.reshape(1, -1), out_weight)
+    summed = pair_then_chips(kept, given)
+    place_tp = lax.axis_index(("x", "core"))
+    own_gain = lax.dynamic_slice_in_dim(norm_gain, place_tp * features, features, 0)
     lifted, tile, merged = call(
         functools.partial(merge_kernel, cols * n_tp),
         [((rows, features), BF16), ((8, features), BF16), ((features, rows), BF16)],
         name="merge",
     )(summed, residual, own_gain.reshape(1, -1))
     stream = jnp.concatenate([lifted, tile, from_behind(tile, SP)], axis=0)
-    stream = exchange(jnp.broadcast_to(stream, (n_tp, *stream.shape)), "tp")
-    down_first = 2 * units // units
-    (down,) = call(
-        functools.partial(channel_kernel, n_tp, features * n_tp),
-        [((n_tp, features, rows), BF16)],
+    own_core = exchange(jnp.broadcast_to(stream, (chips, *stream.shape)), "x")
+    other_core = swapped(own_core)
+    step = 256
+    kept, given = call(
+        functools.partial(channel_kernel, features * n_tp),
+        [((chips, features, rows), BF16)] * 2,
         [
-            ((rows + 16, 2 * units), F32),
-            ((16, features), F32),
+            ((rows + 16, features * n_tp), BF16),
+            ((2 * units // step, features * n_tp, step), BF16),
+            ((features * n_tp, units), BF16),
             ((rows + 8, 2 * units), F32),
             ((rows, units), BF16),
         ],
-        grid=(2 * n_tp,),
-        in_specs=[
-            pl.BlockSpec((1, rows + 16, features), lambda i: (jnp.minimum(i, n_tp - 1), 0, 0)),
-            pl.BlockSpec((features, 2 * units), lambda i: (jnp.minimum(i, n_tp - 1), 0)),
-            pl.BlockSpec((features, units), lambda i: (jnp.maximum(i - n_tp, 0), down_first)),
-            pl.BlockSpec(hidden_conv.shape, lambda i: (0, 0, 0)),
-        ],
-        out_specs=[pl.BlockSpec((1, features, rows), lambda i: (jnp.maximum(i - n_tp, 0), 0, 0))],
+        more_scratch=[pltpu.SemaphoreType.DMA((2 * units // step + 1,))],
+        grant=24,
+        in_specs=[SMEM, VMEM, VMEM, pl.BlockSpec(memory_space=pltpu.HBM), VMEM],
         name="channel_mixer",
-    )(stream, weights, weights, hidden_conv)
-    got = exchange(down, "tp")
+    )(
+        core, own_core, other_core, pltpu.with_memory_space_constraint(weights, pltpu.HBM), hidden_conv
+    )
+    got = pair_then_chips(kept, given)
     return (merged.astype(F32) + jnp.sum(got.astype(F32), axis=0)).astype(BF16)
 
 
 def solution(mesh):
-    split = Mesh(mesh.devices.reshape(8, 8, mesh.shape["tp"]), ("sp_0", "sp_1", "tp"))
+    split = Mesh(mesh.devices.reshape(8, 8, 4, 2), ("sp_0", "sp_1", "x", "core"))
+    tp = ("x", "core")
     placed = (
-        P("tp", SP),
-        P(SP, "tp"),
-        P(SP, "tp"),
-        P(SP, "tp"),
-        P("tp", SP),
-        P("tp"),
-        P("tp"),
-        P(None, "tp"),
-        P(None, "tp"),
-        P("tp"),
-        P("tp", None),
+        P(tp, SP),
+        P(SP, tp),
+        P(SP, tp),
+        P(SP, tp),
+        P(tp, SP),
+        P(tp),
+        P(tp),
+        P(None, tp),
+        P(None, tp),
+        P(tp),
+        P(tp, None),
         P(),
-        P(SP, "tp"),
-        P(SP, "tp"),
-        P(None, None, "tp"),
-        P("tp", SP),
-    )
-    return jax.shard_map(local, mesh=split, in_specs=placed, out_specs=P("tp", SP), check_vma=False)
+        P(SP, tp),
+        P(SP, tp),
+        P(None, None, tp),
+        P(tp, SP),
+    )
+    return jax.shard_map(local, mesh=split, in_specs=placed, out_specs=P(tp, SP), check_vma=False)

time: 175 us -> 145 us (0.83); the launches traced: 172 us -> 144 us
  Pallas kernels: 30.1 us -> 15 us
  waiting for transfers between devices: 42.9 us -> 29 us
  local copies, waits for them, and re-layouts: 11.3 us -> 5.77 us
  starting transfers between devices: 35.2 us -> 40.5 us
  blocking collectives: 35.5 us -> 38.7 us
    all_to_all x4 -> x3, waiting for transfers between devices: 41.9 us -> 19 us  [exchange(): return lax.all_to_all(parts, axis, split_axis=0, concat_axis=0, tiled=True)]
    ppermute x0 -> x3, starting transfers between devices: none -> 16.2 us  [swapped(): return lax.ppermute(value, 'core', [(0, 1), (1, 0)])]
    all_to_all x4 -> x3, starting transfers between devices: 29.1 us -> 18.1 us  [exchange(): return lax.all_to_all(parts, axis, split_axis=0, concat_axis=0, tiled=True)]
    pallas_call x2 -> x3, Pallas kernels: 18.2 us -> 9.07 us  [the longest x1 6.75 us: local(): call(functools.partial(channel_kernel, features * n_tp), [((chips, featur...]
    ppermute x0 -> x3, waiting for transfers between devices: none -> 4.61 us  [swapped(): return lax.ppermute(value, 'core', [(0, 1), (1, 0)])]
    all_gather x1, waiting for transfers between devices: 0.01 us -> 3.56 us  [local(): weights = lax.all_gather(own_rows, SP, axis=0, tiled=True)]
    all_to_all x2 -> x3, blocking collectives: 35.5 us -> 38.7 us  [exchange(): return lax.all_to_all(parts, axis, split_axis=0, concat_axis=0, tiled=True)]
    pallas_call x1, Pallas kernels: 3.17 us -> 1.06 us  [local(): call(inside_kernel, [((rows, cols), F32), ((rows, cols), F32)], name='ins...]
  transfers between devices with their start and end apart: 7 -> 9, of which waited for: 5 -> 9; matrix products, arithmetic and copies ran while one was open for 4% -> 1% of each run, Pallas kernels for 9% -> 5%
where the time goes in v2:
time: 145 us; the launch traced here: 144 us
  starting transfers between devices  40.5 us (28%)
  blocking collectives  38.7 us (27%)
  waiting for transfers between devices  29 us (20%)
  Pallas kernels  15 us (10%)
  between operations  13.5 us (9%)
  local copies, waits for them, and re-layouts  5.77 us (4%)
  other arithmetic  1.9 us (1%)
    all_to_all x3, blocking collectives, exchange(): return lax.all_to_all(parts, axis, split_axis=0, concat_axis=0, tiled=True)  38.7 us
    all_to_all x3, waiting for transfers between devices, exchange(): return lax.all_to_all(parts, axis, split_axis=0, concat_axis=0, tiled=True)  19 us
    all_to_all x3, starting transfers between devices, exchange(): return lax.all_to_all(parts, axis, split_axis=0, concat_axis=0, tiled=True)  18.1 us
    ppermute x3, starting transfers between devices, swapped(): return lax.ppermute(value, 'core', [(0, 1), (1, 0)])  16.2 us
    pallas_call x1, Pallas kernels, local(): call(functools.partial(channel_kernel, features * n_tp), [((chips, featur...  6.75 us
    ppermute x2, starting transfers between devices, from_behind(): lax.ppermute(value, axis, [(source, source + 1) for source in range(count...  6.21 us
    unnamed x25, local copies, waits for them, and re-layouts  4.82 us
    ppermute x3, waiting for transfers between devices, swapped(): return lax.ppermute(value, 'core', [(0, 1), (1, 0)])  4.61 us
  transfers between devices with their start and end apart: 9, of which 9 were waited for; matrix products, arithmetic and copies ran while one was open for 1% of the time, Pallas kernels for 5%

profile of v2, /device:TPU:1, one launch (start us, length us, event | category | flops | bytes accessed | tf_op | source)
XLA Modules:
  0.0 144.4 jit_solution(15465318632848412040)
XLA Ops:
  6.5 0.0 all-gather.2.cloned.1.call-start
  6.5 1.5 %pack.1 = (bf16[32,1920]{1,0:T(8,128)(2,1)}, bf16[8,896]{1,0:T(8,128)(2,1)}) custom-call(bf16[32,640]{1,0:T(8,128)(2,1)} %gate.2, bf16[32,640]{1,0:T(8,128)(2,1)} %up.1, bf16[32,640]{1,0:T(8,128)(2,1)} %bitcast.7, bf16[256,512]{1,0:T(8,128)(2,1)} %values.3, bf16[256,384]{1,0:T(8,128)(2,1)} %keys.3), custom_call_target="tpu_custom_call" | custom-call | tf_op jit(solution)/shard_map/pack/pallas_call | solution.py:357
  8.0 0.0 all-gather.2.cloned.1.call-update
  8.1 4.0 %collective-permute-start = (bf16[8,896]{1,0:T(8,128)(2,1)}, bf16[8,896]{1,0:T(8,128)(2,1)S(1)}, u32[]{:S(2)}, u32[]{:S(2)}) collective-permute-start(bf16[8,896]{1,0:T(8,128)(2,1)} %get-tuple-element.22), channel_id=1, source_target_pairs={{0,8},{8,16},{16,24},{24,32},{32,40},{40,48},{48,56},{56,64},{64,7... | collective-permute-start | bytes 43016 | tf_op jit(solution)/shard_map/ppermute | solution.py:323
  12.1 1.0 collective-permute-done.before
  13.1 0.6 copy-done.9
  13.7 3.0 %span_state.1 = (bf16[256,512]{1,0:T(8,128)(2,1)}, bf16[256,384]{1,0:T(8,128)(2,1)}, f32[8,256]{1,0:T(8,128)}, f32[8,256]{1,0:T(8,128)}, f32[256,8]{1,0:T(8,128)}, /*index=5*/bf16[8,32,256]{2,1,0:T(8,128)(2,1)}) custom-call(bf16[256,512]{1,0:T(8,128)(2,1)} %values.3, bf16[256,384]{1,0:T(8,128)(2,1)} %keys.3, bf16[8,896]{1,0:T(8,128)(2,1)} %copy-done.9, ...), custom_call_target="tpu_custom_call" | custom-call | tf_op jit(solution)/shard_map/span_state/pallas_call | solution.py:375
  16.8 16.6 %all_to_all.30.got = bf16[8,32,256]{2,1,0:T(8,128)(2,1)S(1)} all-to-all(bf16[8,32,256]{2,1,0:T(8,128)(2,1)} %get-tuple-element.30), channel_id=1, replica_groups=mesh['sp_0'=8,'sp_1'=8,'x'=4,'core'=2] {'sp_1'}, dimensions={0} | all-to-all | bytes 262144 | tf_op jit(solution)/shard_map/all_to_all | solution.py:318
  33.4 0.7 row_total.1
  34.1 10.6 %all-to-all-start.1 = ((bf16[8,32,256]{2,1,0:T(8,128)(2,1)}), bf16[8,32,256]{2,1,0:T(8,128)(2,1)S(1)}, u32[]{:S(2)}, u32[]{:S(2)}) async-start(bf16[8,32,256]{2,1,0:T(8,128)(2,1)} %row_total.1), calls=%async_computation.1 | async-start | bytes 262144 | tf_op jit(solution)/shard_map/all_to_all | solution.py:318
  44.7 8.1 %all-to-all-done.1.totals = bf16[8,32,256]{2,1,0:T(8,128)(2,1)S(1)} async-done(((bf16[8,32,256]{2,1,0:T(8,128)(2,1)}), bf16[8,32,256]{2,1,0:T(8,128)(2,1)S(1)}, u32[]{:S(2)}, u32[]{:S(2)}) %all-to-all-start.1) | async-done | bytes 131104 | tf_op jit(solution)/shard_map/all_to_all | solution.py:318
  52.8 0.7 prefix.1
  53.5 3.4 %all-to-all-start.2 = ((bf16[8,32,256]{2,1,0:T(8,128)(2,1)}), bf16[8,32,256]{2,1,0:T(8,128)(2,1)S(1)}, u32[]{:S(2)}, u32[]{:S(2)}) async-start(bf16[8,32,256]{2,1,0:T(8,128)(2,1)} %prefix.1), calls=%async_computation.2 | async-start | bytes 262144 | tf_op jit(solution)/shard_map/all_to_all | solution.py:318
  56.9 0.0 copy-done.11
  56.9 0.1 broadcast_in_dim.6
  57.0 0.1 reshape_reshape.3.skip
  57.0 0.0 copy-done.1
  57.1 0.9 copy-done.2
  58.0 0.9 copy-done.3
  59.0 0.9 copy-done.5
  59.9 0.7 copy-done.6
  60.6 0.7 copy-done.7
  61.3 1.1 inside_span.1
  62.3 2.4 %all-to-all-done.2.got = bf16[8,32,256]{2,1,0:T(8,128)(2,1)S(1)} async-done(((bf16[8,32,256]{2,1,0:T(8,128)(2,1)}), bf16[8,32,256]{2,1,0:T(8,128)(2,1)S(1)}, u32[]{:S(2)}, u32[]{:S(2)}) %all-to-all-start.2) | async-done | bytes 131104 | tf_op jit(solution)/shard_map/all_to_all | solution.py:318
  64.7 0.0 copy-done.8
  64.7 0.0 copy-done
  64.7 0.8 apply_project.1
  65.6 7.8 %collective-permute-start.1 = (bf16[4,272,256]{2,1,0:T(8,128)(2,1)S(1)}, bf16[4,272,256]{2,1,0:T(8,128)(2,1)S(1)}, u32[]{:S(2)}, u32[]{:S(2)}) collective-permute-start(bf16[4,272,256]{2,1,0:T(8,128)(2,1)S(1)} %get-tuple-element.32), channel_id=1, source_target_pairs={{0,1},{1,0},{2,3},{3,2},{4,5},{5,4},{6,7},{7,6},{8,9},{9,8},{10,11... | collective-permute-start | bytes 1671176 | tf_op jit(solution)/shard_map/ppermute | solution.py:327
  73.4 1.6 %collective-permute-done.1 = bf16[4,272,256]{2,1,0:T(8,128)(2,1)S(1)} collective-permute-done((bf16[4,272,256]{2,1,0:T(8,128)(2,1)S(1)}, bf16[4,272,256]{2,1,0:T(8,128)(2,1)S(1)}, u32[]{:S(2)}, u32[]{:S(2)}) %collective-permute-start.1) | collective-permute-done | bytes 557088 | tf_op jit(solution)/shard_map/ppermute | solution.py:327
  75.0 1.0 add_convert_fusion
  75.9 4.2 %all-to-all-start.3 = ((bf16[4,272,256]{2,1,0:T(8,128)(2,1)}), bf16[4,272,256]{2,1,0:T(8,128)(2,1)S(1)}, u32[]{:S(2)}, u32[]{:S(2)}) async-start(bf16[4,272,256]{2,1,0:T(8,128)(2,1)} %add_convert_fusion), calls=%async_computation.3 | async-start | bytes 1114112 | tf_op jit(solution)/shard_map/all_to_all | solution.py:318
  80.1 0.8 dynamic_slice.3
  80.9 8.5 %all-to-all-done.3.got = bf16[4,272,256]{2,1,0:T(8,128)(2,1)S(1)} async-done(((bf16[4,272,256]{2,1,0:T(8,128)(2,1)}), bf16[4,272,256]{2,1,0:T(8,128)(2,1)S(1)}, u32[]{:S(2)}, u32[]{:S(2)}) %all-to-all-start.3) | async-done | bytes 557088 | tf_op jit(solution)/shard_map/all_to_all | solution.py:318
  89.4 0.4 merge.1
  89.8 0.0 copy-start.10
  89.8 2.2 %collective-permute-start.2 = (bf16[8,256]{1,0:T(8,128)(2,1)S(1)}, bf16[8,256]{1,0:T(8,128)(2,1)S(1)}, u32[]{:S(2)}, u32[]{:S(2)}) collective-permute-start(bf16[8,256]{1,0:T(8,128)(2,1)S(1)} %get-tuple-element.35), channel_id=1, source_target_pairs={{0,8},{8,16},{16,24},{24,32},{32,40},{40,48},{48,56},{56,64},{64,7... | collective-permute-start | bytes 12296 | tf_op jit(solution)/shard_map/ppermute | solution.py:323
  92.0 0.7 collective-permute-done.2
  92.8 9.7 %all_to_all.31.own = bf16[4,272,256]{2,1,0:T(8,128)(2,1)S(1)} all-to-all(bf16[4,272,256]{2,1,0:T(8,128)(2,1)S(1)} %broadcast_in_dim.7), channel_id=1, replica_groups=mesh['sp_0'=8,'sp_1'=8,'x'=4,'core'=2] {'x'}, dimensions={0} | all-to-all | bytes 1114112 | tf_op jit(solution)/shard_map/all_to_all | solution.py:318
  102.5 5.4 %collective-permute-start.3 = (bf16[4,272,256]{2,1,0:T(8,128)(2,1)S(1)}, bf16[4,272,256]{2,1,0:T(8,128)(2,1)S(1)}, u32[]{:S(2)}, u32[]{:S(2)}) collective-permute-start(bf16[4,272,256]{2,1,0:T(8,128)(2,1)S(1)} %all_to_all.31.own), channel_id=1, source_target_pairs={{0,1},{1,0},{2,3},{3,2},{4,5},{5,4},{6,7},{7,6},{8,9},{9,8},{10,11... | collective-permute-start | bytes 1671176 | tf_op jit(solution)/shard_map/ppermute | solution.py:327
  107.9 1.5 %collective-permute-done.3.other = bf16[4,272,256]{2,1,0:T(8,128)(2,1)S(1)} collective-permute-done((bf16[4,272,256]{2,1,0:T(8,128)(2,1)S(1)}, bf16[4,272,256]{2,1,0:T(8,128)(2,1)S(1)}, u32[]{:S(2)}, u32[]{:S(2)}) %collective-permute-start.3) | collective-permute-done | bytes 557088 | tf_op jit(solution)/shard_map/ppermute | solution.py:327
  109.4 3.6 %all-gather.2.cloned.1.call-done.weights = bf16[2048,1920]{1,0:T(8,128)(2,1)} async-done(((bf16[32,1920]{1,0:T(8,128)(2,1)}), bf16[2048,1920]{1,0:T(8,128)(2,1)}) %all-gather.2.cloned.1.call-update) | async-done | bytes 7864336 | tf_op jit(solution)/shard_map/all_gather | solution.py:366
  113.0 6.7 %channel_mixer.1 = (bf16[4,256,256]{2,1,0:T(8,128)(2,1)S(1)}, bf16[4,256,256]{2,1,0:T(8,128)(2,1)S(1)}) custom-call(s32[1]{0:T(128)} %bitcast.core, bf16[4,272,256]{2,1,0:T(8,128)(2,1)S(1)} %all_to_all.31.own, bf16[4,272,256]{2,1,0:T(8,128)(2,1)S(1)} %collective-permute-done.3.other, bf16[2048,1920]{1,0:T(8,128)(2,1)} %all-gather.2.cloned.1.call-done.weights, ...), custom_call_target="tpu_custom_call" | custom-call | tf_op jit(solution)/shard_map/channel_mixer/pallas_call | solution.py:436
  119.8 3.0 %collective-permute-start.4 = (bf16[4,256,256]{2,1,0:T(8,128)(2,1)S(1)}, bf16[4,256,256]{2,1,0:T(8,128)(2,1)S(1)}, u32[]{:S(2)}, u32[]{:S(2)}) collective-permute-start(bf16[4,256,256]{2,1,0:T(8,128)(2,1)S(1)} %get-tuple-element.38), channel_id=1, source_target_pairs={{0,1},{1,0},{2,3},{3,2},{4,5},{5,4},{6,7},{7,6},{8,9},{9,8},{10,11... | collective-permute-start | bytes 1572872 | tf_op jit(solution)/shard_map/ppermute | solution.py:327
  122.8 1.5 %collective-permute-done.4 = bf16[4,256,256]{2,1,0:T(8,128)(2,1)S(1)} collective-permute-done((bf16[4,256,256]{2,1,0:T(8,128)(2,1)S(1)}, bf16[4,256,256]{2,1,0:T(8,128)(2,1)S(1)}, u32[]{:S(2)}, u32[]{:S(2)}) %collective-permute-start.4) | collective-permute-done | bytes 524320 | tf_op jit(solution)/shard_map/ppermute | solution.py:327
  124.3 0.1 add_convert_fusion.1
  124.4 12.4 %all_to_all.32 = bf16[4,256,256]{2,1,0:T(8,128)(2,1)S(1)} all-to-all(bf16[4,256,256]{2,1,0:T(8,128)(2,1)S(1)} %add_convert_fusion.1), channel_id=1, replica_groups=mesh['sp_0'=8,'sp_1'=8,'x'=4,'core'=2] {'x'}, dimensions={0} | all-to-all | bytes 1048576 | tf_op jit(solution)/shard_map/all_to_all | solution.py:318
  136.8 0.1 convert_reduce_fusion
  136.9 0.7 add_convert_fusion.2
  (16 shorter events, 0.1 us)
Async XLA Ops:
  6.5 106.5 %all-gather.2.cloned.1.call-start = ((), (), s32[]{:S(2)}) async-start(), calls=%async_computation.6 | async-start | bytes 7987200 | tf_op jit(solution)/shard_map/all_gather | solution.py:366
  8.0 48.9 %copy-start.11 = (f32[8]{0:T(128)S(1)}, f32[8]{0:T(128)}, u32[]{:S(2)}) copy-start(f32[8]{0:T(128)} %param.22) | copy-start | bytes 100
  8.1 5.1 %collective-permute-start = (bf16[8,896]{1,0:T(8,128)(2,1)}, bf16[8,896]{1,0:T(8,128)(2,1)S(1)}, u32[]{:S(2)}, u32[]{:S(2)}) collective-permute-start(bf16[8,896]{1,0:T(8,128)(2,1)} %get-tuple-element.22), channel_id=1, source_target_pairs={{0,8},{8,16},{16,24},{24,32},{32,40},{40,48},{48,56},{56,64},{64,7... | collective-permute-start | bytes 43016 | tf_op jit(solution)/shard_map/ppermute | solution.py:323
  13.1 0.6 copy-start.9
  13.7 51.0 %copy-start.8 = (f32[512]{0:T(512)S(1)}, f32[512]{0:T(512)}, u32[]{:S(2)}) copy-start(f32[512]{0:T(512)} %param.25) | copy-start | bytes 6148
  16.7 40.3 %copy-start.1 = (bf16[256,384]{1,0:T(8,128)(2,1)S(1)}, bf16[256,384]{1,0:T(8,128)(2,1)}, u32[]{:S(2)}) copy-start(bf16[256,384]{1,0:T(8,128)(2,1)} %get-tuple-element.24.keys) | copy-start | bytes 589828
  16.7 48.0 %copy-start = (bf16[512,2048]{1,0:T(8,128)(2,1)S(1)}, bf16[512,2048]{1,0:T(8,128)(2,1)}, u32[]{:S(2)}) copy-start(bf16[512,2048]{1,0:T(8,128)(2,1)} %weight.1) | copy-start | bytes 6291460
  34.1 18.7 %all-to-all-start.1 = ((bf16[8,32,256]{2,1,0:T(8,128)(2,1)}), bf16[8,32,256]{2,1,0:T(8,128)(2,1)S(1)}, u32[]{:S(2)}, u32[]{:S(2)}) async-start(bf16[8,32,256]{2,1,0:T(8,128)(2,1)} %row_total.1), calls=%async_computation.1 | async-start | bytes 262144 | tf_op jit(solution)/shard_map/all_to_all | solution.py:318
  53.5 11.2 %all-to-all-start.2 = ((bf16[8,32,256]{2,1,0:T(8,128)(2,1)}), bf16[8,32,256]{2,1,0:T(8,128)(2,1)S(1)}, u32[]{:S(2)}, u32[]{:S(2)}) async-start(bf16[8,32,256]{2,1,0:T(8,128)(2,1)} %prefix.1), calls=%async_computation.2 | async-start | bytes 262144 | tf_op jit(solution)/shard_map/all_to_all | solution.py:318
  57.0 1.0 copy-start.2
  58.0 0.9 copy-start.3
  59.0 0.9 copy-start.5
  59.9 0.7 copy-start.6
  60.6 0.7 copy-start.7
  65.6 9.4 %collective-permute-start.1 = (bf16[4,272,256]{2,1,0:T(8,128)(2,1)S(1)}, bf16[4,272,256]{2,1,0:T(8,128)(2,1)S(1)}, u32[]{:S(2)}, u32[]{:S(2)}) collective-permute-start(bf16[4,272,256]{2,1,0:T(8,128)(2,1)S(1)} %get-tuple-element.32), channel_id=1, source_target_pairs={{0,1},{1,0},{2,3},{3,2},{4,5},{5,4},{6,7},{7,6},{8,9},{9,8},{10,11... | collective-permute-start | bytes 1671176 | tf_op jit(solution)/shard_map/ppermute | solution.py:327
  74.9 14.5 %copy-start.4 = (bf16[256,256]{1,0:T(8,128)(2,1)S(1)}, bf16[256,256]{1,0:T(8,128)(2,1)}, u32[]{:S(2)}) copy-start(bf16[256,256]{1,0:T(8,128)(2,1)} %residual.1) | copy-start | bytes 393220
  75.9 13.5 %all-to-all-start.3 = ((bf16[4,272,256]{2,1,0:T(8,128)(2,1)}), bf16[4,272,256]{2,1,0:T(8,128)(2,1)S(1)}, u32[]{:S(2)}, u32[]{:S(2)}) async-start(bf16[4,272,256]{2,1,0:T(8,128)(2,1)} %add_convert_fusion), calls=%async_computation.3 | async-start | bytes 1114112 | tf_op jit(solution)/shard_map/all_to_all | solution.py:318
  89.8 18.1 %copy-start.10 = (bf16[2,3,640]{2,0,1:T(2,128)(2,1)S(1)}, bf16[2,3,640]{2,0,1:T(2,128)(2,1)}, u32[]{:S(2)}) copy-start(bf16[2,3,640]{2,0,1:T(2,128)(2,1)} %param.30) | copy-start | bytes 23044
  89.8 2.9 %collective-permute-start.2 = (bf16[8,256]{1,0:T(8,128)(2,1)S(1)}, bf16[8,256]{1,0:T(8,128)(2,1)S(1)}, u32[]{:S(2)}, u32[]{:S(2)}) collective-permute-start(bf16[8,256]{1,0:T(8,128)(2,1)S(1)} %get-tuple-element.35), channel_id=1, source_target_pairs={{0,8},{8,16},{16,24},{24,32},{32,40},{40,48},{48,56},{56,64},{64,7... | collective-permute-start | bytes 12296 | tf_op jit(solution)/shard_map/ppermute | solution.py:323
  102.5 6.9 %collective-permute-start.3 = (bf16[4,272,256]{2,1,0:T(8,128)(2,1)S(1)}, bf16[4,272,256]{2,1,0:T(8,128)(2,1)S(1)}, u32[]{:S(2)}, u32[]{:S(2)}) collective-permute-start(bf16[4,272,256]{2,1,0:T(8,128)(2,1)S(1)} %all_to_all.31.own), channel_id=1, source_target_pairs={{0,1},{1,0},{2,3},{3,2},{4,5},{5,4},{6,7},{7,6},{8,9},{9,8},{10,11... | collective-permute-start | bytes 1671176 | tf_op jit(solution)/shard_map/ppermute | solution.py:327
  119.8 4.5 %collective-permute-start.4 = (bf16[4,256,256]{2,1,0:T(8,128)(2,1)S(1)}, bf16[4,256,256]{2,1,0:T(8,128)(2,1)S(1)}, u32[]{:S(2)}, u32[]{:S(2)}) collective-permute-start(bf16[4,256,256]{2,1,0:T(8,128)(2,1)S(1)} %get-tuple-element.38), channel_id=1, source_target_pairs={{0,1},{1,0},{2,3},{3,2},{4,5},{5,4},{6,7},{7,6},{8,9},{9,8},{10,11... | collective-permute-start | bytes 1572872 | tf_op jit(solution)/shard_map/ppermute | solution.py:327
Sparse Core Ops, SparseCore 0:
  10.3 102.6 all-gather.1

commit v3 on v2

--- a/solution.py
+++ b/solution.py
@@ -37,11 +37,12 @@
 
 
 def pack_kernel(gate, up, down, values, keys, rows_out, tail_out):
-    units = gate.shape[1]
+    rows, units = gate.shape
     cols = values.shape[1]
-    rows_out[:, :units] = gate[...]
-    rows_out[:, units : 2 * units] = up[...]
-    rows_out[:, 2 * units :] = down[...]
+    rows_out[:rows, :units] = gate[...]
+    rows_out[:rows, units:] = up[...]
+    rows_out[rows:, :units] = down[: rows // 2]
+    rows_out[rows:, units:] = down[rows // 2 :]
     tail_out[:, :cols] = values[...]
     tail_out[:, cols:] = keys[...]
 
@@ -256,19 +257,25 @@
     tile_out[...] = jnp.concatenate(tile, axis=0).astype(BF16)
 
 
-def channel_kernel(features, core, own, other, weights, taps, keep, give, lhs, wide, down, buf, hidden, sems):
+def channel_kernel(
+    features, core, own, other, weights, taps, keep, give, lhs, wide, down, buf, hidden, total, sems
+):
     chips, high, share = own.shape
     rows = high - 16
     units = hidden.shape[1]
-    step = wide.shape[2]
+    spans, each, _ = wide.shape
+    half = down.shape[1]
+    quarters = 4
     copies = []
-    for n in range(wide.shape[0]):
-        copies.append(
-            pltpu.make_async_copy(weights.at[:, n * step : (n + 1) * step], wide.at[n], sems.at[n])
-        )
-    copies.append(
-        pltpu.make_async_copy(weights.at[:, 2 * units :], down, sems.at[wide.shape[0]])
-    )
+    for first, last, target, count in ((0, each, wide, quarters), (each, each + half, down, 2)):
+        step = spans // count
+        for n in range(count):
+            part = pl.ds(n * step, step)
+            copies.append(
+                pltpu.make_async_copy(
+                    weights.at[part, first:last], target.at[part], sems.at[len(copies)]
+                )
+            )
     for copy in copies:
         copy.start()
     mine = core[0]
@@ -285,13 +292,23 @@
         return as_col(lax.rsqrt(squares / features + NORM_FLOOR))
 
     scale, before = inverse_of(0), inverse_of(8)
-    for n in range(wide.shape[0]):
+    step = spans // quarters
+    depth = step * each
+    for n in range(quarters):
         copies[n].wait()
-        total = jnp.dot(lhs[...], wide[n], preferred_element_type=F32)
-        at = n * step
-        edge = total[rows + 8 :] * before[rows - 8 :, :]
-        buf[0:8, at : at + step] = edge.astype(BF16).astype(F32)
-        buf[8 : 8 + rows, at : at + step] = (total[:rows] * scale).astype(BF16).astype(F32)
+        block = wide[n * step : (n + 1) * step].reshape(depth, 2 * units)
+        part = jnp.dot(
+            lhs[:, n * depth : (n + 1) * depth], block, preferred_element_type=F32
+        )
+        if n == 0:
+            total[...] = part
+        elif n < quarters - 1:
+            total[...] += part
+        else:
+            part = total[...] + part
+            edge = part[rows + 8 :] * before[rows - 8 :, :]
+            buf[0:8, :] = edge.astype(BF16).astype(F32)
+            buf[8 : 8 + rows, :] = (part[:rows] * scale).astype(BF16).astype(F32)
 
     def conv(branch):
         first, last = branch * units, (branch + 1) * units
@@ -304,14 +321,24 @@
         return summed
 
     hidden[...] = (silu(conv(0)) * conv(1)).astype(BF16)
-    copies[-1].wait()
+    for copy in copies[quarters:]:
+        copy.wait()
+    step = share // each
     for target, side in ((give, 1 - mine), (keep, mine)):
         for c in range(chips):
-            at = pl.multiple_of((2 * c + side) * share, share)
+            block = down[pl.ds((2 * c + side) * step, step)]
+            block = jnp.concatenate([block[:, :, :units], block[:, :, units:]], axis=1)
             part = lax.dot_general(
-                down[pl.ds(at, share), :], hidden[...], LAST, preferred_element_type=F32
+                block.reshape(share, units), hidden[...], LAST, preferred_element_type=F32
             )
             target[c] = part.astype(BF16)
+
+
+def finish_kernel(merged, got, out):
+    total = merged[...].astype(F32)
+    for c in range(got.shape[0]):
+        total = total + got[c].astype(F32)
+    out[...] = total.astype(BF16)
 
 
 def exchange(parts, axis):
@@ -356,14 +383,17 @@
     whole = lambda a: pl.BlockSpec(a.shape, lambda i: (0, 0))
     own_rows, tail = call(
         pack_kernel,
-        [((hidden_gate.shape[0], 3 * hidden_gate.shape[1]), BF16), ((8, cols + key_cols), BF16)],
+        [
+            ((hidden_gate.shape[0] * 3 // 2, 2 * hidden_gate.shape[1]), BF16),
+            ((8, cols + key_cols), BF16),
+        ],
         grid=(1,),
         in_specs=[whole(hidden_gate), whole(hidden_up), whole(hidden_gate)]
         + [pl.BlockSpec((8, width), lambda i: (last, 0)) for width in (cols, key_cols)],
         grant=60,
         name="pack",
     )(hidden_gate, hidden_up, hidden_down.T, values, group_keys)
-    weights = lax.all_gather(own_rows, SP, axis=0, tiled=True)
+    weights = lax.all_gather(own_rows, SP, axis=0)
     chips = lax.axis_size("x")
     n_tp = chips * lax.axis_size("core")
     n_row = lax.axis_size(SP[1])
@@ -432,18 +462,19 @@
     stream = jnp.concatenate([lifted, tile, from_behind(tile, SP)], axis=0)
     own_core = exchange(jnp.broadcast_to(stream, (chips, *stream.shape)), "x")
     other_core = swapped(own_core)
-    step = 256
+    spans, each = weights.shape[0], hidden_gate.shape[0]
     kept, given = call(
         functools.partial(channel_kernel, features * n_tp),
         [((chips, features, rows), BF16)] * 2,
         [
             ((rows + 16, features * n_tp), BF16),
-            ((2 * units // step, features * n_tp, step), BF16),
-            ((features * n_tp, units), BF16),
+            ((spans, each, 2 * units), BF16),
+            ((spans, each // 2, 2 * units), BF16),
             ((rows + 8, 2 * units), F32),
             ((rows, units), BF16),
+            ((rows + 16, 2 * units), F32),
         ],
-        more_scratch=[pltpu.SemaphoreType.DMA((2 * units // step + 1,))],
+        more_scratch=[pltpu.SemaphoreType.DMA((6,))],
         grant=24,
         in_specs=[SMEM, VMEM, VMEM, pl.BlockSpec(memory_space=pltpu.HBM), VMEM],
         name="channel_mixer",
@@ -451,7 +482,8 @@
         core, own_core, other_core, pltpu.with_memory_space_constraint(weights, pltpu.HBM), hidden_conv
     )
     got = pair_then_chips(kept, given)
-    return (merged.astype(F32) + jnp.sum(got.astype(F32), axis=0)).astype(BF16)
+    (out,) = call(finish_kernel, [((features, rows), BF16)], name="finish")(merged, got)
+    return out
 
 
 def solution(mesh):

time: 145 us -> 144 us (level)
    pallas_call x1, Pallas kernels: 6.75 us -> 5.08 us  [local(): call(functools.partial(channel_kernel, features * n_tp), [((chips, featur...]
where the time goes in v3:
time: 144 us; the launch traced here: 143 us
  starting transfers between devices  40.8 us (28%)
  blocking collectives  38.7 us (27%)
  waiting for transfers between devices  28.7 us (20%)
  Pallas kernels  14.1 us (10%)
  between operations  13.5 us (9%)
  local copies, waits for them, and re-layouts  5.77 us (4%)
    all_to_all x3, blocking collectives, exchange(): return lax.all_to_all(parts, axis, split_axis=0, concat_axis=0, tiled=True)  38.7 us
    all_to_all x3, waiting for transfers between devices, exchange(): return lax.all_to_all(parts, axis, split_axis=0, concat_axis=0, tiled=True)  18.8 us
    all_to_all x3, starting transfers between devices, exchange(): return lax.all_to_all(parts, axis, split_axis=0, concat_axis=0, tiled=True)  18.2 us
    ppermute x3, starting transfers between devices, swapped(): return lax.ppermute(value, 'core', [(0, 1), (1, 0)])  16.4 us
    ppermute x2, starting transfers between devices, from_behind(): lax.ppermute(value, axis, [(source, source + 1) for source in range(count...  6.21 us
    pallas_call x1, Pallas kernels, local(): call(functools.partial(channel_kernel, features * n_tp), [((chips, featur...  5.08 us
    unnamed x25, local copies, waits for them, and re-layouts  4.82 us
    ppermute x3, waiting for transfers between devices, swapped(): return lax.ppermute(value, 'core', [(0, 1), (1, 0)])  4.61 us
  transfers between devices with their start and end apart: 9, of which 9 were waited for; matrix products, arithmetic and copies ran while one was open for 1% of the time, Pallas kernels for 5%

profile of v3, /device:TPU:1, one launch (start us, length us, event | category | flops | bytes accessed | tf_op | source)
XLA Modules:
  0.0 142.8 jit_solution(10305743234032700307)
XLA Ops:
  6.5 0.0 all-gather.3.cloned.1.call-start
  6.5 1.5 %pack.1 = (bf16[48,1280]{1,0:T(8,128)(2,1)}, bf16[8,896]{1,0:T(8,128)(2,1)}) custom-call(bf16[32,640]{1,0:T(8,128)(2,1)} %gate.2, bf16[32,640]{1,0:T(8,128)(2,1)} %up.1, bf16[32,640]{1,0:T(8,128)(2,1)} %bitcast.9, bf16[256,512]{1,0:T(8,128)(2,1)} %values.3, bf16[256,384]{1,0:T(8,128)(2,1)} %keys.3), custom_call_target="tpu_custom_call" | custom-call | tf_op jit(solution)/shard_map/pack/pallas_call | solution.py:384
  8.0 0.0 all-gather.3.cloned.1.call-update
  8.1 4.0 %collective-permute-start = (bf16[8,896]{1,0:T(8,128)(2,1)}, bf16[8,896]{1,0:T(8,128)(2,1)S(1)}, u32[]{:S(2)}, u32[]{:S(2)}) collective-permute-start(bf16[8,896]{1,0:T(8,128)(2,1)} %get-tuple-element.22), channel_id=1, source_target_pairs={{0,8},{8,16},{16,24},{24,32},{32,40},{40,48},{48,56},{56,64},{64,7... | collective-permute-start | bytes 43016 | tf_op jit(solution)/shard_map/ppermute | solution.py:350
  12.1 1.0 collective-permute-done.before
  13.1 0.6 copy-done.9
  13.7 3.0 %span_state.1 = (bf16[256,512]{1,0:T(8,128)(2,1)}, bf16[256,384]{1,0:T(8,128)(2,1)}, f32[8,256]{1,0:T(8,128)}, f32[8,256]{1,0:T(8,128)}, f32[256,8]{1,0:T(8,128)}, /*index=5*/bf16[8,32,256]{2,1,0:T(8,128)(2,1)}) custom-call(bf16[256,512]{1,0:T(8,128)(2,1)} %values.3, bf16[256,384]{1,0:T(8,128)(2,1)} %keys.3, bf16[8,896]{1,0:T(8,128)(2,1)} %copy-done.9, ...), custom_call_target="tpu_custom_call" | custom-call | tf_op jit(solution)/shard_map/span_state/pallas_call | solution.py:405
  16.7 16.6 %all_to_all.30.got = bf16[8,32,256]{2,1,0:T(8,128)(2,1)S(1)} all-to-all(bf16[8,32,256]{2,1,0:T(8,128)(2,1)} %get-tuple-element.30), channel_id=1, replica_groups=mesh['sp_0'=8,'sp_1'=8,'x'=4,'core'=2] {'sp_1'}, dimensions={0} | all-to-all | bytes 262144 | tf_op jit(solution)/shard_map/all_to_all | solution.py:345
  33.4 0.7 row_total.1
  34.1 10.6 %all-to-all-start.1 = ((bf16[8,32,256]{2,1,0:T(8,128)(2,1)}), bf16[8,32,256]{2,1,0:T(8,128)(2,1)S(1)}, u32[]{:S(2)}, u32[]{:S(2)}) async-start(bf16[8,32,256]{2,1,0:T(8,128)(2,1)} %row_total.1), calls=%async_computation.1 | async-start | bytes 262144 | tf_op jit(solution)/shard_map/all_to_all | solution.py:345
  44.7 7.8 %all-to-all-done.1.totals = bf16[8,32,256]{2,1,0:T(8,128)(2,1)S(1)} async-done(((bf16[8,32,256]{2,1,0:T(8,128)(2,1)}), bf16[8,32,256]{2,1,0:T(8,128)(2,1)S(1)}, u32[]{:S(2)}, u32[]{:S(2)}) %all-to-all-start.1) | async-done | bytes 131104 | tf_op jit(solution)/shard_map/all_to_all | solution.py:345
  52.5 0.7 prefix.1
  53.2 3.4 %all-to-all-start.2 = ((bf16[8,32,256]{2,1,0:T(8,128)(2,1)}), bf16[8,32,256]{2,1,0:T(8,128)(2,1)S(1)}, u32[]{:S(2)}, u32[]{:S(2)}) async-start(bf16[8,32,256]{2,1,0:T(8,128)(2,1)} %prefix.1), calls=%async_computation.2 | async-start | bytes 262144 | tf_op jit(solution)/shard_map/all_to_all | solution.py:345
  56.6 0.0 copy-done.11
  56.6 0.1 broadcast_in_dim.6
  56.7 0.1 reshape_reshape.3.skip
  56.8 0.0 copy-done.1
  56.8 0.9 copy-done.2
  57.7 0.9 copy-done.3
  58.7 0.9 copy-done.5
  59.6 0.7 copy-done.6
  60.3 0.7 copy-done.7
  61.0 1.1 inside_span.1
  62.0 2.4 %all-to-all-done.2.got = bf16[8,32,256]{2,1,0:T(8,128)(2,1)S(1)} async-done(((bf16[8,32,256]{2,1,0:T(8,128)(2,1)}), bf16[8,32,256]{2,1,0:T(8,128)(2,1)S(1)}, u32[]{:S(2)}, u32[]{:S(2)}) %all-to-all-start.2) | async-done | bytes 131104 | tf_op jit(solution)/shard_map/all_to_all | solution.py:345
  64.5 0.0 copy-done.8
  64.5 0.0 copy-done
  64.5 0.8 apply_project.1
  65.3 8.1 %collective-permute-start.1 = (bf16[4,272,256]{2,1,0:T(8,128)(2,1)S(1)}, bf16[4,272,256]{2,1,0:T(8,128)(2,1)S(1)}, u32[]{:S(2)}, u32[]{:S(2)}) collective-permute-start(bf16[4,272,256]{2,1,0:T(8,128)(2,1)S(1)} %get-tuple-element.32), channel_id=1, source_target_pairs={{0,1},{1,0},{2,3},{3,2},{4,5},{5,4},{6,7},{7,6},{8,9},{9,8},{10,11... | collective-permute-start | bytes 1671176 | tf_op jit(solution)/shard_map/ppermute | solution.py:354
  73.4 1.6 %collective-permute-done.1 = bf16[4,272,256]{2,1,0:T(8,128)(2,1)S(1)} collective-permute-done((bf16[4,272,256]{2,1,0:T(8,128)(2,1)S(1)}, bf16[4,272,256]{2,1,0:T(8,128)(2,1)S(1)}, u32[]{:S(2)}, u32[]{:S(2)}) %collective-permute-start.1) | collective-permute-done | bytes 557088 | tf_op jit(solution)/shard_map/ppermute | solution.py:354
  74.9 1.0 add_convert_fusion
  75.9 4.2 %all-to-all-start.3 = ((bf16[4,272,256]{2,1,0:T(8,128)(2,1)}), bf16[4,272,256]{2,1,0:T(8,128)(2,1)S(1)}, u32[]{:S(2)}, u32[]{:S(2)}) async-start(bf16[4,272,256]{2,1,0:T(8,128)(2,1)} %add_convert_fusion), calls=%async_computation.3 | async-start | bytes 1114112 | tf_op jit(solution)/shard_map/all_to_all | solution.py:345
  80.1 0.8 dynamic_slice.3
  80.9 8.5 %all-to-all-done.3.got = bf16[4,272,256]{2,1,0:T(8,128)(2,1)S(1)} async-done(((bf16[4,272,256]{2,1,0:T(8,128)(2,1)}), bf16[4,272,256]{2,1,0:T(8,128)(2,1)S(1)}, u32[]{:S(2)}, u32[]{:S(2)}) %all-to-all-start.3) | async-done | bytes 557088 | tf_op jit(solution)/shard_map/all_to_all | solution.py:345
  89.4 0.0 copy-done.4
  89.4 0.4 merge.1
  89.8 0.0 copy-start.10
  89.8 2.2 %collective-permute-start.2 = (bf16[8,256]{1,0:T(8,128)(2,1)S(1)}, bf16[8,256]{1,0:T(8,128)(2,1)S(1)}, u32[]{:S(2)}, u32[]{:S(2)}) collective-permute-start(bf16[8,256]{1,0:T(8,128)(2,1)S(1)} %get-tuple-element.35), channel_id=1, source_target_pairs={{0,8},{8,16},{16,24},{24,32},{32,40},{40,48},{48,56},{56,64},{64,7... | collective-permute-start | bytes 12296 | tf_op jit(solution)/shard_map/ppermute | solution.py:350
  92.0 0.7 collective-permute-done.2
  92.8 9.7 %all_to_all.31.own = bf16[4,272,256]{2,1,0:T(8,128)(2,1)S(1)} all-to-all(bf16[4,272,256]{2,1,0:T(8,128)(2,1)S(1)} %broadcast_in_dim.7), channel_id=1, replica_groups=mesh['sp_0'=8,'sp_1'=8,'x'=4,'core'=2] {'x'}, dimensions={0} | all-to-all | bytes 1114112 | tf_op jit(solution)/shard_map/all_to_all | solution.py:345
  102.5 5.4 %collective-permute-start.3 = (bf16[4,272,256]{2,1,0:T(8,128)(2,1)S(1)}, bf16[4,272,256]{2,1,0:T(8,128)(2,1)S(1)}, u32[]{:S(2)}, u32[]{:S(2)}) collective-permute-start(bf16[4,272,256]{2,1,0:T(8,128)(2,1)S(1)} %all_to_all.31.own), channel_id=1, source_target_pairs={{0,1},{1,0},{2,3},{3,2},{4,5},{5,4},{6,7},{7,6},{8,9},{9,8},{10,11... | collective-permute-start | bytes 1671176 | tf_op jit(solution)/shard_map/ppermute | solution.py:354
  107.9 1.5 %collective-permute-done.3.other = bf16[4,272,256]{2,1,0:T(8,128)(2,1)S(1)} collective-permute-done((bf16[4,272,256]{2,1,0:T(8,128)(2,1)S(1)}, bf16[4,272,256]{2,1,0:T(8,128)(2,1)S(1)}, u32[]{:S(2)}, u32[]{:S(2)}) %collective-permute-start.3) | collective-permute-done | bytes 557088 | tf_op jit(solution)/shard_map/ppermute | solution.py:354
  109.4 3.6 %all-gather.3.cloned.1.call-done = bf16[3072,1280]{1,0:T(8,128)(2,1)} async-done(((bf16[48,1280]{1,0:T(8,128)(2,1)}), bf16[3072,1280]{1,0:T(8,128)(2,1)}) %all-gather.3.cloned.1.call-update) | async-done | bytes 7864336 | tf_op jit(solution)/shard_map/all_gather | solution.py:396
  113.0 5.1 %channel_mixer.1 = (bf16[4,256,256]{2,1,0:T(8,128)(2,1)S(1)}, bf16[4,256,256]{2,1,0:T(8,128)(2,1)S(1)}) custom-call(s32[1]{0:T(128)} %bitcast.core, bf16[4,272,256]{2,1,0:T(8,128)(2,1)S(1)} %all_to_all.31.own, bf16[4,272,256]{2,1,0:T(8,128)(2,1)S(1)} %collective-permute-done.3.other, bf16[64,48,1280]{2,1,0:T(8,128)(2,1)} %bitcast.8, ...), custom_call_target="tpu_custom_call" | custom-call | tf_op jit(solution)/shard_map/channel_mixer/pallas_call | solution.py:466
  118.1 3.0 %collective-permute-start.4 = (bf16[4,256,256]{2,1,0:T(8,128)(2,1)S(1)}, bf16[4,256,256]{2,1,0:T(8,128)(2,1)S(1)}, u32[]{:S(2)}, u32[]{:S(2)}) collective-permute-start(bf16[4,256,256]{2,1,0:T(8,128)(2,1)S(1)} %get-tuple-element.38), channel_id=1, source_target_pairs={{0,1},{1,0},{2,3},{3,2},{4,5},{5,4},{6,7},{7,6},{8,9},{9,8},{10,11... | collective-permute-start | bytes 1572872 | tf_op jit(solution)/shard_map/ppermute | solution.py:354
  121.1 1.5 %collective-permute-done.4 = bf16[4,256,256]{2,1,0:T(8,128)(2,1)S(1)} collective-permute-done((bf16[4,256,256]{2,1,0:T(8,128)(2,1)S(1)}, bf16[4,256,256]{2,1,0:T(8,128)(2,1)S(1)}, u32[]{:S(2)}, u32[]{:S(2)}) %collective-permute-start.4) | collective-permute-done | bytes 524320 | tf_op jit(solution)/shard_map/ppermute | solution.py:354
  122.6 0.1 add_convert_fusion.1
  122.7 12.4 %all_to_all.32.got = bf16[4,256,256]{2,1,0:T(8,128)(2,1)S(1)} all-to-all(bf16[4,256,256]{2,1,0:T(8,128)(2,1)S(1)} %add_convert_fusion.1), channel_id=1, replica_groups=mesh['sp_0'=8,'sp_1'=8,'x'=4,'core'=2] {'x'}, dimensions={0} | all-to-all | bytes 1048576 | tf_op jit(solution)/shard_map/all_to_all | solution.py:345
  135.2 0.7 finish.1
  (15 shorter events, 0.1 us)
Async XLA Ops:
  6.5 106.5 %all-gather.3.cloned.1.call-start = ((), (), s32[]{:S(2)}) async-start(), calls=%async_computation.6 | async-start | bytes 7987200 | tf_op jit(solution)/shard_map/all_gather | solution.py:396
  8.0 48.6 %copy-start.11 = (f32[8]{0:T(128)S(1)}, f32[8]{0:T(128)}, u32[]{:S(2)}) copy-start(f32[8]{0:T(128)} %param.22) | copy-start | bytes 100
  8.1 5.1 %collective-permute-start = (bf16[8,896]{1,0:T(8,128)(2,1)}, bf16[8,896]{1,0:T(8,128)(2,1)S(1)}, u32[]{:S(2)}, u32[]{:S(2)}) collective-permute-start(bf16[8,896]{1,0:T(8,128)(2,1)} %get-tuple-element.22), channel_id=1, source_target_pairs={{0,8},{8,16},{16,24},{24,32},{32,40},{40,48},{48,56},{56,64},{64,7... | collective-permute-start | bytes 43016 | tf_op jit(solution)/shard_map/ppermute | solution.py:350
  13.1 0.6 copy-start.9
  13.7 50.7 %copy-start.8 = (f32[512]{0:T(512)S(1)}, f32[512]{0:T(512)}, u32[]{:S(2)}) copy-start(f32[512]{0:T(512)} %param.25) | copy-start | bytes 6148
  16.7 40.0 %copy-start.1 = (bf16[256,384]{1,0:T(8,128)(2,1)S(1)}, bf16[256,384]{1,0:T(8,128)(2,1)}, u32[]{:S(2)}) copy-start(bf16[256,384]{1,0:T(8,128)(2,1)} %get-tuple-element.24.keys) | copy-start | bytes 589828
  16.7 47.7 %copy-start = (bf16[512,2048]{1,0:T(8,128)(2,1)S(1)}, bf16[512,2048]{1,0:T(8,128)(2,1)}, u32[]{:S(2)}) copy-start(bf16[512,2048]{1,0:T(8,128)(2,1)} %weight.1) | copy-start | bytes 6291460
  34.1 18.4 %all-to-all-start.1 = ((bf16[8,32,256]{2,1,0:T(8,128)(2,1)}), bf16[8,32,256]{2,1,0:T(8,128)(2,1)S(1)}, u32[]{:S(2)}, u32[]{:S(2)}) async-start(bf16[8,32,256]{2,1,0:T(8,128)(2,1)} %row_total.1), calls=%async_computation.1 | async-start | bytes 262144 | tf_op jit(solution)/shard_map/all_to_all | solution.py:345
  53.2 11.2 %all-to-all-start.2 = ((bf16[8,32,256]{2,1,0:T(8,128)(2,1)}), bf16[8,32,256]{2,1,0:T(8,128)(2,1)S(1)}, u32[]{:S(2)}, u32[]{:S(2)}) async-start(bf16[8,32,256]{2,1,0:T(8,128)(2,1)} %prefix.1), calls=%async_computation.2 | async-start | bytes 262144 | tf_op jit(solution)/shard_map/all_to_all | solution.py:345
  56.8 1.0 copy-start.2
  57.7 0.9 copy-start.3
  58.7 0.9 copy-start.5
  59.6 0.7 copy-start.6
  60.3 0.7 copy-start.7
  65.3 9.6 %collective-permute-start.1 = (bf16[4,272,256]{2,1,0:T(8,128)(2,1)S(1)}, bf16[4,272,256]{2,1,0:T(8,128)(2,1)S(1)}, u32[]{:S(2)}, u32[]{:S(2)}) collective-permute-start(bf16[4,272,256]{2,1,0:T(8,128)(2,1)S(1)} %get-tuple-element.32), channel_id=1, source_target_pairs={{0,1},{1,0},{2,3},{3,2},{4,5},{5,4},{6,7},{7,6},{8,9},{9,8},{10,11... | collective-permute-start | bytes 1671176 | tf_op jit(solution)/shard_map/ppermute | solution.py:354
  74.9 14.5 %copy-start.4 = (bf16[256,256]{1,0:T(8,128)(2,1)S(1)}, bf16[256,256]{1,0:T(8,128)(2,1)}, u32[]{:S(2)}) copy-start(bf16[256,256]{1,0:T(8,128)(2,1)} %residual.1) | copy-start | bytes 393220
  75.9 13.5 %all-to-all-start.3 = ((bf16[4,272,256]{2,1,0:T(8,128)(2,1)}), bf16[4,272,256]{2,1,0:T(8,128)(2,1)S(1)}, u32[]{:S(2)}, u32[]{:S(2)}) async-start(bf16[4,272,256]{2,1,0:T(8,128)(2,1)} %add_convert_fusion), calls=%async_computation.3 | async-start | bytes 1114112 | tf_op jit(solution)/shard_map/all_to_all | solution.py:345
  89.8 18.1 %copy-start.10 = (bf16[2,3,640]{2,0,1:T(2,128)(2,1)S(1)}, bf16[2,3,640]{2,0,1:T(2,128)(2,1)}, u32[]{:S(2)}) copy-start(bf16[2,3,640]{2,0,1:T(2,128)(2,1)} %param.30) | copy-start | bytes 23044
  89.8 2.9 %collective-permute-start.2 = (bf16[8,256]{1,0:T(8,128)(2,1)S(1)}, bf16[8,256]{1,0:T(8,128)(2,1)S(1)}, u32[]{:S(2)}, u32[]{:S(2)}) collective-permute-start(bf16[8,256]{1,0:T(8,128)(2,1)S(1)} %get-tuple-element.35), channel_id=1, source_target_pairs={{0,8},{8,16},{16,24},{24,32},{32,40},{40,48},{48,56},{56,64},{64,7... | collective-permute-start | bytes 12296 | tf_op jit(solution)/shard_map/ppermute | solution.py:350
  102.5 6.9 %collective-permute-start.3 = (bf16[4,272,256]{2,1,0:T(8,128)(2,1)S(1)}, bf16[4,272,256]{2,1,0:T(8,128)(2,1)S(1)}, u32[]{:S(2)}, u32[]{:S(2)}) collective-permute-start(bf16[4,272,256]{2,1,0:T(8,128)(2,1)S(1)} %all_to_all.31.own), channel_id=1, source_target_pairs={{0,1},{1,0},{2,3},{3,2},{4,5},{5,4},{6,7},{7,6},{8,9},{9,8},{10,11... | collective-permute-start | bytes 1671176 | tf_op jit(solution)/shard_map/ppermute | solution.py:354
  118.1 4.5 %collective-permute-start.4 = (bf16[4,256,256]{2,1,0:T(8,128)(2,1)S(1)}, bf16[4,256,256]{2,1,0:T(8,128)(2,1)S(1)}, u32[]{:S(2)}, u32[]{:S(2)}) collective-permute-start(bf16[4,256,256]{2,1,0:T(8,128)(2,1)S(1)} %get-tuple-element.38), channel_id=1, source_target_pairs={{0,1},{1,0},{2,3},{3,2},{4,5},{5,4},{6,7},{7,6},{8,9},{9,8},{10,11... | collective-permute-start | bytes 1572872 | tf_op jit(solution)/shard_map/ppermute | solution.py:354
Sparse Core Ops, SparseCore 0:
  10.3 102.6 all-gather.2

commit v4 on v3

--- a/solution.py
+++ b/solution.py
@@ -278,7 +278,11 @@
             )
     for copy in copies:
         copy.start()
-    mine = core[0]
+    mine, chip = core[0], core[1]
+    odd = chip % 2
+    near = chip + 1 - 2 * odd
+    back = (chip + 2 * odd + 3) % 4
+    across = (chip + 2) % 4
     marks = jnp.zeros((16, share), F32)
     for c in range(chips):
         first, second = own[c], other[c]
@@ -325,8 +329,10 @@
         copy.wait()
     step = share // each
     for target, side in ((give, 1 - mine), (keep, mine)):
-        for c in range(chips):
-            block = down[pl.ds((2 * c + side) * step, step)]
+        first = jnp.where(side == 0, near, back)
+        second = near + back - first
+        for c, block in enumerate((chip, second, first, across)):
+            block = down[pl.ds((2 * block + side) * step, step)]
             block = jnp.concatenate([block[:, :, :units], block[:, :, units:]], axis=1)
             part = lax.dot_general(
                 block.reshape(share, units), hidden[...], LAST, preferred_element_type=F32
@@ -334,11 +340,29 @@
             target[c] = part.astype(BF16)
 
 
-def finish_kernel(merged, got, out):
-    total = merged[...].astype(F32)
-    for c in range(got.shape[0]):
-        total = total + got[c].astype(F32)
+def finish_kernel(merged, kept, swapped_in, first_in, second_in, out):
+    total = merged[...].astype(F32) + kept[0].astype(F32) + swapped_in[0].astype(F32)
+    total = total + first_in[0].astype(F32) + second_in[...].astype(F32)
     out[...] = total.astype(BF16)
+
+
+def halved(kept, given, merged):
+    near = [(0, 1), (1, 0), (2, 3), (3, 2)]
+    back = [(0, 3), (3, 0), (1, 2), (2, 1)]
+    rounds = [
+        [(2 * a, 2 * b) for a, b in even] + [(2 * a + 1, 2 * b + 1) for a, b in odd]
+        for even, odd in ((near, back), (back, near))
+    ]
+    tp = ("x", "core")
+    got = swapped(given)
+    sent = (kept[2:].astype(F32) + got[2:].astype(F32)).astype(BF16)
+    first = lax.ppermute(sent, tp, rounds[0])
+    sent = kept[1].astype(F32) + got[1].astype(F32) + first[1].astype(F32)
+    second = lax.ppermute(sent.astype(BF16), tp, rounds[1])
+    (out,) = call(finish_kernel, [(merged.shape, BF16)], name="finish")(
+        merged, kept, got, first, second
+    )
+    return out
 
 
 def exchange(parts, axis):
@@ -400,7 +424,7 @@
     features = residual.shape[0]
     units = hidden_gate.shape[1]
     before = from_behind(tail, SP)
-    core = lax.axis_index("core").astype(jnp.int32).reshape(1)
+    core = jnp.stack([lax.axis_index("core"), lax.axis_index("x")]).astype(jnp.int32)
     span = STATE_WIDE // n_row + STATE_NARROW // n_row + 8
     x, keys, run, delta, run_col, pay = call(
         state_kernel,
@@ -481,9 +505,7 @@
     )(
         core, own_core, other_core, pltpu.with_memory_space_constraint(weights, pltpu.HBM), hidden_conv
     )
-    got = pair_then_chips(kept, given)
-    (out,) = call(finish_kernel, [((features, rows), BF16)], name="finish")(merged, got)
-    return out
+    return halved(kept, given, merged)
 
 
 def solution(mesh):

time: 144 us -> 147 us (1.021)
  blocking collectives: 38.7 us -> 26.3 us
  waiting for transfers between devices: 28.7 us -> 37.1 us
  starting transfers between devices: 40.8 us -> 47.3 us
    all_to_all x3 -> x2, blocking collectives: 38.7 us -> 26.3 us  [exchange(): return lax.all_to_all(parts, axis, split_axis=0, concat_axis=0, tiled=True)]
    ppermute x0 -> x2, waiting for transfers between devices: none -> 7.52 us  [the longest x1 4 us: halved(): first = lax.ppermute(sent, tp, rounds[0])]
    ppermute x0 -> x2, starting transfers between devices: none -> 6.5 us  [the longest x1 4.32 us: halved(): first = lax.ppermute(sent, tp, rounds[0])]
  transfers between devices with their start and end apart: 9 -> 11, of which waited for: 9 -> 11; matrix products, arithmetic and copies ran while one was open for 1% -> 1% of each run, Pallas kernels for 5% -> 5%
where the time goes in v4:
time: 147 us; the launch traced here: 145 us
  starting transfers between devices  47.3 us (32%)
  waiting for transfers between devices  37.1 us (25%)
  blocking collectives  26.3 us (18%)
  Pallas kernels  15.1 us (10%)
  between operations  13.6 us (9%)
  local copies, waits for them, and re-layouts  4.39 us (3%)
    all_to_all x2, blocking collectives, exchange(): return lax.all_to_all(parts, axis, split_axis=0, concat_axis=0, tiled=True)  26.3 us
    all_to_all x3, waiting for transfers between devices, exchange(): return lax.all_to_all(parts, axis, split_axis=0, concat_axis=0, tiled=True)  20 us
    all_to_all x3, starting transfers between devices, exchange(): return lax.all_to_all(parts, axis, split_axis=0, concat_axis=0, tiled=True)  18 us
    ppermute x3, starting transfers between devices, swapped(): return lax.ppermute(value, 'core', [(0, 1), (1, 0)])  16.6 us
    ppermute x2, starting transfers between devices, from_behind(): lax.ppermute(value, axis, [(source, source + 1) for source in range(count...  6.21 us
    pallas_call x1, Pallas kernels, local(): call(functools.partial(channel_kernel, features * n_tp), [((chips, featur...  5.55 us
    ppermute x3, waiting for transfers between devices, swapped(): return lax.ppermute(value, 'core', [(0, 1), (1, 0)])  4.61 us
    ppermute x1, starting transfers between devices, halved(): first = lax.ppermute(sent, tp, rounds[0])  4.32 us
  transfers between devices with their start and end apart: 11, of which 11 were waited for; matrix products, arithmetic and copies ran while one was open for 1% of the time, Pallas kernels for 5%

profile of v4, /device:TPU:1, one launch (start us, length us, event | category | flops | bytes accessed | tf_op | source)
XLA Modules:
  0.0 145.0 jit_solution(15587143107066734395)
XLA Ops:
  6.5 1.5 %pack.1 = (bf16[48,1280]{1,0:T(8,128)(2,1)}, bf16[8,896]{1,0:T(8,128)(2,1)}) custom-call(bf16[32,640]{1,0:T(8,128)(2,1)} %gate.2, bf16[32,640]{1,0:T(8,128)(2,1)} %up.1, bf16[32,640]{1,0:T(8,128)(2,1)} %bitcast.12, bf16[256,512]{1,0:T(8,128)(2,1)} %values.3, bf16[256,384]{1,0:T(8,128)(2,1)} %keys.3), custom_call_target="tpu_custom_call" | custom-call | tf_op jit(solution)/shard_map/pack/pallas_call | solution.py:408
  8.0 0.0 all-gather.3.cloned.1.call-update
  8.1 4.0 %collective-permute-start = (bf16[8,896]{1,0:T(8,128)(2,1)}, bf16[8,896]{1,0:T(8,128)(2,1)S(1)}, u32[]{:S(2)}, u32[]{:S(2)}) collective-permute-start(bf16[8,896]{1,0:T(8,128)(2,1)} %get-tuple-element.22), channel_id=1, source_target_pairs={{0,8},{8,16},{16,24},{24,32},{32,40},{40,48},{48,56},{56,64},{64,7... | collective-permute-start | bytes 43016 | tf_op jit(solution)/shard_map/ppermute | solution.py:374
  12.1 1.0 collective-permute-done.before
  13.1 0.6 copy-done.9
  13.7 3.0 %span_state.1 = (bf16[256,512]{1,0:T(8,128)(2,1)}, bf16[256,384]{1,0:T(8,128)(2,1)}, f32[8,256]{1,0:T(8,128)}, f32[8,256]{1,0:T(8,128)}, f32[256,8]{1,0:T(8,128)}, /*index=5*/bf16[8,32,256]{2,1,0:T(8,128)(2,1)}) custom-call(bf16[256,512]{1,0:T(8,128)(2,1)} %values.3, bf16[256,384]{1,0:T(8,128)(2,1)} %keys.3, bf16[8,896]{1,0:T(8,128)(2,1)} %copy-done.9, ...), custom_call_target="tpu_custom_call" | custom-call | tf_op jit(solution)/shard_map/span_state/pallas_call | solution.py:429
  16.8 0.0 copy-start.8
  16.8 16.6 %all_to_all.25.got = bf16[8,32,256]{2,1,0:T(8,128)(2,1)S(1)} all-to-all(bf16[8,32,256]{2,1,0:T(8,128)(2,1)} %get-tuple-element.30), channel_id=1, replica_groups=mesh['sp_0'=8,'sp_1'=8,'x'=4,'core'=2] {'sp_1'}, dimensions={0} | all-to-all | bytes 262144 | tf_op jit(solution)/shard_map/all_to_all | solution.py:369
  33.4 0.7 row_total.1
  34.1 10.7 %all-to-all-start.1 = ((bf16[8,32,256]{2,1,0:T(8,128)(2,1)}), bf16[8,32,256]{2,1,0:T(8,128)(2,1)S(1)}, u32[]{:S(2)}, u32[]{:S(2)}) async-start(bf16[8,32,256]{2,1,0:T(8,128)(2,1)} %row_total.1), calls=%async_computation.1 | async-start | bytes 262144 | tf_op jit(solution)/shard_map/all_to_all | solution.py:369
  44.8 7.8 %all-to-all-done.1.totals = bf16[8,32,256]{2,1,0:T(8,128)(2,1)S(1)} async-done(((bf16[8,32,256]{2,1,0:T(8,128)(2,1)}), bf16[8,32,256]{2,1,0:T(8,128)(2,1)S(1)}, u32[]{:S(2)}, u32[]{:S(2)}) %all-to-all-start.1) | async-done | bytes 131104 | tf_op jit(solution)/shard_map/all_to_all | solution.py:369
  52.6 0.7 prefix.1
  53.3 3.4 %all-to-all-start.2 = ((bf16[8,32,256]{2,1,0:T(8,128)(2,1)}), bf16[8,32,256]{2,1,0:T(8,128)(2,1)S(1)}, u32[]{:S(2)}, u32[]{:S(2)}) async-start(bf16[8,32,256]{2,1,0:T(8,128)(2,1)} %prefix.1), calls=%async_computation.2 | async-start | bytes 262144 | tf_op jit(solution)/shard_map/all_to_all | solution.py:369
  56.7 0.0 copy-done.11
  56.7 0.1 broadcast_in_dim.6
  56.8 0.1 reshape_reshape.3.skip
  56.8 0.1 pad_add_fusion.core
  56.9 0.9 copy-done.2
  57.9 0.9 copy-done.3
  58.8 0.9 copy-done.5
  59.7 1.1 inside_span.1
  60.8 3.7 %all-to-all-done.2.got = bf16[8,32,256]{2,1,0:T(8,128)(2,1)S(1)} async-done(((bf16[8,32,256]{2,1,0:T(8,128)(2,1)}), bf16[8,32,256]{2,1,0:T(8,128)(2,1)S(1)}, u32[]{:S(2)}, u32[]{:S(2)}) %all-to-all-start.2) | async-done | bytes 131104 | tf_op jit(solution)/shard_map/all_to_all | solution.py:369
  64.5 0.0 copy-done
  64.5 1.4 apply_project.1
  65.9 8.2 %collective-permute-start.1 = (bf16[4,272,256]{2,1,0:T(8,128)(2,1)S(1)}, bf16[4,272,256]{2,1,0:T(8,128)(2,1)S(1)}, u32[]{:S(2)}, u32[]{:S(2)}) collective-permute-start(bf16[4,272,256]{2,1,0:T(8,128)(2,1)S(1)} %get-tuple-element.32), channel_id=1, source_target_pairs={{0,1},{1,0},{2,3},{3,2},{4,5},{5,4},{6,7},{7,6},{8,9},{9,8},{10,11... | collective-permute-start | bytes 1671176 | tf_op jit(solution)/shard_map/ppermute | solution.py:378
  74.1 1.6 %collective-permute-done.1 = bf16[4,272,256]{2,1,0:T(8,128)(2,1)S(1)} collective-permute-done((bf16[4,272,256]{2,1,0:T(8,128)(2,1)S(1)}, bf16[4,272,256]{2,1,0:T(8,128)(2,1)S(1)}, u32[]{:S(2)}, u32[]{:S(2)}) %collective-permute-start.1) | collective-permute-done | bytes 557088 | tf_op jit(solution)/shard_map/ppermute | solution.py:378
  75.7 1.0 add_convert_fusion
  76.7 3.9 %all-to-all-start.3 = ((bf16[4,272,256]{2,1,0:T(8,128)(2,1)}), bf16[4,272,256]{2,1,0:T(8,128)(2,1)S(1)}, u32[]{:S(2)}, u32[]{:S(2)}) async-start(bf16[4,272,256]{2,1,0:T(8,128)(2,1)} %add_convert_fusion), calls=%async_computation.3 | async-start | bytes 1114112 | tf_op jit(solution)/shard_map/all_to_all | solution.py:369
  80.6 0.8 dynamic_slice.3
  81.4 8.5 %all-to-all-done.3.got = bf16[4,272,256]{2,1,0:T(8,128)(2,1)S(1)} async-done(((bf16[4,272,256]{2,1,0:T(8,128)(2,1)}), bf16[4,272,256]{2,1,0:T(8,128)(2,1)S(1)}, u32[]{:S(2)}, u32[]{:S(2)}) %all-to-all-start.3) | async-done | bytes 557088 | tf_op jit(solution)/shard_map/all_to_all | solution.py:369
  89.9 0.4 merge.1
  90.3 0.0 copy-start.10
  90.3 2.2 %collective-permute-start.2 = (bf16[8,256]{1,0:T(8,128)(2,1)S(1)}, bf16[8,256]{1,0:T(8,128)(2,1)S(1)}, u32[]{:S(2)}, u32[]{:S(2)}) collective-permute-start(bf16[8,256]{1,0:T(8,128)(2,1)S(1)} %get-tuple-element.35), channel_id=1, source_target_pairs={{0,8},{8,16},{16,24},{24,32},{32,40},{40,48},{48,56},{56,64},{64,7... | collective-permute-start | bytes 12296 | tf_op jit(solution)/shard_map/ppermute | solution.py:374
  92.5 0.7 collective-permute-done.2
  93.3 9.7 %all_to_all.26.own = bf16[4,272,256]{2,1,0:T(8,128)(2,1)S(1)} all-to-all(bf16[4,272,256]{2,1,0:T(8,128)(2,1)S(1)} %broadcast_in_dim.7), channel_id=1, replica_groups=mesh['sp_0'=8,'sp_1'=8,'x'=4,'core'=2] {'x'}, dimensions={0} | all-to-all | bytes 1114112 | tf_op jit(solution)/shard_map/all_to_all | solution.py:369
  103.0 5.4 %collective-permute-start.3 = (bf16[4,272,256]{2,1,0:T(8,128)(2,1)S(1)}, bf16[4,272,256]{2,1,0:T(8,128)(2,1)S(1)}, u32[]{:S(2)}, u32[]{:S(2)}) collective-permute-start(bf16[4,272,256]{2,1,0:T(8,128)(2,1)S(1)} %all_to_all.26.own), channel_id=1, source_target_pairs={{0,1},{1,0},{2,3},{3,2},{4,5},{5,4},{6,7},{7,6},{8,9},{9,8},{10,11... | collective-permute-start | bytes 1671176 | tf_op jit(solution)/shard_map/ppermute | solution.py:378
  108.4 1.5 %collective-permute-done.3.other = bf16[4,272,256]{2,1,0:T(8,128)(2,1)S(1)} collective-permute-done((bf16[4,272,256]{2,1,0:T(8,128)(2,1)S(1)}, bf16[4,272,256]{2,1,0:T(8,128)(2,1)S(1)}, u32[]{:S(2)}, u32[]{:S(2)}) %collective-permute-start.3) | collective-permute-done | bytes 557088 | tf_op jit(solution)/shard_map/ppermute | solution.py:378
  109.9 3.2 %all-gather.3.cloned.1.call-done = bf16[3072,1280]{1,0:T(8,128)(2,1)} async-done(((bf16[48,1280]{1,0:T(8,128)(2,1)}), bf16[3072,1280]{1,0:T(8,128)(2,1)}) %all-gather.3.cloned.1.call-update) | async-done | bytes 7864336 | tf_op jit(solution)/shard_map/all_gather | solution.py:420
  113.1 5.5 %channel_mixer.1 = (bf16[4,256,256]{2,1,0:T(8,128)(2,1)S(1)}, bf16[4,256,256]{2,1,0:T(8,128)(2,1)S(1)}) custom-call(s32[2]{0:T(128)S(1)} %pad_add_fusion.core, bf16[4,272,256]{2,1,0:T(8,128)(2,1)S(1)} %all_to_all.26.own, bf16[4,272,256]{2,1,0:T(8,128)(2,1)S(1)} %collective-permute-done.3.other, bf16[64,48,1280]{2,1,0:T(8,128)(2,1)} %bitcast.11, ...), custom_call_target="tpu_custom_call" | custom-call | tf_op jit(solution)/shard_map/channel_mixer/pallas_call | solution.py:490
  118.7 3.0 %collective-permute-start.4 = (bf16[4,256,256]{2,1,0:T(8,128)(2,1)S(1)}, bf16[4,256,256]{2,1,0:T(8,128)(2,1)S(1)}, u32[]{:S(2)}, u32[]{:S(2)}) collective-permute-start(bf16[4,256,256]{2,1,0:T(8,128)(2,1)S(1)} %get-tuple-element.38), channel_id=1, source_target_pairs={{0,1},{1,0},{2,3},{3,2},{4,5},{5,4},{6,7},{7,6},{8,9},{9,8},{10,11... | collective-permute-start | bytes 1572872 | tf_op jit(solution)/shard_map/ppermute | solution.py:378
  121.7 1.5 %collective-permute-done.4.swapped_in = bf16[4,256,256]{2,1,0:T(8,128)(2,1)S(1)} collective-permute-done((bf16[4,256,256]{2,1,0:T(8,128)(2,1)S(1)}, bf16[4,256,256]{2,1,0:T(8,128)(2,1)S(1)}, u32[]{:S(2)}, u32[]{:S(2)}) %collective-permute-start.4) | collective-permute-done | bytes 524320 | tf_op jit(solution)/shard_map/ppermute | solution.py:378
  123.2 0.1 add_convert_fusion.1
  123.3 4.3 %collective-permute-start.5 = (bf16[2,256,256]{2,1,0:T(8,128)(2,1)S(1)}, bf16[2,256,256]{2,1,0:T(8,128)(2,1)S(1)}, u32[]{:S(2)}, u32[]{:S(2)}) collective-permute-start(bf16[2,256,256]{2,1,0:T(8,128)(2,1)S(1)} %add_convert_fusion.1), channel_id=1, source_target_pairs={{0,2},{2,0},{4,6},{6,4},{1,7},{7,1},{3,5},{5,3},{8,10},{10,8},{12,... | collective-permute-start | bytes 786440 | tf_op jit(solution)/shard_map/ppermute | solution.py:359
  127.6 4.0 %collective-permute-done.5.first_in = bf16[2,256,256]{2,1,0:T(8,128)(2,1)S(1)} collective-permute-done((bf16[2,256,256]{2,1,0:T(8,128)(2,1)S(1)}, bf16[2,256,256]{2,1,0:T(8,128)(2,1)S(1)}, u32[]{:S(2)}, u32[]{:S(2)}) %collective-permute-start.5) | collective-permute-done | bytes 262176 | tf_op jit(solution)/shard_map/ppermute | solution.py:359
  131.6 0.1 fusion
  131.7 2.2 %collective-permute-start.6 = (bf16[256,256]{1,0:T(8,128)(2,1)S(1)}, bf16[256,256]{1,0:T(8,128)(2,1)S(1)}, u32[]{:S(2)}, u32[]{:S(2)}) collective-permute-start(bf16[256,256]{1,0:T(8,128)(2,1)S(1)} %fusion), channel_id=1, source_target_pairs={{0,6},{6,0},{2,4},{4,2},{1,3},{3,1},{5,7},{7,5},{8,14},{14,8},{10,... | collective-permute-start | bytes 393224 | tf_op jit(solution)/shard_map/ppermute | solution.py:361
  133.9 3.5 %collective-permute-done.6.second_in = bf16[256,256]{1,0:T(8,128)(2,1)S(1)} collective-permute-done((bf16[256,256]{1,0:T(8,128)(2,1)S(1)}, bf16[256,256]{1,0:T(8,128)(2,1)S(1)}, u32[]{:S(2)}, u32[]{:S(2)}) %collective-permute-start.6) | collective-permute-done | bytes 131104 | tf_op jit(solution)/shard_map/ppermute | solution.py:361
  137.4 0.7 finish.1
  (20 shorter events, 0.1 us)
Async XLA Ops:
  6.5 106.6 %all-gather.3.cloned.1.call-start = ((), (), s32[]{:S(2)}) async-start(), calls=%async_computation.5 | async-start | bytes 7987200 | tf_op jit(solution)/shard_map/all_gather | solution.py:420
  8.0 48.6 %copy-start.11 = (f32[8]{0:T(128)S(1)}, f32[8]{0:T(128)}, u32[]{:S(2)}) copy-start(f32[8]{0:T(128)} %param.22) | copy-start | bytes 100
  8.1 5.1 %collective-permute-start = (bf16[8,896]{1,0:T(8,128)(2,1)}, bf16[8,896]{1,0:T(8,128)(2,1)S(1)}, u32[]{:S(2)}, u32[]{:S(2)}) collective-permute-start(bf16[8,896]{1,0:T(8,128)(2,1)} %get-tuple-element.22), channel_id=1, source_target_pairs={{0,8},{8,16},{16,24},{24,32},{32,40},{40,48},{48,56},{56,64},{64,7... | collective-permute-start | bytes 43016 | tf_op jit(solution)/shard_map/ppermute | solution.py:374
  13.1 0.6 copy-start.9
  16.8 40.2 %copy-start.1 = (bf16[256,384]{1,0:T(8,128)(2,1)S(1)}, bf16[256,384]{1,0:T(8,128)(2,1)}, u32[]{:S(2)}) copy-start(bf16[256,384]{1,0:T(8,128)(2,1)} %get-tuple-element.24.keys) | copy-start | bytes 589828
  16.8 40.2 %copy-start.6 = (f32[8,256]{1,0:T(8,128)S(1)}, f32[8,256]{1,0:T(8,128)}, u32[]{:S(2)}) copy-start(f32[8,256]{1,0:T(8,128)} %get-tuple-element.25.run) | copy-start | bytes 24580
  16.8 40.2 %copy-start.7 = (f32[8,256]{1,0:T(8,128)S(1)}, f32[8,256]{1,0:T(8,128)}, u32[]{:S(2)}) copy-start(f32[8,256]{1,0:T(8,128)} %get-tuple-element.26.delta) | copy-start | bytes 24580
  16.8 47.7 %copy-start.8 = (f32[512]{0:T(512)S(1)}, f32[512]{0:T(512)}, u32[]{:S(2)}) copy-start(f32[512]{0:T(512)} %param.25) | copy-start | bytes 6148
  33.4 31.1 %copy-start = (bf16[512,2048]{1,0:T(8,128)(2,1)S(1)}, bf16[512,2048]{1,0:T(8,128)(2,1)}, u32[]{:S(2)}) copy-start(bf16[512,2048]{1,0:T(8,128)(2,1)} %weight.1) | copy-start | bytes 6291460
  34.1 18.4 %all-to-all-start.1 = ((bf16[8,32,256]{2,1,0:T(8,128)(2,1)}), bf16[8,32,256]{2,1,0:T(8,128)(2,1)S(1)}, u32[]{:S(2)}, u32[]{:S(2)}) async-start(bf16[8,32,256]{2,1,0:T(8,128)(2,1)} %row_total.1), calls=%async_computation.1 | async-start | bytes 262144 | tf_op jit(solution)/shard_map/all_to_all | solution.py:369
  53.3 11.2 %all-to-all-start.2 = ((bf16[8,32,256]{2,1,0:T(8,128)(2,1)}), bf16[8,32,256]{2,1,0:T(8,128)(2,1)S(1)}, u32[]{:S(2)}, u32[]{:S(2)}) async-start(bf16[8,32,256]{2,1,0:T(8,128)(2,1)} %prefix.1), calls=%async_computation.2 | async-start | bytes 262144 | tf_op jit(solution)/shard_map/all_to_all | solution.py:369
  56.9 1.0 copy-start.2
  57.9 0.9 copy-start.3
  58.8 0.9 copy-start.5
  65.9 9.8 %collective-permute-start.1 = (bf16[4,272,256]{2,1,0:T(8,128)(2,1)S(1)}, bf16[4,272,256]{2,1,0:T(8,128)(2,1)S(1)}, u32[]{:S(2)}, u32[]{:S(2)}) collective-permute-start(bf16[4,272,256]{2,1,0:T(8,128)(2,1)S(1)} %get-tuple-element.32), channel_id=1, source_target_pairs={{0,1},{1,0},{2,3},{3,2},{4,5},{5,4},{6,7},{7,6},{8,9},{9,8},{10,11... | collective-permute-start | bytes 1671176 | tf_op jit(solution)/shard_map/ppermute | solution.py:378
  75.7 14.2 %copy-start.4 = (bf16[256,256]{1,0:T(8,128)(2,1)S(1)}, bf16[256,256]{1,0:T(8,128)(2,1)}, u32[]{:S(2)}) copy-start(bf16[256,256]{1,0:T(8,128)(2,1)} %residual.1) | copy-start | bytes 393220
  76.7 13.2 %all-to-all-start.3 = ((bf16[4,272,256]{2,1,0:T(8,128)(2,1)}), bf16[4,272,256]{2,1,0:T(8,128)(2,1)S(1)}, u32[]{:S(2)}, u32[]{:S(2)}) async-start(bf16[4,272,256]{2,1,0:T(8,128)(2,1)} %add_convert_fusion), calls=%async_computation.3 | async-start | bytes 1114112 | tf_op jit(solution)/shard_map/all_to_all | solution.py:369
  90.3 18.1 %copy-start.10 = (bf16[2,3,640]{2,0,1:T(2,128)(2,1)S(1)}, bf16[2,3,640]{2,0,1:T(2,128)(2,1)}, u32[]{:S(2)}) copy-start(bf16[2,3,640]{2,0,1:T(2,128)(2,1)} %param.30) | copy-start | bytes 23044
  90.3 2.9 %collective-permute-start.2 = (bf16[8,256]{1,0:T(8,128)(2,1)S(1)}, bf16[8,256]{1,0:T(8,128)(2,1)S(1)}, u32[]{:S(2)}, u32[]{:S(2)}) collective-permute-start(bf16[8,256]{1,0:T(8,128)(2,1)S(1)} %get-tuple-element.35), channel_id=1, source_target_pairs={{0,8},{8,16},{16,24},{24,32},{32,40},{40,48},{48,56},{56,64},{64,7... | collective-permute-start | bytes 12296 | tf_op jit(solution)/shard_map/ppermute | solution.py:374
  103.0 6.9 %collective-permute-start.3 = (bf16[4,272,256]{2,1,0:T(8,128)(2,1)S(1)}, bf16[4,272,256]{2,1,0:T(8,128)(2,1)S(1)}, u32[]{:S(2)}, u32[]{:S(2)}) collective-permute-start(bf16[4,272,256]{2,1,0:T(8,128)(2,1)S(1)} %all_to_all.26.own), channel_id=1, source_target_pairs={{0,1},{1,0},{2,3},{3,2},{4,5},{5,4},{6,7},{7,6},{8,9},{9,8},{10,11... | collective-permute-start | bytes 1671176 | tf_op jit(solution)/shard_map/ppermute | solution.py:378
  118.7 4.6 %collective-permute-start.4 = (bf16[4,256,256]{2,1,0:T(8,128)(2,1)S(1)}, bf16[4,256,256]{2,1,0:T(8,128)(2,1)S(1)}, u32[]{:S(2)}, u32[]{:S(2)}) collective-permute-start(bf16[4,256,256]{2,1,0:T(8,128)(2,1)S(1)} %get-tuple-element.38), channel_id=1, source_target_pairs={{0,1},{1,0},{2,3},{3,2},{4,5},{5,4},{6,7},{7,6},{8,9},{9,8},{10,11... | collective-permute-start | bytes 1572872 | tf_op jit(solution)/shard_map/ppermute | solution.py:378
  123.3 8.3 %collective-permute-start.5 = (bf16[2,256,256]{2,1,0:T(8,128)(2,1)S(1)}, bf16[2,256,256]{2,1,0:T(8,128)(2,1)S(1)}, u32[]{:S(2)}, u32[]{:S(2)}) collective-permute-start(bf16[2,256,256]{2,1,0:T(8,128)(2,1)S(1)} %add_convert_fusion.1), channel_id=1, source_target_pairs={{0,2},{2,0},{4,6},{6,4},{1,7},{7,1},{3,5},{5,3},{8,10},{10,8},{12,... | collective-permute-start | bytes 786440 | tf_op jit(solution)/shard_map/ppermute | solution.py:359
  131.7 5.7 %collective-permute-start.6 = (bf16[256,256]{1,0:T(8,128)(2,1)S(1)}, bf16[256,256]{1,0:T(8,128)(2,1)S(1)}, u32[]{:S(2)}, u32[]{:S(2)}) collective-permute-start(bf16[256,256]{1,0:T(8,128)(2,1)S(1)} %fusion), channel_id=1, source_target_pairs={{0,6},{6,0},{2,4},{4,2},{1,3},{3,1},{5,7},{7,5},{8,14},{14,8},{10,... | collective-permute-start | bytes 393224 | tf_op jit(solution)/shard_map/ppermute | solution.py:361
Sparse Core Ops, SparseCore 0:
  10.3 102.7 all-gather.2

commit v5 on v3

--- a/solution.py
+++ b/solution.py
@@ -257,8 +257,25 @@
     tile_out[...] = jnp.concatenate(tile, axis=0).astype(BF16)
 
 
+def down_blocks(target, side, down, hidden):
+    units = hidden.shape[1]
+    share = target.shape[1]
+    step = share // (2 * down.shape[1])
+    for c in range(target.shape[0]):
+        block = down[pl.ds((2 * c + side) * step, step)]
+        block = jnp.concatenate([block[:, :, :units], block[:, :, units:]], axis=1)
+        part = lax.dot_general(
+            block.reshape(share, units), hidden[...], LAST, preferred_element_type=F32
+        )
+        target[c] = part.astype(BF16)
+
+
+def keep_kernel(core, hidden, down, keep):
+    down_blocks(keep, core[0], down, hidden)
+
+
 def channel_kernel(
-    features, core, own, other, weights, taps, keep, give, lhs, wide, down, buf, hidden, total, sems
+    features, core, own, other, weights, taps, give, hidden, down, lhs, wide, buf, total, sems
 ):
     chips, high, share = own.shape
     rows = high - 16
@@ -323,15 +340,7 @@
     hidden[...] = (silu(conv(0)) * conv(1)).astype(BF16)
     for copy in copies[quarters:]:
         copy.wait()
-    step = share // each
-    for target, side in ((give, 1 - mine), (keep, mine)):
-        for c in range(chips):
-            block = down[pl.ds((2 * c + side) * step, step)]
-            block = jnp.concatenate([block[:, :, :units], block[:, :, units:]], axis=1)
-            part = lax.dot_general(
-                block.reshape(share, units), hidden[...], LAST, preferred_element_type=F32
-            )
-            target[c] = part.astype(BF16)
+    down_blocks(give, 1 - mine, down, hidden)
 
 
 def finish_kernel(merged, got, out):
@@ -463,24 +472,34 @@
     own_core = exchange(jnp.broadcast_to(stream, (chips, *stream.shape)), "x")
     other_core = swapped(own_core)
     spans, each = weights.shape[0], hidden_gate.shape[0]
-    kept, given = call(
+    given, hidden, down = call(
         functools.partial(channel_kernel, features * n_tp),
-        [((chips, features, rows), BF16)] * 2,
+        [
+            ((chips, features, rows), BF16),
+            ((rows, units), BF16),
+            ((spans, each // 2, 2 * units), BF16),
+        ],
         [
             ((rows + 16, features * n_tp), BF16),
             ((spans, each, 2 * units), BF16),
-            ((spans, each // 2, 2 * units), BF16),
             ((rows + 8, 2 * units), F32),
-            ((rows, units), BF16),
             ((rows + 16, 2 * units), F32),
         ],
         more_scratch=[pltpu.SemaphoreType.DMA((6,))],
         grant=24,
         in_specs=[SMEM, VMEM, VMEM, pl.BlockSpec(memory_space=pltpu.HBM), VMEM],
+        out_specs=[VMEM] * 3,
         name="channel_mixer",
     )(
         core, own_core, other_core, pltpu.with_memory_space_constraint(weights, pltpu.HBM), hidden_conv
     )
+    (kept,) = call(
+        keep_kernel,
+        [((chips, features, rows), BF16)],
+        in_specs=[SMEM, VMEM, VMEM],
+        out_specs=[VMEM],
+        name="keep_blocks",
+    )(core, hidden, down)
     got = pair_then_chips(kept, given)
     (out,) = call(finish_kernel, [((features, rows), BF16)], name="finish")(merged, got)
     return out

time: 144 us -> 143 us (level)
  waiting for transfers between devices: 28.7 us -> 27.2 us
    unnamed x25 -> x27, local copies, waits for them, and re-layouts: 4.82 us -> 5.75 us
where the time goes in v5:
time: 143 us; the launch traced here: 142 us
  starting transfers between devices  40.8 us (29%)
  blocking collectives  38.7 us (27%)
  waiting for transfers between devices  27.2 us (19%)
  Pallas kernels  14.5 us (10%)
  between operations  13.5 us (9%)
  local copies, waits for them, and re-layouts  6.69 us (5%)
    all_to_all x3, blocking collectives, exchange(): return lax.all_to_all(parts, axis, split_axis=0, concat_axis=0, tiled=True)  38.7 us
    all_to_all x3, starting transfers between devices, exchange(): return lax.all_to_all(parts, axis, split_axis=0, concat_axis=0, tiled=True)  18.1 us
    all_to_all x3, waiting for transfers between devices, exchange(): return lax.all_to_all(parts, axis, split_axis=0, concat_axis=0, tiled=True)  17.9 us
    ppermute x3, starting transfers between devices, swapped(): return lax.ppermute(value, 'core', [(0, 1), (1, 0)])  16.4 us
    ppermute x2, starting transfers between devices, from_behind(): lax.ppermute(value, axis, [(source, source + 1) for source in range(count...  6.21 us
    unnamed x27, local copies, waits for them, and re-layouts  5.75 us
    pallas_call x1, Pallas kernels, local(): call(functools.partial(channel_kernel, features * n_tp), [((chips, featur...  4.67 us
    ppermute x3, waiting for transfers between devices, swapped(): return lax.ppermute(value, 'core', [(0, 1), (1, 0)])  4.01 us
  transfers between devices with their start and end apart: 9, of which 9 were waited for; matrix products, arithmetic and copies ran while one was open for 1% of the time, Pallas kernels for 5%

profile of v5, /device:TPU:1, one launch (start us, length us, event | category | flops | bytes accessed | tf_op | source)
XLA Modules:
  0.0 142.5 jit_solution(3922498949412399344)
XLA Ops:
  6.5 0.0 all-gather.3.cloned.1.call-start
  6.5 1.7 %pack.1 = (bf16[48,1280]{1,0:T(8,128)(2,1)}, bf16[8,896]{1,0:T(8,128)(2,1)}) custom-call(bf16[32,640]{1,0:T(8,128)(2,1)} %gate.2, bf16[32,640]{1,0:T(8,128)(2,1)} %up.1, bf16[32,640]{1,0:T(8,128)(2,1)} %bitcast.9, bf16[256,512]{1,0:T(8,128)(2,1)} %values.3, bf16[256,384]{1,0:T(8,128)(2,1)} %keys.3), custom_call_target="tpu_custom_call" | custom-call | tf_op jit(solution)/shard_map/pack/pallas_call | solution.py:393
  8.2 0.0 all-gather.3.cloned.1.call-update
  8.2 4.0 %collective-permute-start = (bf16[8,896]{1,0:T(8,128)(2,1)}, bf16[8,896]{1,0:T(8,128)(2,1)S(1)}, u32[]{:S(2)}, u32[]{:S(2)}) collective-permute-start(bf16[8,896]{1,0:T(8,128)(2,1)} %get-tuple-element.23), channel_id=1, source_target_pairs={{0,8},{8,16},{16,24},{24,32},{32,40},{40,48},{48,56},{56,64},{64,7... | collective-permute-start | bytes 43016 | tf_op jit(solution)/shard_map/ppermute | solution.py:359
  12.2 1.0 collective-permute-done.before
  13.3 0.6 copy-done.10
  13.9 3.0 %span_state.1 = (bf16[256,512]{1,0:T(8,128)(2,1)}, bf16[256,384]{1,0:T(8,128)(2,1)}, f32[8,256]{1,0:T(8,128)}, f32[8,256]{1,0:T(8,128)}, f32[256,8]{1,0:T(8,128)}, /*index=5*/bf16[8,32,256]{2,1,0:T(8,128)(2,1)}) custom-call(bf16[256,512]{1,0:T(8,128)(2,1)} %values.3, bf16[256,384]{1,0:T(8,128)(2,1)} %keys.3, bf16[8,896]{1,0:T(8,128)(2,1)} %copy-done.10, ...), custom_call_target="tpu_custom_call" | custom-call | tf_op jit(solution)/shard_map/span_state/pallas_call | solution.py:414
  16.9 16.6 %all_to_all.30.got = bf16[8,32,256]{2,1,0:T(8,128)(2,1)S(1)} all-to-all(bf16[8,32,256]{2,1,0:T(8,128)(2,1)} %get-tuple-element.31), channel_id=1, replica_groups=mesh['sp_0'=8,'sp_1'=8,'x'=4,'core'=2] {'sp_1'}, dimensions={0} | all-to-all | bytes 262144 | tf_op jit(solution)/shard_map/all_to_all | solution.py:354
  33.5 0.7 row_total.1
  34.3 10.6 %all-to-all-start.1 = ((bf16[8,32,256]{2,1,0:T(8,128)(2,1)}), bf16[8,32,256]{2,1,0:T(8,128)(2,1)S(1)}, u32[]{:S(2)}, u32[]{:S(2)}) async-start(bf16[8,32,256]{2,1,0:T(8,128)(2,1)} %row_total.1), calls=%async_computation.1 | async-start | bytes 262144 | tf_op jit(solution)/shard_map/all_to_all | solution.py:354
  44.9 7.9 %all-to-all-done.1.totals = bf16[8,32,256]{2,1,0:T(8,128)(2,1)S(1)} async-done(((bf16[8,32,256]{2,1,0:T(8,128)(2,1)}), bf16[8,32,256]{2,1,0:T(8,128)(2,1)S(1)}, u32[]{:S(2)}, u32[]{:S(2)}) %all-to-all-start.1) | async-done | bytes 131104 | tf_op jit(solution)/shard_map/all_to_all | solution.py:354
  52.8 0.8 prefix.1
  53.5 3.4 %all-to-all-start.2 = ((bf16[8,32,256]{2,1,0:T(8,128)(2,1)}), bf16[8,32,256]{2,1,0:T(8,128)(2,1)S(1)}, u32[]{:S(2)}, u32[]{:S(2)}) async-start(bf16[8,32,256]{2,1,0:T(8,128)(2,1)} %prefix.1), calls=%async_computation.2 | async-start | bytes 262144 | tf_op jit(solution)/shard_map/all_to_all | solution.py:354
  56.9 0.0 copy-done.12
  56.9 0.1 broadcast_in_dim.6
  57.0 0.1 reshape_reshape.3.skip
  57.1 0.9 copy-done.1
  58.0 0.9 copy-done.3
  58.9 0.9 copy-done.4
  59.9 0.9 copy-done.6
  60.8 0.7 copy-done.7
  61.5 0.7 copy-done.8
  62.2 1.1 inside_span.1
  63.3 1.5 %all-to-all-done.2.got = bf16[8,32,256]{2,1,0:T(8,128)(2,1)S(1)} async-done(((bf16[8,32,256]{2,1,0:T(8,128)(2,1)}), bf16[8,32,256]{2,1,0:T(8,128)(2,1)S(1)}, u32[]{:S(2)}, u32[]{:S(2)}) %all-to-all-start.2) | async-done | bytes 131104 | tf_op jit(solution)/shard_map/all_to_all | solution.py:354
  64.7 0.0 copy-done
  64.7 0.0 copy-done.9
  64.7 0.8 apply_project.1
  65.6 0.0 copy-start.5
  65.6 8.1 %collective-permute-start.1 = (bf16[4,272,256]{2,1,0:T(8,128)(2,1)S(1)}, bf16[4,272,256]{2,1,0:T(8,128)(2,1)S(1)}, u32[]{:S(2)}, u32[]{:S(2)}) collective-permute-start(bf16[4,272,256]{2,1,0:T(8,128)(2,1)S(1)} %get-tuple-element.33), channel_id=1, source_target_pairs={{0,1},{1,0},{2,3},{3,2},{4,5},{5,4},{6,7},{7,6},{8,9},{9,8},{10,11... | collective-permute-start | bytes 1671176 | tf_op jit(solution)/shard_map/ppermute | solution.py:363
  73.7 1.6 %collective-permute-done.1 = bf16[4,272,256]{2,1,0:T(8,128)(2,1)S(1)} collective-permute-done((bf16[4,272,256]{2,1,0:T(8,128)(2,1)S(1)}, bf16[4,272,256]{2,1,0:T(8,128)(2,1)S(1)}, u32[]{:S(2)}, u32[]{:S(2)}) %collective-permute-start.1) | collective-permute-done | bytes 557088 | tf_op jit(solution)/shard_map/ppermute | solution.py:363
  75.2 1.0 add_convert_fusion
  76.2 4.2 %all-to-all-start.3 = ((bf16[4,272,256]{2,1,0:T(8,128)(2,1)}), bf16[4,272,256]{2,1,0:T(8,128)(2,1)S(1)}, u32[]{:S(2)}, u32[]{:S(2)}) async-start(bf16[4,272,256]{2,1,0:T(8,128)(2,1)} %add_convert_fusion), calls=%async_computation.3 | async-start | bytes 1114112 | tf_op jit(solution)/shard_map/all_to_all | solution.py:354
  80.4 0.8 dynamic_slice.3
  81.1 8.5 %all-to-all-done.3.got = bf16[4,272,256]{2,1,0:T(8,128)(2,1)S(1)} async-done(((bf16[4,272,256]{2,1,0:T(8,128)(2,1)}), bf16[4,272,256]{2,1,0:T(8,128)(2,1)S(1)}, u32[]{:S(2)}, u32[]{:S(2)}) %all-to-all-start.3) | async-done | bytes 557088 | tf_op jit(solution)/shard_map/all_to_all | solution.py:354
  89.7 0.4 merge.1
  90.1 2.2 %collective-permute-start.2 = (bf16[8,256]{1,0:T(8,128)(2,1)S(1)}, bf16[8,256]{1,0:T(8,128)(2,1)S(1)}, u32[]{:S(2)}, u32[]{:S(2)}) collective-permute-start(bf16[8,256]{1,0:T(8,128)(2,1)S(1)} %get-tuple-element.36), channel_id=1, source_target_pairs={{0,8},{8,16},{16,24},{24,32},{32,40},{40,48},{48,56},{56,64},{64,7... | collective-permute-start | bytes 12296 | tf_op jit(solution)/shard_map/ppermute | solution.py:359
  92.3 0.7 collective-permute-done.2
  93.1 9.7 %all_to_all.31.own = bf16[4,272,256]{2,1,0:T(8,128)(2,1)S(1)} all-to-all(bf16[4,272,256]{2,1,0:T(8,128)(2,1)S(1)} %broadcast_in_dim.7), channel_id=1, replica_groups=mesh['sp_0'=8,'sp_1'=8,'x'=4,'core'=2] {'x'}, dimensions={0} | all-to-all | bytes 1114112 | tf_op jit(solution)/shard_map/all_to_all | solution.py:354
  102.7 5.4 %collective-permute-start.3 = (bf16[4,272,256]{2,1,0:T(8,128)(2,1)S(1)}, bf16[4,272,256]{2,1,0:T(8,128)(2,1)S(1)}, u32[]{:S(2)}, u32[]{:S(2)}) collective-permute-start(bf16[4,272,256]{2,1,0:T(8,128)(2,1)S(1)} %all_to_all.31.own), channel_id=1, source_target_pairs={{0,1},{1,0},{2,3},{3,2},{4,5},{5,4},{6,7},{7,6},{8,9},{9,8},{10,11... | collective-permute-start | bytes 1671176 | tf_op jit(solution)/shard_map/ppermute | solution.py:363
  108.1 1.5 %collective-permute-done.3.other = bf16[4,272,256]{2,1,0:T(8,128)(2,1)S(1)} collective-permute-done((bf16[4,272,256]{2,1,0:T(8,128)(2,1)S(1)}, bf16[4,272,256]{2,1,0:T(8,128)(2,1)S(1)}, u32[]{:S(2)}, u32[]{:S(2)}) %collective-permute-start.3) | collective-permute-done | bytes 557088 | tf_op jit(solution)/shard_map/ppermute | solution.py:363
  109.7 3.5 %all-gather.3.cloned.1.call-done = bf16[3072,1280]{1,0:T(8,128)(2,1)} async-done(((bf16[48,1280]{1,0:T(8,128)(2,1)}), bf16[3072,1280]{1,0:T(8,128)(2,1)}) %all-gather.3.cloned.1.call-update) | async-done | bytes 7864336 | tf_op jit(solution)/shard_map/all_gather | solution.py:405
  113.2 4.7 %channel_mixer.1 = (bf16[4,256,256]{2,1,0:T(8,128)(2,1)S(1)}, bf16[256,640]{1,0:T(8,128)(2,1)S(1)}, bf16[64,16,1280]{2,1,0:T(8,128)(2,1)S(1)}) custom-call(s32[1]{0:T(128)} %bitcast.core, bf16[4,272,256]{2,1,0:T(8,128)(2,1)S(1)} %all_to_all.31.own, bf16[4,272,256]{2,1,0:T(8,128)(2,1)S(1)} %collective-permute-done.3.other, bf16[64,48,1280]{2,1,0:T(8,128)(2,1)} %bitcast.8, ...), custom_call_target="tpu_custom_call" | custom-call | tf_op jit(solution)/shard_map/channel_mixer/pallas_call | solution.py:475
  117.8 3.0 %collective-permute-start.4 = (bf16[4,256,256]{2,1,0:T(8,128)(2,1)S(1)}, bf16[4,256,256]{2,1,0:T(8,128)(2,1)S(1)}, u32[]{:S(2)}, u32[]{:S(2)}) collective-permute-start(bf16[4,256,256]{2,1,0:T(8,128)(2,1)S(1)} %get-tuple-element.40), channel_id=1, source_target_pairs={{0,1},{1,0},{2,3},{3,2},{4,5},{5,4},{6,7},{7,6},{8,9},{9,8},{10,11... | collective-permute-start | bytes 1572872 | tf_op jit(solution)/shard_map/ppermute | solution.py:363
  120.8 0.6 keep_blocks.1
  121.5 0.9 collective-permute-done.4
  122.4 0.1 add_convert_fusion.1
  122.5 12.4 %all_to_all.32.got = bf16[4,256,256]{2,1,0:T(8,128)(2,1)S(1)} all-to-all(bf16[4,256,256]{2,1,0:T(8,128)(2,1)S(1)} %add_convert_fusion.1), channel_id=1, replica_groups=mesh['sp_0'=8,'sp_1'=8,'x'=4,'core'=2] {'x'}, dimensions={0} | all-to-all | bytes 1048576 | tf_op jit(solution)/shard_map/all_to_all | solution.py:354
  134.9 0.7 finish.1
  (18 shorter events, 0.1 us)
Async XLA Ops:
  6.5 50.4 %copy-start.12 = (f32[8]{0:T(128)S(1)}, f32[8]{0:T(128)}, u32[]{:S(2)}) copy-start(f32[8]{0:T(128)} %param.22) | copy-start | bytes 100
  6.5 58.2 %copy-start = (bf16[512,2048]{1,0:T(8,128)(2,1)S(1)}, bf16[512,2048]{1,0:T(8,128)(2,1)}, u32[]{:S(2)}) copy-start(bf16[512,2048]{1,0:T(8,128)(2,1)} %weight.1) | copy-start | bytes 6291460
  6.5 58.2 %copy-start.9 = (f32[512]{0:T(512)S(1)}, f32[512]{0:T(512)}, u32[]{:S(2)}) copy-start(f32[512]{0:T(512)} %param.25) | copy-start | bytes 6148
  6.5 106.6 %all-gather.3.cloned.1.call-start = ((), (), s32[]{:S(2)}) async-start(), calls=%async_computation.6 | async-start | bytes 7987200 | tf_op jit(solution)/shard_map/all_gather | solution.py:405
  8.2 5.1 %collective-permute-start = (bf16[8,896]{1,0:T(8,128)(2,1)}, bf16[8,896]{1,0:T(8,128)(2,1)S(1)}, u32[]{:S(2)}, u32[]{:S(2)}) collective-permute-start(bf16[8,896]{1,0:T(8,128)(2,1)} %get-tuple-element.23), channel_id=1, source_target_pairs={{0,8},{8,16},{16,24},{24,32},{32,40},{40,48},{48,56},{56,64},{64,7... | collective-permute-start | bytes 43016 | tf_op jit(solution)/shard_map/ppermute | solution.py:359
  13.3 0.6 copy-start.10
  16.9 47.8 %copy-start.2 = (bf16[256,384]{1,0:T(8,128)(2,1)S(1)}, bf16[256,384]{1,0:T(8,128)(2,1)}, u32[]{:S(2)}) copy-start(bf16[256,384]{1,0:T(8,128)(2,1)} %get-tuple-element.25.keys) | copy-start | bytes 589828
  34.3 18.5 %all-to-all-start.1 = ((bf16[8,32,256]{2,1,0:T(8,128)(2,1)}), bf16[8,32,256]{2,1,0:T(8,128)(2,1)S(1)}, u32[]{:S(2)}, u32[]{:S(2)}) async-start(bf16[8,32,256]{2,1,0:T(8,128)(2,1)} %row_total.1), calls=%async_computation.1 | async-start | bytes 262144 | tf_op jit(solution)/shard_map/all_to_all | solution.py:354
  53.5 11.2 %all-to-all-start.2 = ((bf16[8,32,256]{2,1,0:T(8,128)(2,1)}), bf16[8,32,256]{2,1,0:T(8,128)(2,1)S(1)}, u32[]{:S(2)}, u32[]{:S(2)}) async-start(bf16[8,32,256]{2,1,0:T(8,128)(2,1)} %prefix.1), calls=%async_computation.2 | async-start | bytes 262144 | tf_op jit(solution)/shard_map/all_to_all | solution.py:354
  57.1 0.9 copy-start.1
  58.0 0.9 copy-start.3
  58.9 0.9 copy-start.4
  59.9 0.9 copy-start.6
  60.8 0.7 copy-start.7
  61.5 0.7 copy-start.8
  65.6 24.1 %copy-start.5 = (bf16[256,256]{1,0:T(8,128)(2,1)S(1)}, bf16[256,256]{1,0:T(8,128)(2,1)}, u32[]{:S(2)}) copy-start(bf16[256,256]{1,0:T(8,128)(2,1)} %residual.1) | copy-start | bytes 393220
  65.6 9.6 %collective-permute-start.1 = (bf16[4,272,256]{2,1,0:T(8,128)(2,1)S(1)}, bf16[4,272,256]{2,1,0:T(8,128)(2,1)S(1)}, u32[]{:S(2)}, u32[]{:S(2)}) collective-permute-start(bf16[4,272,256]{2,1,0:T(8,128)(2,1)S(1)} %get-tuple-element.33), channel_id=1, source_target_pairs={{0,1},{1,0},{2,3},{3,2},{4,5},{5,4},{6,7},{7,6},{8,9},{9,8},{10,11... | collective-permute-start | bytes 1671176 | tf_op jit(solution)/shard_map/ppermute | solution.py:363
  76.2 31.9 %copy-start.11 = (bf16[2,3,640]{2,0,1:T(2,128)(2,1)S(1)}, bf16[2,3,640]{2,0,1:T(2,128)(2,1)}, u32[]{:S(2)}) copy-start(bf16[2,3,640]{2,0,1:T(2,128)(2,1)} %param.30) | copy-start | bytes 23044
  76.2 13.4 %all-to-all-start.3 = ((bf16[4,272,256]{2,1,0:T(8,128)(2,1)}), bf16[4,272,256]{2,1,0:T(8,128)(2,1)S(1)}, u32[]{:S(2)}, u32[]{:S(2)}) async-start(bf16[4,272,256]{2,1,0:T(8,128)(2,1)} %add_convert_fusion), calls=%async_computation.3 | async-start | bytes 1114112 | tf_op jit(solution)/shard_map/all_to_all | solution.py:354
  90.1 2.9 %collective-permute-start.2 = (bf16[8,256]{1,0:T(8,128)(2,1)S(1)}, bf16[8,256]{1,0:T(8,128)(2,1)S(1)}, u32[]{:S(2)}, u32[]{:S(2)}) collective-permute-start(bf16[8,256]{1,0:T(8,128)(2,1)S(1)} %get-tuple-element.36), channel_id=1, source_target_pairs={{0,8},{8,16},{16,24},{24,32},{32,40},{40,48},{48,56},{56,64},{64,7... | collective-permute-start | bytes 12296 | tf_op jit(solution)/shard_map/ppermute | solution.py:359
  102.7 6.9 %collective-permute-start.3 = (bf16[4,272,256]{2,1,0:T(8,128)(2,1)S(1)}, bf16[4,272,256]{2,1,0:T(8,128)(2,1)S(1)}, u32[]{:S(2)}, u32[]{:S(2)}) collective-permute-start(bf16[4,272,256]{2,1,0:T(8,128)(2,1)S(1)} %all_to_all.31.own), channel_id=1, source_target_pairs={{0,1},{1,0},{2,3},{3,2},{4,5},{5,4},{6,7},{7,6},{8,9},{9,8},{10,11... | collective-permute-start | bytes 1671176 | tf_op jit(solution)/shard_map/ppermute | solution.py:363
  117.8 4.5 %collective-permute-start.4 = (bf16[4,256,256]{2,1,0:T(8,128)(2,1)S(1)}, bf16[4,256,256]{2,1,0:T(8,128)(2,1)S(1)}, u32[]{:S(2)}, u32[]{:S(2)}) collective-permute-start(bf16[4,256,256]{2,1,0:T(8,128)(2,1)S(1)} %get-tuple-element.40), channel_id=1, source_target_pairs={{0,1},{1,0},{2,3},{3,2},{4,5},{5,4},{6,7},{7,6},{8,9},{9,8},{10,11... | collective-permute-start | bytes 1572872 | tf_op jit(solution)/shard_map/ppermute | solution.py:363
Sparse Core Ops, SparseCore 0:
  10.3 102.7 all-gather.2

commit v6 on v5

--- a/solution.py
+++ b/solution.py
@@ -275,7 +275,7 @@
 
 
 def channel_kernel(
-    features, core, own, other, weights, taps, give, hidden, down, lhs, wide, buf, total, sems
+    features, core, own, other, weights, taps, give, hidden, down, lhs, wide, total, sems
 ):
     chips, high, share = own.shape
     rows = high - 16
@@ -308,7 +308,7 @@
         squares = marks[at : at + 1, :] + marks[at + 1 : at + 2, :]
         return as_col(lax.rsqrt(squares / features + NORM_FLOOR))
 
-    scale, before = inverse_of(0), inverse_of(8)
+    scale = jnp.concatenate([inverse_of(0), inverse_of(8)[rows - 16 :]], axis=0)
     step = spans // quarters
     depth = step * each
     for n in range(quarters):
@@ -322,22 +322,22 @@
         elif n < quarters - 1:
             total[...] += part
         else:
-            part = total[...] + part
-            edge = part[rows + 8 :] * before[rows - 8 :, :]
-            buf[0:8, :] = edge.astype(BF16).astype(F32)
-            buf[8 : 8 + rows, :] = (part[:rows] * scale).astype(BF16).astype(F32)
-
-    def conv(branch):
-        first, last = branch * units, (branch + 1) * units
-        count = taps.shape[1]
-        summed = None
-        for k in range(count):
-            at = 8 - (count - 1) + k
-            term = taps[branch, k : k + 1, :].astype(F32) * buf[at : at + rows, first:last]
-            summed = term if summed is None else summed + term
-        return summed
-
-    hidden[...] = (silu(conv(0)) * conv(1)).astype(BF16)
+            part = (total[...] + part) * scale
+            total[...] = part.astype(BF16).astype(F32)
+
+    def conv(branch, lane):
+        at = branch * units + lane
+        held = total[:, at : at + 128]
+        row = taps[branch, :, lane : lane + 128].astype(F32)
+        count = row.shape[0]
+        summed = row[count - 1 : count] * held
+        for k in range(1, count):
+            summed = summed + row[count - 1 - k : count - k] * pltpu.roll(held, k, 0)
+        return summed[:rows]
+
+    for lane in range(0, units, 128):
+        gated = silu(conv(0, lane)) * conv(1, lane)
+        hidden[:, lane : lane + 128] = gated.astype(BF16)
     for copy in copies[quarters:]:
         copy.wait()
     down_blocks(give, 1 - mine, down, hidden)
@@ -482,7 +482,6 @@
         [
             ((rows + 16, features * n_tp), BF16),
             ((spans, each, 2 * units), BF16),
-            ((rows + 8, 2 * units), F32),
             ((rows + 16, 2 * units), F32),
         ],
         more_scratch=[pltpu.SemaphoreType.DMA((6,))],

time: 143 us -> 143 us (level)
  no operation moved by 1% of the time
where the time goes in v6:
time: 143 us; the launch traced here: 142 us
  starting transfers between devices  40.8 us (29%)
  blocking collectives  38.7 us (27%)
  waiting for transfers between devices  27.2 us (19%)
  Pallas kernels  14.4 us (10%)
  between operations  13.5 us (9%)
  local copies, waits for them, and re-layouts  6.69 us (5%)
    all_to_all x3, blocking collectives, exchange(): return lax.all_to_all(parts, axis, split_axis=0, concat_axis=0, tiled=True)  38.7 us
    all_to_all x3, starting transfers between devices, exchange(): return lax.all_to_all(parts, axis, split_axis=0, concat_axis=0, tiled=True)  18.1 us
    all_to_all x3, waiting for transfers between devices, exchange(): return lax.all_to_all(parts, axis, split_axis=0, concat_axis=0, tiled=True)  17.9 us
    ppermute x3, starting transfers between devices, swapped(): return lax.ppermute(value, 'core', [(0, 1), (1, 0)])  16.4 us
    ppermute x2, starting transfers between devices, from_behind(): lax.ppermute(value, axis, [(source, source + 1) for source in range(count...  6.21 us
    unnamed x27, local copies, waits for them, and re-layouts  5.75 us
    pallas_call x1, Pallas kernels, local(): call(functools.partial(channel_kernel, features * n_tp), [((chips, featur...  4.59 us
    ppermute x3, waiting for transfers between devices, swapped(): return lax.ppermute(value, 'core', [(0, 1), (1, 0)])  4.01 us
  transfers between devices with their start and end apart: 9, of which 9 were waited for; matrix products, arithmetic and copies ran while one was open for 1% of the time, Pallas kernels for 5%

profile of v6, /device:TPU:1, one launch (start us, length us, event | category | flops | bytes accessed | tf_op | source)
XLA Modules:
  0.0 142.4 jit_solution(11890532342273061538)
XLA Ops:
  6.5 0.0 all-gather.3.cloned.1.call-start
  6.5 1.7 %pack.1 = (bf16[48,1280]{1,0:T(8,128)(2,1)}, bf16[8,896]{1,0:T(8,128)(2,1)}) custom-call(bf16[32,640]{1,0:T(8,128)(2,1)} %gate.2, bf16[32,640]{1,0:T(8,128)(2,1)} %up.1, bf16[32,640]{1,0:T(8,128)(2,1)} %bitcast.9, bf16[256,512]{1,0:T(8,128)(2,1)} %values.3, bf16[256,384]{1,0:T(8,128)(2,1)} %keys.3), custom_call_target="tpu_custom_call" | custom-call | tf_op jit(solution)/shard_map/pack/pallas_call | solution.py:393
  8.2 0.0 all-gather.3.cloned.1.call-update
  8.2 4.0 %collective-permute-start = (bf16[8,896]{1,0:T(8,128)(2,1)}, bf16[8,896]{1,0:T(8,128)(2,1)S(1)}, u32[]{:S(2)}, u32[]{:S(2)}) collective-permute-start(bf16[8,896]{1,0:T(8,128)(2,1)} %get-tuple-element.23), channel_id=1, source_target_pairs={{0,8},{8,16},{16,24},{24,32},{32,40},{40,48},{48,56},{56,64},{64,7... | collective-permute-start | bytes 43016 | tf_op jit(solution)/shard_map/ppermute | solution.py:359
  12.2 1.0 collective-permute-done.before
  13.3 0.6 copy-done.10
  13.9 3.0 %span_state.1 = (bf16[256,512]{1,0:T(8,128)(2,1)}, bf16[256,384]{1,0:T(8,128)(2,1)}, f32[8,256]{1,0:T(8,128)}, f32[8,256]{1,0:T(8,128)}, f32[256,8]{1,0:T(8,128)}, /*index=5*/bf16[8,32,256]{2,1,0:T(8,128)(2,1)}) custom-call(bf16[256,512]{1,0:T(8,128)(2,1)} %values.3, bf16[256,384]{1,0:T(8,128)(2,1)} %keys.3, bf16[8,896]{1,0:T(8,128)(2,1)} %copy-done.10, ...), custom_call_target="tpu_custom_call" | custom-call | tf_op jit(solution)/shard_map/span_state/pallas_call | solution.py:414
  16.9 16.6 %all_to_all.30.got = bf16[8,32,256]{2,1,0:T(8,128)(2,1)S(1)} all-to-all(bf16[8,32,256]{2,1,0:T(8,128)(2,1)} %get-tuple-element.31), channel_id=1, replica_groups=mesh['sp_0'=8,'sp_1'=8,'x'=4,'core'=2] {'sp_1'}, dimensions={0} | all-to-all | bytes 262144 | tf_op jit(solution)/shard_map/all_to_all | solution.py:354
  33.5 0.7 row_total.1
  34.3 10.6 %all-to-all-start.1 = ((bf16[8,32,256]{2,1,0:T(8,128)(2,1)}), bf16[8,32,256]{2,1,0:T(8,128)(2,1)S(1)}, u32[]{:S(2)}, u32[]{:S(2)}) async-start(bf16[8,32,256]{2,1,0:T(8,128)(2,1)} %row_total.1), calls=%async_computation.1 | async-start | bytes 262144 | tf_op jit(solution)/shard_map/all_to_all | solution.py:354
  44.9 7.9 %all-to-all-done.1.totals = bf16[8,32,256]{2,1,0:T(8,128)(2,1)S(1)} async-done(((bf16[8,32,256]{2,1,0:T(8,128)(2,1)}), bf16[8,32,256]{2,1,0:T(8,128)(2,1)S(1)}, u32[]{:S(2)}, u32[]{:S(2)}) %all-to-all-start.1) | async-done | bytes 131104 | tf_op jit(solution)/shard_map/all_to_all | solution.py:354
  52.8 0.8 prefix.1
  53.5 3.4 %all-to-all-start.2 = ((bf16[8,32,256]{2,1,0:T(8,128)(2,1)}), bf16[8,32,256]{2,1,0:T(8,128)(2,1)S(1)}, u32[]{:S(2)}, u32[]{:S(2)}) async-start(bf16[8,32,256]{2,1,0:T(8,128)(2,1)} %prefix.1), calls=%async_computation.2 | async-start | bytes 262144 | tf_op jit(solution)/shard_map/all_to_all | solution.py:354
  56.9 0.0 copy-done.12
  56.9 0.1 broadcast_in_dim.6
  57.0 0.1 reshape_reshape.3.skip
  57.1 0.9 copy-done.1
  58.0 0.9 copy-done.3
  58.9 0.9 copy-done.4
  59.9 0.9 copy-done.6
  60.8 0.7 copy-done.7
  61.5 0.7 copy-done.8
  62.2 1.1 inside_span.1
  63.3 1.5 %all-to-all-done.2.got = bf16[8,32,256]{2,1,0:T(8,128)(2,1)S(1)} async-done(((bf16[8,32,256]{2,1,0:T(8,128)(2,1)}), bf16[8,32,256]{2,1,0:T(8,128)(2,1)S(1)}, u32[]{:S(2)}, u32[]{:S(2)}) %all-to-all-start.2) | async-done | bytes 131104 | tf_op jit(solution)/shard_map/all_to_all | solution.py:354
  64.7 0.0 copy-done
  64.7 0.8 apply_project.1
  65.6 0.0 copy-start.5
  65.6 8.1 %collective-permute-start.1 = (bf16[4,272,256]{2,1,0:T(8,128)(2,1)S(1)}, bf16[4,272,256]{2,1,0:T(8,128)(2,1)S(1)}, u32[]{:S(2)}, u32[]{:S(2)}) collective-permute-start(bf16[4,272,256]{2,1,0:T(8,128)(2,1)S(1)} %get-tuple-element.33), channel_id=1, source_target_pairs={{0,1},{1,0},{2,3},{3,2},{4,5},{5,4},{6,7},{7,6},{8,9},{9,8},{10,11... | collective-permute-start | bytes 1671176 | tf_op jit(solution)/shard_map/ppermute | solution.py:363
  73.7 1.6 %collective-permute-done.1 = bf16[4,272,256]{2,1,0:T(8,128)(2,1)S(1)} collective-permute-done((bf16[4,272,256]{2,1,0:T(8,128)(2,1)S(1)}, bf16[4,272,256]{2,1,0:T(8,128)(2,1)S(1)}, u32[]{:S(2)}, u32[]{:S(2)}) %collective-permute-start.1) | collective-permute-done | bytes 557088 | tf_op jit(solution)/shard_map/ppermute | solution.py:363
  75.2 1.0 add_convert_fusion
  76.2 4.2 %all-to-all-start.3 = ((bf16[4,272,256]{2,1,0:T(8,128)(2,1)}), bf16[4,272,256]{2,1,0:T(8,128)(2,1)S(1)}, u32[]{:S(2)}, u32[]{:S(2)}) async-start(bf16[4,272,256]{2,1,0:T(8,128)(2,1)} %add_convert_fusion), calls=%async_computation.3 | async-start | bytes 1114112 | tf_op jit(solution)/shard_map/all_to_all | solution.py:354
  80.4 0.8 dynamic_slice.3
  81.1 8.5 %all-to-all-done.3.got = bf16[4,272,256]{2,1,0:T(8,128)(2,1)S(1)} async-done(((bf16[4,272,256]{2,1,0:T(8,128)(2,1)}), bf16[4,272,256]{2,1,0:T(8,128)(2,1)S(1)}, u32[]{:S(2)}, u32[]{:S(2)}) %all-to-all-start.3) | async-done | bytes 557088 | tf_op jit(solution)/shard_map/all_to_all | solution.py:354
  89.6 0.0 copy-done.5
  89.7 0.4 merge.1
  90.1 2.2 %collective-permute-start.2 = (bf16[8,256]{1,0:T(8,128)(2,1)S(1)}, bf16[8,256]{1,0:T(8,128)(2,1)S(1)}, u32[]{:S(2)}, u32[]{:S(2)}) collective-permute-start(bf16[8,256]{1,0:T(8,128)(2,1)S(1)} %get-tuple-element.36), channel_id=1, source_target_pairs={{0,8},{8,16},{16,24},{24,32},{32,40},{40,48},{48,56},{56,64},{64,7... | collective-permute-start | bytes 12296 | tf_op jit(solution)/shard_map/ppermute | solution.py:359
  92.3 0.7 collective-permute-done.2
  93.1 9.7 %all_to_all.31.own = bf16[4,272,256]{2,1,0:T(8,128)(2,1)S(1)} all-to-all(bf16[4,272,256]{2,1,0:T(8,128)(2,1)S(1)} %broadcast_in_dim.7), channel_id=1, replica_groups=mesh['sp_0'=8,'sp_1'=8,'x'=4,'core'=2] {'x'}, dimensions={0} | all-to-all | bytes 1114112 | tf_op jit(solution)/shard_map/all_to_all | solution.py:354
  102.7 5.4 %collective-permute-start.3 = (bf16[4,272,256]{2,1,0:T(8,128)(2,1)S(1)}, bf16[4,272,256]{2,1,0:T(8,128)(2,1)S(1)}, u32[]{:S(2)}, u32[]{:S(2)}) collective-permute-start(bf16[4,272,256]{2,1,0:T(8,128)(2,1)S(1)} %all_to_all.31.own), channel_id=1, source_target_pairs={{0,1},{1,0},{2,3},{3,2},{4,5},{5,4},{6,7},{7,6},{8,9},{9,8},{10,11... | collective-permute-start | bytes 1671176 | tf_op jit(solution)/shard_map/ppermute | solution.py:363
  108.1 1.5 %collective-permute-done.3.other = bf16[4,272,256]{2,1,0:T(8,128)(2,1)S(1)} collective-permute-done((bf16[4,272,256]{2,1,0:T(8,128)(2,1)S(1)}, bf16[4,272,256]{2,1,0:T(8,128)(2,1)S(1)}, u32[]{:S(2)}, u32[]{:S(2)}) %collective-permute-start.3) | collective-permute-done | bytes 557088 | tf_op jit(solution)/shard_map/ppermute | solution.py:363
  109.7 3.5 %all-gather.3.cloned.1.call-done = bf16[3072,1280]{1,0:T(8,128)(2,1)} async-done(((bf16[48,1280]{1,0:T(8,128)(2,1)}), bf16[3072,1280]{1,0:T(8,128)(2,1)}) %all-gather.3.cloned.1.call-update) | async-done | bytes 7864336 | tf_op jit(solution)/shard_map/all_gather | solution.py:405
  113.2 4.6 %channel_mixer.1 = (bf16[4,256,256]{2,1,0:T(8,128)(2,1)S(1)}, bf16[256,640]{1,0:T(8,128)(2,1)S(1)}, bf16[64,16,1280]{2,1,0:T(8,128)(2,1)S(1)}) custom-call(s32[1]{0:T(128)} %bitcast.core, bf16[4,272,256]{2,1,0:T(8,128)(2,1)S(1)} %all_to_all.31.own, bf16[4,272,256]{2,1,0:T(8,128)(2,1)S(1)} %collective-permute-done.3.other, bf16[64,48,1280]{2,1,0:T(8,128)(2,1)} %bitcast.8, ...), custom_call_target="tpu_custom_call" | custom-call | tf_op jit(solution)/shard_map/channel_mixer/pallas_call | solution.py:475
  117.8 3.0 %collective-permute-start.4 = (bf16[4,256,256]{2,1,0:T(8,128)(2,1)S(1)}, bf16[4,256,256]{2,1,0:T(8,128)(2,1)S(1)}, u32[]{:S(2)}, u32[]{:S(2)}) collective-permute-start(bf16[4,256,256]{2,1,0:T(8,128)(2,1)S(1)} %get-tuple-element.40), channel_id=1, source_target_pairs={{0,1},{1,0},{2,3},{3,2},{4,5},{5,4},{6,7},{7,6},{8,9},{9,8},{10,11... | collective-permute-start | bytes 1572872 | tf_op jit(solution)/shard_map/ppermute | solution.py:363
  120.8 0.6 keep_blocks.1
  121.4 0.9 collective-permute-done.4
  122.3 0.1 add_convert_fusion.1
  122.4 12.4 %all_to_all.32.got = bf16[4,256,256]{2,1,0:T(8,128)(2,1)S(1)} all-to-all(bf16[4,256,256]{2,1,0:T(8,128)(2,1)S(1)} %add_convert_fusion.1), channel_id=1, replica_groups=mesh['sp_0'=8,'sp_1'=8,'x'=4,'core'=2] {'x'}, dimensions={0} | all-to-all | bytes 1048576 | tf_op jit(solution)/shard_map/all_to_all | solution.py:354
  134.8 0.7 finish.1
  (18 shorter events, 0.1 us)
Async XLA Ops:
  6.5 50.4 %copy-start.12 = (f32[8]{0:T(128)S(1)}, f32[8]{0:T(128)}, u32[]{:S(2)}) copy-start(f32[8]{0:T(128)} %param.22) | copy-start | bytes 100
  6.5 58.2 %copy-start = (bf16[512,2048]{1,0:T(8,128)(2,1)S(1)}, bf16[512,2048]{1,0:T(8,128)(2,1)}, u32[]{:S(2)}) copy-start(bf16[512,2048]{1,0:T(8,128)(2,1)} %weight.1) | copy-start | bytes 6291460
  6.5 58.2 %copy-start.9 = (f32[512]{0:T(512)S(1)}, f32[512]{0:T(512)}, u32[]{:S(2)}) copy-start(f32[512]{0:T(512)} %param.25) | copy-start | bytes 6148
  6.5 106.6 %all-gather.3.cloned.1.call-start = ((), (), s32[]{:S(2)}) async-start(), calls=%async_computation.6 | async-start | bytes 7987200 | tf_op jit(solution)/shard_map/all_gather | solution.py:405
  8.2 5.1 %collective-permute-start = (bf16[8,896]{1,0:T(8,128)(2,1)}, bf16[8,896]{1,0:T(8,128)(2,1)S(1)}, u32[]{:S(2)}, u32[]{:S(2)}) collective-permute-start(bf16[8,896]{1,0:T(8,128)(2,1)} %get-tuple-element.23), channel_id=1, source_target_pairs={{0,8},{8,16},{16,24},{24,32},{32,40},{40,48},{48,56},{56,64},{64,7... | collective-permute-start | bytes 43016 | tf_op jit(solution)/shard_map/ppermute | solution.py:359
  13.3 0.6 copy-start.10
  16.9 47.8 %copy-start.2 = (bf16[256,384]{1,0:T(8,128)(2,1)S(1)}, bf16[256,384]{1,0:T(8,128)(2,1)}, u32[]{:S(2)}) copy-start(bf16[256,384]{1,0:T(8,128)(2,1)} %get-tuple-element.25.keys) | copy-start | bytes 589828
  34.3 18.5 %all-to-all-start.1 = ((bf16[8,32,256]{2,1,0:T(8,128)(2,1)}), bf16[8,32,256]{2,1,0:T(8,128)(2,1)S(1)}, u32[]{:S(2)}, u32[]{:S(2)}) async-start(bf16[8,32,256]{2,1,0:T(8,128)(2,1)} %row_total.1), calls=%async_computation.1 | async-start | bytes 262144 | tf_op jit(solution)/shard_map/all_to_all | solution.py:354
  53.5 11.2 %all-to-all-start.2 = ((bf16[8,32,256]{2,1,0:T(8,128)(2,1)}), bf16[8,32,256]{2,1,0:T(8,128)(2,1)S(1)}, u32[]{:S(2)}, u32[]{:S(2)}) async-start(bf16[8,32,256]{2,1,0:T(8,128)(2,1)} %prefix.1), calls=%async_computation.2 | async-start | bytes 262144 | tf_op jit(solution)/shard_map/all_to_all | solution.py:354
  57.1 0.9 copy-start.1
  58.0 0.9 copy-start.3
  58.9 0.9 copy-start.4
  59.9 0.9 copy-start.6
  60.8 0.7 copy-start.7
  61.5 0.7 copy-start.8
  65.6 24.1 %copy-start.5 = (bf16[256,256]{1,0:T(8,128)(2,1)S(1)}, bf16[256,256]{1,0:T(8,128)(2,1)}, u32[]{:S(2)}) copy-start(bf16[256,256]{1,0:T(8,128)(2,1)} %residual.1) | copy-start | bytes 393220
  65.6 9.6 %collective-permute-start.1 = (bf16[4,272,256]{2,1,0:T(8,128)(2,1)S(1)}, bf16[4,272,256]{2,1,0:T(8,128)(2,1)S(1)}, u32[]{:S(2)}, u32[]{:S(2)}) collective-permute-start(bf16[4,272,256]{2,1,0:T(8,128)(2,1)S(1)} %get-tuple-element.33), channel_id=1, source_target_pairs={{0,1},{1,0},{2,3},{3,2},{4,5},{5,4},{6,7},{7,6},{8,9},{9,8},{10,11... | collective-permute-start | bytes 1671176 | tf_op jit(solution)/shard_map/ppermute | solution.py:363
  76.2 31.9 %copy-start.11 = (bf16[2,3,640]{2,0,1:T(2,128)(2,1)S(1)}, bf16[2,3,640]{2,0,1:T(2,128)(2,1)}, u32[]{:S(2)}) copy-start(bf16[2,3,640]{2,0,1:T(2,128)(2,1)} %param.30) | copy-start | bytes 23044
  76.2 13.4 %all-to-all-start.3 = ((bf16[4,272,256]{2,1,0:T(8,128)(2,1)}), bf16[4,272,256]{2,1,0:T(8,128)(2,1)S(1)}, u32[]{:S(2)}, u32[]{:S(2)}) async-start(bf16[4,272,256]{2,1,0:T(8,128)(2,1)} %add_convert_fusion), calls=%async_computation.3 | async-start | bytes 1114112 | tf_op jit(solution)/shard_map/all_to_all | solution.py:354
  90.1 2.9 %collective-permute-start.2 = (bf16[8,256]{1,0:T(8,128)(2,1)S(1)}, bf16[8,256]{1,0:T(8,128)(2,1)S(1)}, u32[]{:S(2)}, u32[]{:S(2)}) collective-permute-start(bf16[8,256]{1,0:T(8,128)(2,1)S(1)} %get-tuple-element.36), channel_id=1, source_target_pairs={{0,8},{8,16},{16,24},{24,32},{32,40},{40,48},{48,56},{56,64},{64,7... | collective-permute-start | bytes 12296 | tf_op jit(solution)/shard_map/ppermute | solution.py:359
  102.7 6.9 %collective-permute-start.3 = (bf16[4,272,256]{2,1,0:T(8,128)(2,1)S(1)}, bf16[4,272,256]{2,1,0:T(8,128)(2,1)S(1)}, u32[]{:S(2)}, u32[]{:S(2)}) collective-permute-start(bf16[4,272,256]{2,1,0:T(8,128)(2,1)S(1)} %all_to_all.31.own), channel_id=1, source_target_pairs={{0,1},{1,0},{2,3},{3,2},{4,5},{5,4},{6,7},{7,6},{8,9},{9,8},{10,11... | collective-permute-start | bytes 1671176 | tf_op jit(solution)/shard_map/ppermute | solution.py:363
  117.8 4.5 %collective-permute-start.4 = (bf16[4,256,256]{2,1,0:T(8,128)(2,1)S(1)}, bf16[4,256,256]{2,1,0:T(8,128)(2,1)S(1)}, u32[]{:S(2)}, u32[]{:S(2)}) collective-permute-start(bf16[4,256,256]{2,1,0:T(8,128)(2,1)S(1)} %get-tuple-element.40), channel_id=1, source_target_pairs={{0,1},{1,0},{2,3},{3,2},{4,5},{5,4},{6,7},{7,6},{8,9},{9,8},{10,11... | collective-permute-start | bytes 1572872 | tf_op jit(solution)/shard_map/ppermute | solution.py:363
Sparse Core Ops, SparseCore 0:
  10.3 102.7 all-gather.2

commit v7 on v5

--- a/solution.py
+++ b/solution.py
@@ -198,13 +198,12 @@
 def prefix_kernel(place, got, totals, pay):
     count = got.shape[0]
     mine = place[0]
-    total = jnp.zeros((pay.shape[1] - 8, pay.shape[2]), F32)
+    total = jnp.zeros((pay.shape[1], pay.shape[2]), F32)
     for c in range(totals.shape[0]):
         state, wide, narrow = span_parts(totals[c].astype(F32))
         total = jnp.where(c < mine, total * fade(wide, narrow) + state, total)
-    pad = jnp.zeros((8, pay.shape[2]), F32)
     for c in range(count):
-        pay[c] = jnp.concatenate([total, pad], axis=0).astype(BF16)
+        pay[c] = total.astype(BF16)
         state, wide, narrow = span_parts(got[c].astype(F32))
         total = total * fade(wide, narrow) + state
 
@@ -445,7 +444,7 @@
     place = lax.axis_index(SP[0]).astype(jnp.int32).reshape(1)
     (starts,) = call(
         prefix_kernel,
-        [((n_row, span, HALF), BF16)],
+        [((n_row, span - 8, HALF), BF16)],
         in_specs=[
             pl.BlockSpec(memory_space=pltpu.SMEM),
             pl.BlockSpec(memory_space=pltpu.VMEM),

time: 143 us -> 143 us (level)
  no operation moved by 1% of the time
where the time goes in v7:
time: 143 us; the launch traced here: 142 us
  starting transfers between devices  40.7 us (28%)
  blocking collectives  38.7 us (27%)
  waiting for transfers between devices  27.2 us (19%)
  Pallas kernels  14.4 us (10%)
  between operations  13.5 us (9%)
  local copies, waits for them, and re-layouts  6.69 us (5%)
    all_to_all x3, blocking collectives, exchange(): return lax.all_to_all(parts, axis, split_axis=0, concat_axis=0, tiled=True)  38.7 us
    all_to_all x3, starting transfers between devices, exchange(): return lax.all_to_all(parts, axis, split_axis=0, concat_axis=0, tiled=True)  18.1 us
    all_to_all x3, waiting for transfers between devices, exchange(): return lax.all_to_all(parts, axis, split_axis=0, concat_axis=0, tiled=True)  17.6 us
    ppermute x3, starting transfers between devices, swapped(): return lax.ppermute(value, 'core', [(0, 1), (1, 0)])  16.4 us
    ppermute x2, starting transfers between devices, from_behind(): lax.ppermute(value, axis, [(source, source + 1) for source in range(count...  6.21 us
    unnamed x27, local copies, waits for them, and re-layouts  5.75 us
    pallas_call x1, Pallas kernels, local(): call(functools.partial(channel_kernel, features * n_tp), [((chips, featur...  4.67 us
    ppermute x3, waiting for transfers between devices, swapped(): return lax.ppermute(value, 'core', [(0, 1), (1, 0)])  4 us
  transfers between devices with their start and end apart: 9, of which 9 were waited for; matrix products, arithmetic and copies ran while one was open for 1% of the time, Pallas kernels for 5%

profile of v7, /device:TPU:1, one launch (start us, length us, event | category | flops | bytes accessed | tf_op | source)
XLA Modules:
  0.0 142.5 jit_solution(2564075180128148033)
XLA Ops:
  6.5 0.0 all-gather.3.cloned.1.call-start
  6.5 1.7 %pack.1 = (bf16[48,1280]{1,0:T(8,128)(2,1)}, bf16[8,896]{1,0:T(8,128)(2,1)}) custom-call(bf16[32,640]{1,0:T(8,128)(2,1)} %gate.2, bf16[32,640]{1,0:T(8,128)(2,1)} %up.1, bf16[32,640]{1,0:T(8,128)(2,1)} %bitcast.9, bf16[256,512]{1,0:T(8,128)(2,1)} %values.3, bf16[256,384]{1,0:T(8,128)(2,1)} %keys.3), custom_call_target="tpu_custom_call" | custom-call | tf_op jit(solution)/shard_map/pack/pallas_call | solution.py:392
  8.2 0.0 all-gather.3.cloned.1.call-update
  8.2 4.0 %collective-permute-start = (bf16[8,896]{1,0:T(8,128)(2,1)}, bf16[8,896]{1,0:T(8,128)(2,1)S(1)}, u32[]{:S(2)}, u32[]{:S(2)}) collective-permute-start(bf16[8,896]{1,0:T(8,128)(2,1)} %get-tuple-element.23), channel_id=1, source_target_pairs={{0,8},{8,16},{16,24},{24,32},{32,40},{40,48},{48,56},{56,64},{64,7... | collective-permute-start | bytes 43016 | tf_op jit(solution)/shard_map/ppermute | solution.py:358
  12.2 1.0 collective-permute-done.before
  13.3 0.6 copy-done.10
  13.9 3.0 %span_state.1 = (bf16[256,512]{1,0:T(8,128)(2,1)}, bf16[256,384]{1,0:T(8,128)(2,1)}, f32[8,256]{1,0:T(8,128)}, f32[8,256]{1,0:T(8,128)}, f32[256,8]{1,0:T(8,128)}, /*index=5*/bf16[8,32,256]{2,1,0:T(8,128)(2,1)}) custom-call(bf16[256,512]{1,0:T(8,128)(2,1)} %values.3, bf16[256,384]{1,0:T(8,128)(2,1)} %keys.3, bf16[8,896]{1,0:T(8,128)(2,1)} %copy-done.10, ...), custom_call_target="tpu_custom_call" | custom-call | tf_op jit(solution)/shard_map/span_state/pallas_call | solution.py:413
  16.9 16.6 %all_to_all.30.got = bf16[8,32,256]{2,1,0:T(8,128)(2,1)S(1)} all-to-all(bf16[8,32,256]{2,1,0:T(8,128)(2,1)} %get-tuple-element.31), channel_id=1, replica_groups=mesh['sp_0'=8,'sp_1'=8,'x'=4,'core'=2] {'sp_1'}, dimensions={0} | all-to-all | bytes 262144 | tf_op jit(solution)/shard_map/all_to_all | solution.py:353
  33.5 0.7 row_total.1
  34.3 10.6 %all-to-all-start.1 = ((bf16[8,32,256]{2,1,0:T(8,128)(2,1)}), bf16[8,32,256]{2,1,0:T(8,128)(2,1)S(1)}, u32[]{:S(2)}, u32[]{:S(2)}) async-start(bf16[8,32,256]{2,1,0:T(8,128)(2,1)} %row_total.1), calls=%async_computation.1 | async-start | bytes 262144 | tf_op jit(solution)/shard_map/all_to_all | solution.py:353
  44.9 7.9 %all-to-all-done.1.totals = bf16[8,32,256]{2,1,0:T(8,128)(2,1)S(1)} async-done(((bf16[8,32,256]{2,1,0:T(8,128)(2,1)}), bf16[8,32,256]{2,1,0:T(8,128)(2,1)S(1)}, u32[]{:S(2)}, u32[]{:S(2)}) %all-to-all-start.1) | async-done | bytes 131104 | tf_op jit(solution)/shard_map/all_to_all | solution.py:353
  52.8 0.7 prefix.1
  53.5 3.4 %all-to-all-start.2 = ((bf16[8,24,256]{2,1,0:T(8,128)(2,1)}), bf16[8,24,256]{2,1,0:T(8,128)(2,1)S(1)}, u32[]{:S(2)}, u32[]{:S(2)}) async-start(bf16[8,24,256]{2,1,0:T(8,128)(2,1)} %prefix.1), calls=%async_computation.2 | async-start | bytes 196608 | tf_op jit(solution)/shard_map/all_to_all | solution.py:353
  56.9 0.0 copy-done.12
  56.9 0.1 broadcast_in_dim.6
  57.0 0.1 reshape_reshape.3.skip
  57.0 0.9 copy-done.1
  58.0 0.9 copy-done.3
  58.9 0.9 copy-done.4
  59.9 0.9 copy-done.6
  60.8 0.7 copy-done.7
  61.5 0.7 copy-done.8
  62.2 1.1 inside_span.1
  63.2 1.1 all-to-all-done.2.got
  64.4 0.0 copy-done
  64.4 0.0 copy-done.9
  64.4 0.8 apply_project.1
  65.2 0.0 copy-start.5
  65.2 8.1 %collective-permute-start.1 = (bf16[4,272,256]{2,1,0:T(8,128)(2,1)S(1)}, bf16[4,272,256]{2,1,0:T(8,128)(2,1)S(1)}, u32[]{:S(2)}, u32[]{:S(2)}) collective-permute-start(bf16[4,272,256]{2,1,0:T(8,128)(2,1)S(1)} %get-tuple-element.33), channel_id=1, source_target_pairs={{0,1},{1,0},{2,3},{3,2},{4,5},{5,4},{6,7},{7,6},{8,9},{9,8},{10,11... | collective-permute-start | bytes 1671176 | tf_op jit(solution)/shard_map/ppermute | solution.py:362
  73.3 1.6 %collective-permute-done.1 = bf16[4,272,256]{2,1,0:T(8,128)(2,1)S(1)} collective-permute-done((bf16[4,272,256]{2,1,0:T(8,128)(2,1)S(1)}, bf16[4,272,256]{2,1,0:T(8,128)(2,1)S(1)}, u32[]{:S(2)}, u32[]{:S(2)}) %collective-permute-start.1) | collective-permute-done | bytes 557088 | tf_op jit(solution)/shard_map/ppermute | solution.py:362
  74.8 1.0 add_convert_fusion
  75.8 4.2 %all-to-all-start.3 = ((bf16[4,272,256]{2,1,0:T(8,128)(2,1)}), bf16[4,272,256]{2,1,0:T(8,128)(2,1)S(1)}, u32[]{:S(2)}, u32[]{:S(2)}) async-start(bf16[4,272,256]{2,1,0:T(8,128)(2,1)} %add_convert_fusion), calls=%async_computation.3 | async-start | bytes 1114112 | tf_op jit(solution)/shard_map/all_to_all | solution.py:353
  80.0 0.8 dynamic_slice.3
  80.8 8.5 %all-to-all-done.3.got = bf16[4,272,256]{2,1,0:T(8,128)(2,1)S(1)} async-done(((bf16[4,272,256]{2,1,0:T(8,128)(2,1)}), bf16[4,272,256]{2,1,0:T(8,128)(2,1)S(1)}, u32[]{:S(2)}, u32[]{:S(2)}) %all-to-all-start.3) | async-done | bytes 557088 | tf_op jit(solution)/shard_map/all_to_all | solution.py:353
  89.3 0.4 merge.1
  89.7 2.2 %collective-permute-start.2 = (bf16[8,256]{1,0:T(8,128)(2,1)S(1)}, bf16[8,256]{1,0:T(8,128)(2,1)S(1)}, u32[]{:S(2)}, u32[]{:S(2)}) collective-permute-start(bf16[8,256]{1,0:T(8,128)(2,1)S(1)} %get-tuple-element.36), channel_id=1, source_target_pairs={{0,8},{8,16},{16,24},{24,32},{32,40},{40,48},{48,56},{56,64},{64,7... | collective-permute-start | bytes 12296 | tf_op jit(solution)/shard_map/ppermute | solution.py:358
  91.9 0.7 collective-permute-done.2
  92.7 9.7 %all_to_all.31.own = bf16[4,272,256]{2,1,0:T(8,128)(2,1)S(1)} all-to-all(bf16[4,272,256]{2,1,0:T(8,128)(2,1)S(1)} %broadcast_in_dim.7), channel_id=1, replica_groups=mesh['sp_0'=8,'sp_1'=8,'x'=4,'core'=2] {'x'}, dimensions={0} | all-to-all | bytes 1114112 | tf_op jit(solution)/shard_map/all_to_all | solution.py:353
  102.4 5.4 %collective-permute-start.3 = (bf16[4,272,256]{2,1,0:T(8,128)(2,1)S(1)}, bf16[4,272,256]{2,1,0:T(8,128)(2,1)S(1)}, u32[]{:S(2)}, u32[]{:S(2)}) collective-permute-start(bf16[4,272,256]{2,1,0:T(8,128)(2,1)S(1)} %all_to_all.31.own), channel_id=1, source_target_pairs={{0,1},{1,0},{2,3},{3,2},{4,5},{5,4},{6,7},{7,6},{8,9},{9,8},{10,11... | collective-permute-start | bytes 1671176 | tf_op jit(solution)/shard_map/ppermute | solution.py:362
  107.8 1.5 %collective-permute-done.3.other = bf16[4,272,256]{2,1,0:T(8,128)(2,1)S(1)} collective-permute-done((bf16[4,272,256]{2,1,0:T(8,128)(2,1)S(1)}, bf16[4,272,256]{2,1,0:T(8,128)(2,1)S(1)}, u32[]{:S(2)}, u32[]{:S(2)}) %collective-permute-start.3) | collective-permute-done | bytes 557088 | tf_op jit(solution)/shard_map/ppermute | solution.py:362
  109.3 3.9 %all-gather.3.cloned.1.call-done = bf16[3072,1280]{1,0:T(8,128)(2,1)} async-done(((bf16[48,1280]{1,0:T(8,128)(2,1)}), bf16[3072,1280]{1,0:T(8,128)(2,1)}) %all-gather.3.cloned.1.call-update) | async-done | bytes 7864336 | tf_op jit(solution)/shard_map/all_gather | solution.py:404
  113.2 4.7 %channel_mixer.1 = (bf16[4,256,256]{2,1,0:T(8,128)(2,1)S(1)}, bf16[256,640]{1,0:T(8,128)(2,1)S(1)}, bf16[64,16,1280]{2,1,0:T(8,128)(2,1)S(1)}) custom-call(s32[1]{0:T(128)} %bitcast.core, bf16[4,272,256]{2,1,0:T(8,128)(2,1)S(1)} %all_to_all.31.own, bf16[4,272,256]{2,1,0:T(8,128)(2,1)S(1)} %collective-permute-done.3.other, bf16[64,48,1280]{2,1,0:T(8,128)(2,1)} %bitcast.8, ...), custom_call_target="tpu_custom_call" | custom-call | tf_op jit(solution)/shard_map/channel_mixer/pallas_call | solution.py:474
  117.9 3.0 %collective-permute-start.4 = (bf16[4,256,256]{2,1,0:T(8,128)(2,1)S(1)}, bf16[4,256,256]{2,1,0:T(8,128)(2,1)S(1)}, u32[]{:S(2)}, u32[]{:S(2)}) collective-permute-start(bf16[4,256,256]{2,1,0:T(8,128)(2,1)S(1)} %get-tuple-element.40), channel_id=1, source_target_pairs={{0,1},{1,0},{2,3},{3,2},{4,5},{5,4},{6,7},{7,6},{8,9},{9,8},{10,11... | collective-permute-start | bytes 1572872 | tf_op jit(solution)/shard_map/ppermute | solution.py:362
  120.8 0.6 keep_blocks.1
  121.5 0.9 collective-permute-done.4
  122.4 0.1 add_convert_fusion.1
  122.5 12.4 %all_to_all.32.got = bf16[4,256,256]{2,1,0:T(8,128)(2,1)S(1)} all-to-all(bf16[4,256,256]{2,1,0:T(8,128)(2,1)S(1)} %add_convert_fusion.1), channel_id=1, replica_groups=mesh['sp_0'=8,'sp_1'=8,'x'=4,'core'=2] {'x'}, dimensions={0} | all-to-all | bytes 1048576 | tf_op jit(solution)/shard_map/all_to_all | solution.py:353
  134.9 0.7 finish.1
  (18 shorter events, 0.1 us)
Async XLA Ops:
  6.5 50.3 %copy-start.12 = (f32[8]{0:T(128)S(1)}, f32[8]{0:T(128)}, u32[]{:S(2)}) copy-start(f32[8]{0:T(128)} %param.22) | copy-start | bytes 100
  6.5 57.8 %copy-start = (bf16[512,2048]{1,0:T(8,128)(2,1)S(1)}, bf16[512,2048]{1,0:T(8,128)(2,1)}, u32[]{:S(2)}) copy-start(bf16[512,2048]{1,0:T(8,128)(2,1)} %weight.1) | copy-start | bytes 6291460
  6.5 57.8 %copy-start.9 = (f32[512]{0:T(512)S(1)}, f32[512]{0:T(512)}, u32[]{:S(2)}) copy-start(f32[512]{0:T(512)} %param.25) | copy-start | bytes 6148
  6.5 106.6 %all-gather.3.cloned.1.call-start = ((), (), s32[]{:S(2)}) async-start(), calls=%async_computation.6 | async-start | bytes 7987200 | tf_op jit(solution)/shard_map/all_gather | solution.py:404
  8.2 5.1 %collective-permute-start = (bf16[8,896]{1,0:T(8,128)(2,1)}, bf16[8,896]{1,0:T(8,128)(2,1)S(1)}, u32[]{:S(2)}, u32[]{:S(2)}) collective-permute-start(bf16[8,896]{1,0:T(8,128)(2,1)} %get-tuple-element.23), channel_id=1, source_target_pairs={{0,8},{8,16},{16,24},{24,32},{32,40},{40,48},{48,56},{56,64},{64,7... | collective-permute-start | bytes 43016 | tf_op jit(solution)/shard_map/ppermute | solution.py:358
  13.3 0.6 copy-start.10
  16.9 47.4 %copy-start.2 = (bf16[256,384]{1,0:T(8,128)(2,1)S(1)}, bf16[256,384]{1,0:T(8,128)(2,1)}, u32[]{:S(2)}) copy-start(bf16[256,384]{1,0:T(8,128)(2,1)} %get-tuple-element.25.keys) | copy-start | bytes 589828
  34.3 18.5 %all-to-all-start.1 = ((bf16[8,32,256]{2,1,0:T(8,128)(2,1)}), bf16[8,32,256]{2,1,0:T(8,128)(2,1)S(1)}, u32[]{:S(2)}, u32[]{:S(2)}) async-start(bf16[8,32,256]{2,1,0:T(8,128)(2,1)} %row_total.1), calls=%async_computation.1 | async-start | bytes 262144 | tf_op jit(solution)/shard_map/all_to_all | solution.py:353
  53.5 10.9 %all-to-all-start.2 = ((bf16[8,24,256]{2,1,0:T(8,128)(2,1)}), bf16[8,24,256]{2,1,0:T(8,128)(2,1)S(1)}, u32[]{:S(2)}, u32[]{:S(2)}) async-start(bf16[8,24,256]{2,1,0:T(8,128)(2,1)} %prefix.1), calls=%async_computation.2 | async-start | bytes 196608 | tf_op jit(solution)/shard_map/all_to_all | solution.py:353
  57.0 0.9 copy-start.1
  58.0 0.9 copy-start.3
  58.9 0.9 copy-start.4
  59.9 0.9 copy-start.6
  60.8 0.7 copy-start.7
  61.5 0.7 copy-start.8
  65.2 24.1 %copy-start.5 = (bf16[256,256]{1,0:T(8,128)(2,1)S(1)}, bf16[256,256]{1,0:T(8,128)(2,1)}, u32[]{:S(2)}) copy-start(bf16[256,256]{1,0:T(8,128)(2,1)} %residual.1) | copy-start | bytes 393220
  65.2 9.6 %collective-permute-start.1 = (bf16[4,272,256]{2,1,0:T(8,128)(2,1)S(1)}, bf16[4,272,256]{2,1,0:T(8,128)(2,1)S(1)}, u32[]{:S(2)}, u32[]{:S(2)}) collective-permute-start(bf16[4,272,256]{2,1,0:T(8,128)(2,1)S(1)} %get-tuple-element.33), channel_id=1, source_target_pairs={{0,1},{1,0},{2,3},{3,2},{4,5},{5,4},{6,7},{7,6},{8,9},{9,8},{10,11... | collective-permute-start | bytes 1671176 | tf_op jit(solution)/shard_map/ppermute | solution.py:362
  75.8 31.9 %copy-start.11 = (bf16[2,3,640]{2,0,1:T(2,128)(2,1)S(1)}, bf16[2,3,640]{2,0,1:T(2,128)(2,1)}, u32[]{:S(2)}) copy-start(bf16[2,3,640]{2,0,1:T(2,128)(2,1)} %param.30) | copy-start | bytes 23044
  75.8 13.4 %all-to-all-start.3 = ((bf16[4,272,256]{2,1,0:T(8,128)(2,1)}), bf16[4,272,256]{2,1,0:T(8,128)(2,1)S(1)}, u32[]{:S(2)}, u32[]{:S(2)}) async-start(bf16[4,272,256]{2,1,0:T(8,128)(2,1)} %add_convert_fusion), calls=%async_computation.3 | async-start | bytes 1114112 | tf_op jit(solution)/shard_map/all_to_all | solution.py:353
  89.7 2.9 %collective-permute-start.2 = (bf16[8,256]{1,0:T(8,128)(2,1)S(1)}, bf16[8,256]{1,0:T(8,128)(2,1)S(1)}, u32[]{:S(2)}, u32[]{:S(2)}) collective-permute-start(bf16[8,256]{1,0:T(8,128)(2,1)S(1)} %get-tuple-element.36), channel_id=1, source_target_pairs={{0,8},{8,16},{16,24},{24,32},{32,40},{40,48},{48,56},{56,64},{64,7... | collective-permute-start | bytes 12296 | tf_op jit(solution)/shard_map/ppermute | solution.py:358
  102.4 6.9 %collective-permute-start.3 = (bf16[4,272,256]{2,1,0:T(8,128)(2,1)S(1)}, bf16[4,272,256]{2,1,0:T(8,128)(2,1)S(1)}, u32[]{:S(2)}, u32[]{:S(2)}) collective-permute-start(bf16[4,272,256]{2,1,0:T(8,128)(2,1)S(1)} %all_to_all.31.own), channel_id=1, source_target_pairs={{0,1},{1,0},{2,3},{3,2},{4,5},{5,4},{6,7},{7,6},{8,9},{9,8},{10,11... | collective-permute-start | bytes 1671176 | tf_op jit(solution)/shard_map/ppermute | solution.py:362
  117.9 4.5 %collective-permute-start.4 = (bf16[4,256,256]{2,1,0:T(8,128)(2,1)S(1)}, bf16[4,256,256]{2,1,0:T(8,128)(2,1)S(1)}, u32[]{:S(2)}, u32[]{:S(2)}) collective-permute-start(bf16[4,256,256]{2,1,0:T(8,128)(2,1)S(1)} %get-tuple-element.40), channel_id=1, source_target_pairs={{0,1},{1,0},{2,3},{3,2},{4,5},{5,4},{6,7},{7,6},{8,9},{9,8},{10,11... | collective-permute-start | bytes 1572872 | tf_op jit(solution)/shard_map/ppermute | solution.py:362
Sparse Core Ops, SparseCore 0:
  10.3 102.7 all-gather.2
